TPU v7x, 512 devices: a whole 4x4x16 slice. The times are simulated.
512 devices in a mesh: ep: 32 (over z, core), tp: 16 (over y, x).
Axes of the slice: x: 4, y: 4, z: 16, core: 2. Of those that a mesh axis runs over, the one named last changes fastest.
Arguments:
- mixer_input: bfloat16 [8192, 2048], P('ep'), may hold values from -6 to 6
- mixer_gain: float32 [2048], replicated, may hold values from 0.1 to 1.9
- query_weight: bfloat16 [2048, 2048], P(None, 'tp'), may hold values from -0.13258252 to 0.13258252
- key_weight: bfloat16 [2048, 1024], P(None, 'tp'), may hold values from -2.78423295 to 2.78423295
- value_weight: bfloat16 [2048, 1024], P(None, 'tp'), may hold values from -0.125 to 0.125
- output_weight: bfloat16 [2048, 2048], P(None, 'tp'), may hold values from -1 to 1
- sink_logit: float32 [32], P('tp'), may hold values from 2 to 7
- expert_input: bfloat16 [4096, 2048], P('ep'), may hold values from -6 to 6
- expert_gain: float32 [2048], replicated, may hold values from 0.1 to 1.9
- routes: int32 [4096, 4], P('ep'), may hold values from 0 to 31, all different within a row; in each aligned block of 128 rows (0 to 127, 128 to 255, ...) at most 32 rows name the same one
- route_logits: float32 [4096, 4], P('ep'), may hold values from -6 to 6
- gate_weight: bfloat16 [32, 2048, 2048], P('ep', None, 'tp'), may hold values from -0.375 to 0.375
- up_weight: bfloat16 [32, 2048, 2048], P('ep', None, 'tp'), may hold values from -0.375 to 0.375
- down_weight: bfloat16 [32, 2048, 2048], P('ep', None, 'tp'), may hold values from -0.03125 to 0.03125
Outputs:
- mixer_output: bfloat16 [8192, 2048], P('ep', 'tp')
- expert_output: bfloat16 [4096, 2048], P('ep', 'tp')
Inputs may be any that keep to these rules, and one draw needn't show every extreme that they name: `routes`: each token names 4 different experts. Among the 128 tokens of one index of ep (aligned blocks) no expert is named more than 32 times, and in some blocks one expert is named exactly 32 times.
All inputs are finite; a program needn't handle non-finite values.
Results may differ from a plain program's by a relative error of at most 0.0055.
The roundings to bfloat16 on the way count: a program that leaves them out, or rounds other values in their place, can miss the bound.
Values may be sent and summed in bfloat16 or wider, within the bound.
No kernel may reach another device: no remote copies, remote signals or barrier semaphores. Data moves between devices by JAX's collectives and lax.ppermute only.
A program may use at most 64 MiB of HBM per device.

v0:
```python
import itertools

import jax
import jax.numpy as jnp
from jax import lax
from jax.experimental import pallas as pl
from jax.experimental.pallas import tpu as pltpu
from jax.sharding import Mesh
from jax.sharding import PartitionSpec as P

HEAD_DIM = 64
TOP_K = 4
WINDOW = 128
GRID_W = 64
EP = ("ep_0", "ep_1")
TP = ("Y", "h", "X", "p")

EPSILON = 1e-06
LIMIT = 7.0
SLOPE = 1.702
BASE = 10000.0


def swap(pieces, axis):
    return lax.all_to_all(pieces, axis, 0, 0, tiled=True)


def spread(shard, axis):
    return swap(jnp.broadcast_to(shard[None], (lax.axis_size(axis), *shard.shape)), axis)


def activate(gate, up):
    capped = jnp.minimum(gate, LIMIT)
    bounded = jnp.clip(up, -LIMIT, LIMIT)
    return (capped * jax.nn.sigmoid(SLOPE * capped) * (bounded + 1.0)).astype(jnp.bfloat16)


def dot(a, b):
    return jnp.dot(a, b, preferred_element_type=jnp.float32)


def tall(wide):
    k, n = wide.shape
    square = jnp.concatenate([wide, jnp.zeros((n - k, n), wide.dtype)], axis=0)
    return square.T


def dispatch(rows, gain, routes, experts, slots, width):
    tokens = rows.shape[0]
    pairs = experts // 2

    def kernel(rows_ref, gain_ref, routes_ref, out_ref, target_ref):
        block = 2 * lax.axis_index("Y") + lax.axis_index("X")
        values = rows_ref[...].astype(jnp.float32)
        scale = lax.rsqrt(jnp.mean(values * values, axis=-1, keepdims=True) + EPSILON)
        start = pl.multiple_of(block * width, width)
        own = rows_ref[:, pl.ds(start, width)].astype(jnp.float32)
        normed = (own * scale * gain_ref[:, pl.ds(start, width)]).astype(jnp.bfloat16)
        first = lax.broadcasted_iota(jnp.int32, (tokens, tokens), 0)
        second = lax.broadcasted_iota(jnp.int32, (tokens, tokens), 1)
        parity = lax.axis_index("p")
        expert = lax.broadcasted_iota(jnp.int32, (pairs, tokens), 0) * 2 + parity
        named = jnp.zeros((pairs, tokens), jnp.float32)
        for k in range(TOP_K):
            named = named + (routes_ref[k : k + 1, :] == expert).astype(jnp.float32)
        earlier = dot(named.astype(jnp.bfloat16), (first < second).astype(jnp.bfloat16))
        rank = jnp.where(named > 0.0, earlier.astype(jnp.int32), -1)
        rank = rank - lax.axis_index("h") * (2 * slots)
        slot = lax.broadcasted_iota(jnp.int32, (pairs, 2 * slots, tokens), 1)
        chosen = (rank[:, None, :] == slot).astype(jnp.float32)
        chosen = chosen.reshape(experts * slots, tokens).astype(jnp.bfloat16)
        out_ref[...] = dot(chosen, normed).astype(jnp.bfloat16)
        routed = tall(routes_ref[...].astype(jnp.float32))
        column = lax.broadcasted_iota(jnp.int32, (tokens, experts), 1)
        wanted = column.astype(jnp.float32)
        marks = [(routed[:, k : k + 1] == wanted).astype(jnp.float32) for k in range(TOP_K)]
        before = dot((second < first).astype(jnp.bfloat16), sum(marks).astype(jnp.bfloat16))
        before = before.astype(jnp.int32)
        core, half, spot = (before // slots) % 2, before // (2 * slots), before % slots
        position = (((column // 2) * 2 + core) * 2 + half) * 2 + column % 2
        position = (position * slots + spot).astype(jnp.float32)
        target_ref[...] = jnp.concatenate(
            [jnp.sum(mark * position, axis=1, keepdims=True) for mark in marks], axis=1
        ).astype(jnp.int32)

    vmem = pl.BlockSpec(memory_space=pltpu.VMEM)
    return pl.pallas_call(
        kernel,
        out_shape=(
            jax.ShapeDtypeStruct((experts * slots, width), jnp.bfloat16),
            jax.ShapeDtypeStruct((tokens, TOP_K), jnp.int32),
        ),
        in_specs=[vmem] * 3,
        out_specs=(vmem, vmem),
        name="dispatch",
    )(rows, gain[None, :], routes.T)


def device_pairs(where):
    names = list(itertools.product(range(2), repeat=5))
    number = {name: i for i, name in enumerate(names)}
    return [(number[n], number[where(*n)]) for n in names if where(*n) is not None]


def gather_shares(own):
    axes = ("ep_1", "Y", "h", "X", "p")

    def outer(c, Y, h, X, p):
        return (c, Y, 1 - h, X, p) if c == p else (1 - c, Y, h, X, 1 - p)

    def cross(c, Y, h, X, p):
        return (1 - c, Y, h, X, p) if c == p else (c, Y, 1 - h, X, 1 - p)

    def trade(c, Y, h, X, p):
        return (1 - c, Y, h, X, p)

    def give(c, Y, h, X, p):
        return (1 - c, Y, h, X, p) if c == p else None

    first = lax.ppermute(own, axes, device_pairs(outer))
    second = lax.ppermute(own, axes, device_pairs(cross))
    third = lax.ppermute(first, axes, device_pairs(trade))
    fourth = lax.ppermute(second, axes, device_pairs(give))
    return own, first, second, third, fourth


def share_order():
    c, h, p = (lax.axis_index(a) for a in ("ep_1", "h", "p"))
    native = c == p
    own, up = 2 * h + p, 2 * (1 - h) + p
    side, across = 2 * h + (1 - p), 2 * (1 - h) + (1 - p)
    return native, [own, jnp.where(native, up, side), across, jnp.where(native, side, up)]


def copy_share(native, shares, index, start, size, target, sem):
    own, first, second, third, fourth = shares
    rows = pl.ds(start, size)
    if index in (1, 3):
        source = first if index == 1 else third
        pltpu.make_async_copy(source.at[rows], target, sem).start()
        return
    here, there = (own, second) if index == 0 else (second, fourth)

    @pl.when(native)
    def _():
        pltpu.make_async_copy(here.at[rows], target, sem).start()

    @pl.when(jnp.logical_not(native))
    def _():
        pltpu.make_async_copy(there.at[rows], target, sem).start()


def gated(rows, mixed, shares):
    parts, n, k = rows.shape
    u = shares[0].shape[1]
    j = mixed.shape[1]
    whole = parts * k

    def kernel(rows_ref, mixed_ref, *refs):
        shares, (out_ref, weights_ref, sems) = refs[:5], refs[5:]
        native, order = share_order()
        targets = [
            (weights_ref.at[i, :, pl.ds(side * u, u)], sems.at[i, side])
            for i in range(4)
            for side in range(2)
        ]
        for i in range(4):
            for side in range(2):
                target, sem = targets[2 * i + side]
                copy_share(native, shares, i, side * whole, whole, target, sem)
        for copy in range(parts):
            out_ref[copy, :, 4 * u :] = mixed_ref[...]
        for i in range(4):
            for side in range(2):
                target, sem = targets[2 * i + side]
                pltpu.make_async_copy(shares[1].at[pl.ds(0, whole)], target, sem).wait()
            total = dot(rows_ref[0], weights_ref[i, :k, :])
            for part in range(1, parts):
                total = total + dot(rows_ref[part], weights_ref[i, part * k : (part + 1) * k, :])
            hidden = activate(total[:, :u], total[:, u:])
            lane = pl.multiple_of(order[i] * u, u)
            for copy in range(parts):
                out_ref[copy, :, pl.ds(lane, u)] = hidden

    vmem = pl.BlockSpec(memory_space=pltpu.VMEM)
    anywhere = pl.BlockSpec(memory_space=pl.ANY)
    return pl.pallas_call(
        kernel,
        out_shape=jax.ShapeDtypeStruct((parts, n, 4 * u + j), jnp.bfloat16),
        in_specs=[vmem, vmem] + [anywhere] * 5,
        out_specs=vmem,
        scratch_shapes=[
            pltpu.VMEM((4, whole, 2 * u), jnp.bfloat16),
            pltpu.SemaphoreType.DMA((4, 2)),
        ],
        name="gated",
    )(rows, mixed, *shares)


def lowered(hidden, shares, slots):
    parts, n, _ = hidden.shape
    f = shares[0].shape[1]
    k = 4 * f
    whole = parts * k
    half = k // 2

    def kernel(hidden_ref, *refs):
        shares, (out_ref, weights_ref, sems) = refs[:5], refs[5:]
        native, order = share_order()
        targets = [
            (weights_ref.at[i // 2, :, pl.ds((i % 2) * f, f)], sems.at[i]) for i in range(4)
        ]
        for i in range(4):
            copy_share(native, shares, i, 2 * whole, whole, *targets[i])
        for pair in range(2):
            for i in (2 * pair, 2 * pair + 1):
                pltpu.make_async_copy(shares[1].at[pl.ds(0, whole)], *targets[i]).wait()
            total = jnp.zeros((n, 2 * f), jnp.float32)
            for Y, X, h in itertools.product(range(2), repeat=3):
                unit = (8 * Y + 4 * h + 2 * X) * f
                piece = hidden_ref[2 * Y + X, :, h * half : (h + 1) * half]
                total = total + dot(piece, weights_ref[pair, unit : unit + half, :])
            rounded = total.astype(jnp.bfloat16).reshape(n // slots, slots, 2 * f)
            out_ref[:, order[2 * pair]] = rounded[:, :, :f]
            out_ref[:, order[2 * pair + 1]] = rounded[:, :, f:]

    vmem = pl.BlockSpec(memory_space=pltpu.VMEM)
    anywhere = pl.BlockSpec(memory_space=pl.ANY)
    return pl.pallas_call(
        kernel,
        out_shape=jax.ShapeDtypeStruct((n // slots, 4, slots, f), jnp.bfloat16),
        in_specs=[vmem] + [anywhere] * 5,
        out_specs=vmem,
        scratch_shapes=[
            pltpu.VMEM((2, whole, 2 * f), jnp.bfloat16),
            pltpu.SemaphoreType.DMA((4,)),
        ],
        name="lowered",
    )(hidden, *shares)


def combine(results, target, chances):
    slots, f = results.shape
    tokens = target.shape[0]

    def kernel(results_ref, target_ref, chances_ref, out_ref):
        chances = tall(chances_ref[...])
        lane = lax.broadcasted_iota(jnp.int32, (tokens, slots), 1)
        total = jnp.zeros((tokens, f), jnp.float32)
        for k in range(TOP_K):
            chosen = (target_ref[:, k : k + 1] == lane).astype(jnp.float32).astype(jnp.bfloat16)
            total = total + dot(chosen, results_ref[...]) * chances[:, k : k + 1]
        out_ref[...] = total.astype(jnp.bfloat16)

    vmem = pl.BlockSpec(memory_space=pltpu.VMEM)
    return pl.pallas_call(
        kernel,
        out_shape=jax.ShapeDtypeStruct((tokens, f), jnp.bfloat16),
        in_specs=[vmem] * 3,
        out_specs=vmem,
        name="combine",
    )(results, target, chances)


def rotary_tables(places, width):
    quarter = HEAD_DIM // 4
    lane = jnp.arange(width, dtype=jnp.int32)
    frequency = BASE ** (-(lane % quarter).astype(jnp.float32) / quarter)
    row = (places // GRID_W).astype(jnp.float32)[:, None]
    column = (places % GRID_W).astype(jnp.float32)[:, None]
    angle = jnp.where(lane % HEAD_DIM < HEAD_DIM // 2, row, column) * frequency
    sign = jnp.where(lane % (2 * quarter) < quarter, -1.0, 1.0)
    return jnp.cos(angle), jnp.sin(angle) * sign


def projections(rows, gain, query_weight, key_weight, value_weight, places):
    tokens, _ = rows.shape
    width = query_weight.shape[1]
    half = width // 2
    quarter = HEAD_DIM // 4
    cosine, sine = rotary_tables(places, width)

    def kernel(
        rows_ref, gain_ref, query_ref, key_ref, value_ref, cos_ref, sin_ref, out_ref, *pair_refs
    ):
        values = rows_ref[...].astype(jnp.float32)
        scale = lax.rsqrt(jnp.mean(values * values, axis=-1, keepdims=True) + EPSILON)
        normed = (values * scale * gain_ref[...]).astype(jnp.bfloat16)
        lane = lax.broadcasted_iota(jnp.int32, (tokens, width), 1) % (2 * quarter)

        def turned(a):
            partner = jnp.where(
                lane < quarter,
                pltpu.roll(a, width - quarter, 1),
                pltpu.roll(a, quarter, 1),
            )
            return (a * cos_ref[...] + partner * sin_ref[...]).astype(jnp.bfloat16)

        def flipped(weight_ref):
            return lax.dot_general(
                normed, weight_ref[...], (((1,), (1,)), ((), ())), preferred_element_type=jnp.float32
            )

        out_ref[...] = turned(dot(normed, query_ref[...]))
        keys, mine = flipped(key_ref), flipped(value_ref)
        both = jnp.concatenate([keys, mine], axis=1)
        rounded = jnp.where(
            lax.broadcasted_iota(jnp.int32, (tokens, width), 1) < half,
            turned(both),
            both.astype(jnp.bfloat16),
        )
        for i, ref in enumerate(pair_refs):
            ref[...] = rounded[i * WINDOW : (i + 1) * WINDOW]

    vmem = pl.BlockSpec(memory_space=pltpu.VMEM)
    return pl.pallas_call(
        kernel,
        out_shape=[jax.ShapeDtypeStruct((tokens, width), jnp.bfloat16)]
        + [jax.ShapeDtypeStruct((WINDOW, width), jnp.bfloat16)] * (tokens // WINDOW),
        in_specs=[vmem] * 7,
        out_specs=[vmem] * (1 + tokens // WINDOW),
        name="projections",
    )(rows, gain[None, :], query_weight, key_weight.T, value_weight.T, cosine, sine)


def banded(query, pieces, sinks):
    tokens, width = query.shape
    blocks = tokens // WINDOW
    heads = width // HEAD_DIM

    def kernel(sink_ref, query_ref, *refs):
        piece_refs, out_ref = refs[:-1], refs[-1]
        place, last = lax.axis_index(EP), lax.axis_size(EP) - 1
        row = lax.broadcasted_iota(jnp.int32, (WINDOW, 3 * WINDOW), 0)
        column = lax.broadcasted_iota(jnp.int32, (WINDOW, 3 * WINDOW), 1)
        band = (column >= row) & (column <= row + 2 * WINDOW)
        for n in range(blocks):
            near = jnp.concatenate([piece_refs[n + i][...] for i in range(3)], axis=0)
            keys, values = near[:, :HEAD_DIM], near[:, HEAD_DIM:]
            least = jnp.where(place == 0, WINDOW, 0) if n == 0 else 0
            most = jnp.where(place == last, 2 * WINDOW, 3 * WINDOW) if n == blocks - 1 else 3 * WINDOW
            allowed = band & (column >= least) & (column < most)
            outs = []
            for r in range(heads):
                here = query_ref[n * WINDOW : (n + 1) * WINDOW, r * HEAD_DIM : (r + 1) * HEAD_DIM]
                scores = lax.dot_general(
                    here, keys, (((1,), (1,)), ((), ())), preferred_element_type=jnp.float32
                )
                scores = jnp.where(allowed, scores * HEAD_DIM ** (-0.5), -1e30)
                sink = sink_ref[r]
                top = jnp.maximum(jnp.max(scores, axis=-1, keepdims=True), sink)
                weights = jnp.exp(scores - top)
                total = jnp.sum(weights, axis=-1, keepdims=True) + jnp.exp(sink - top)
                outs.append(dot((weights / total).astype(jnp.bfloat16), values))
            mixed = jnp.concatenate(outs, axis=1).astype(jnp.bfloat16)
            out_ref[n * WINDOW : (n + 1) * WINDOW, :] = mixed

    vmem = pl.BlockSpec(memory_space=pltpu.VMEM)
    return pl.pallas_call(
        kernel,
        out_shape=jax.ShapeDtypeStruct((tokens, width), jnp.bfloat16),
        in_specs=[pl.BlockSpec(memory_space=pltpu.SMEM)] + [vmem] * (blocks + 3),
        out_specs=vmem,
        name="banded",
    )(sinks, query, *pieces)


def attention(mixer_input, mixer_gain, query_weight, key_weight, value_weight, sink_logit):
    tokens = mixer_input.shape[0]
    places = lax.axis_index(EP) * tokens + jnp.arange(tokens, dtype=jnp.int32)
    query, *pieces = projections(
        mixer_input, mixer_gain, query_weight, key_weight, value_weight, places
    )
    up = [(i, i + 1) for i in range(lax.axis_size(EP) - 1)]
    before = lax.ppermute(pieces[-1], EP, up)
    after = lax.ppermute(pieces[0], EP, [(j, i) for i, j in up])
    return banded(query, [before, *pieces, after], sink_logit)


def projected(heads, weight):
    _, n, j = heads[0].shape
    f = weight.shape[1]

    def kernel(*refs):
        heads_refs, weight_ref, out_ref = refs[:4], refs[4], refs[5]
        total = jnp.zeros((n, f), jnp.float32)
        for k in range(4):
            h, p = lax.axis_index("h") ^ (k // 2), lax.axis_index("p") ^ (k % 2)
            for Y, X in itertools.product(range(2), repeat=2):
                unit = pl.multiple_of((8 * Y + 4 * h + 2 * X + p) * j, j)
                total = total + dot(heads_refs[k][2 * Y + X], weight_ref[pl.ds(unit, j), :])
        out_ref[...] = total.astype(jnp.bfloat16)

    vmem = pl.BlockSpec(memory_space=pltpu.VMEM)
    return pl.pallas_call(
        kernel,
        out_shape=jax.ShapeDtypeStruct((n, f), jnp.bfloat16),
        in_specs=[vmem] * 5,
        out_specs=vmem,
        name="projected",
    )(*heads, weight)


def shards(
    mixer_input,
    mixer_gain,
    query_weight,
    key_weight,
    value_weight,
    output_weight,
    sink_logit,
    expert_input,
    expert_gain,
    routes,
    route_logits,
    gate_weight,
    up_weight,
    down_weight,
):
    experts = lax.axis_size(EP)
    rows_here, features = expert_input.shape
    slots = 2 * rows_here * TOP_K // experts // 4
    width = features // 4
    own = jnp.concatenate([gate_weight[0], up_weight[0], down_weight[0]], axis=0)
    shares = gather_shares(own)
    outgoing, target = dispatch(expert_input, expert_gain, routes, experts, slots, width)
    received = swap(outgoing.reshape(experts, slots, width), EP)
    mixed = attention(mixer_input, mixer_gain, query_weight, key_weight, value_weight, sink_logit)
    rows = spread(received.reshape(experts * slots, width), ("Y", "X"))
    inner = gated(rows, mixed, shares)
    beside = swap(inner, ("Y", "X"))
    chances = jax.nn.softmax(route_logits.T, axis=0)
    result = lowered(beside, shares, slots)
    returned = swap(result.reshape(4 * experts, slots, -1), (*EP, "h", "p"))
    heads = beside[:, :, width:]
    heads = [heads] + [
        lax.ppermute(heads, ("h", "p"), [(i, i ^ k) for i in range(4)])
        for k in range(1, 4)
    ]
    mixer_output = projected(heads, output_weight)
    expert_output = combine(
        returned.reshape(experts * 4 * slots, -1), target, chances
    )
    return (mixer_output, expert_output)


def solution(mesh):
    names = ("ep_0", "ep_1", "Y", "h", "X", "p")
    finer = Mesh(mesh.devices.reshape(16, 2, 2, 2, 2, 2), names)
    in_specs = (
        P(EP, None),
        P(),
        P(None, TP),
        P(None, TP),
        P(None, TP),
        P(None, TP),
        P(TP),
        P(EP, None),
        P(),
        P(EP, None),
        P(EP, None),
        P(EP, None, TP),
        P(EP, None, TP),
        P(EP, None, TP),
    )
    out_specs = (P(EP, TP), P(EP, TP))
    return jax.shard_map(
        shards, mesh=finer, in_specs=in_specs, out_specs=out_specs, check_vma=False
    )
```

profile of v0, /device:TPU:1, one launch (start us, length us, event | category | flops | bytes accessed | tf_op | source)
XLA Modules:
  0.0 156.1 jit_solution(15303319979829296479)
XLA Ops:
  0.6 1.5 pad_maximum_fusion.refs_0_
  2.1 0.0 copy-start
  2.1 4.5 %collective-permute-start.2 = (bf16[6144,128]{1,0:T(8,128)(2,1)S(1)}, bf16[6144,128]{1,0:T(8,128)(2,1)S(1)}, u32[]{:S(2)}, u32[]{:S(2)}) collective-permute-start(bf16[6144,128]{1,0:T(8,128)(2,1)S(1)} %pad_maximum_fusion.refs_0_), channel_id=1, source_target_pairs={{0,4},{1,16},{2,6},{3,18},{4,0},{5,20},{6,2},{7,22},{8,12},{9,24},... | collective-permute-start | bytes 4718600 | tf_op jit(solution)/shard_map/ppermute | solution.py:120
  6.6 2.5 %collective-permute-start.3 = (bf16[6144,128]{1,0:T(8,128)(2,1)S(1)}, bf16[6144,128]{1,0:T(8,128)(2,1)}, u32[]{:S(2)}, u32[]{:S(2)}) collective-permute-start(bf16[6144,128]{1,0:T(8,128)(2,1)S(1)} %pad_maximum_fusion.refs_0_), channel_id=1, source_target_pairs={{0,16},{1,4},{2,18},{3,6},{4,20},{5,0},{6,22},{7,2},{8,24},{9,12},... | collective-permute-start | bytes 4718600 | tf_op jit(solution)/shard_map/ppermute | solution.py:121
  9.1 2.5 %dispatch.1 = (bf16[256,512]{1,0:T(8,128)(2,1)}, s32[128,4]{1,0:T(8,128)}) custom-call(bf16[128,2048]{1,0:T(8,128)(2,1)} %rows_ref.2, f32[1,2048]{1,0:T(1,128)} %bitcast.23, s32[4,128]{1,0:T(4,128)} %bitcast.25), custom_call_target="tpu_custom_call" | custom-call | tf_op jit(solution)/shard_map/dispatch/pallas_call | solution.py:87
  11.7 15.4 %all-to-all-start = ((bf16[32,8,512]{2,1,0:T(8,128)(2,1)}), bf16[32,8,512]{2,1,0:T(8,128)(2,1)S(1)}, u32[]{:S(2)}, u32[]{:S(2)}) async-start(bf16[32,8,512]{2,1,0:T(8,128)(2,1)} %bitcast.22), calls=%async_computation | async-start | bytes 524288 | tf_op jit(solution)/shard_map/all_to_all | solution.py:25
  27.0 0.0 collective-permute-done.2.refs_1_
  27.0 0.0 copy-start.1
  27.0 23.0 %collective-permute-start.4 = (bf16[6144,128]{1,0:T(8,128)(2,1)S(1)}, bf16[6144,128]{1,0:T(8,128)(2,1)}, u32[]{:S(2)}, u32[]{:S(2)}) collective-permute-start(bf16[6144,128]{1,0:T(8,128)(2,1)S(1)} %collective-permute-done.2.refs_1_), channel_id=1, source_target_pairs={{0,16},{1,17},{2,18},{3,19},{4,20},{5,21},{6,22},{7,23},{8,24},{9,... | collective-permute-start | bytes 4718600 | tf_op jit(solution)/shard_map/ppermute | solution.py:122
  50.0 0.0 collective-permute-done.3.refs_2_
  50.0 1.3 collective-permute-start.5
  51.3 0.0 all-to-all-done
  51.3 1.0 broadcast_in_dim.49
  52.4 0.0 copy-done
  52.4 0.0 copy-done.1
  52.4 4.3 %all-to-all-start.1 = ((bf16[4,256,512]{2,1,0:T(8,128)(2,1)}), bf16[4,256,512]{2,1,0:T(8,128)(2,1)}, u32[]{:S(2)}, u32[]{:S(2)}) async-start(bf16[4,256,512]{2,1,0:T(8,128)(2,1)} %broadcast_in_dim.49), calls=%async_computation.1 | async-start | bytes 2097152 | tf_op jit(solution)/shard_map/all_to_all | solution.py:25
  56.7 1.3 sine_multiply_fusion
  58.0 3.6 %projections.1 = (bf16[256,128]{1,0:T(8,128)(2,1)}, bf16[128,128]{1,0:T(8,128)(2,1)}, bf16[128,128]{1,0:T(8,128)(2,1)}) custom-call(bf16[256,2048]{1,0:T(8,128)(2,1)} %rows_ref.3, f32[1,2048]{1,0:T(1,128)} %bitcast.24, bf16[2048,128]{1,0:T(8,128)(2,1)} %query_ref.1, bf16[64,2048]{1,0:T(8,128)(2,1)} %bitcast.20, bf16[64,2048]{1,0:T(8,128)(2,1)} %bitcast.21, ...), custom_call_target="tpu_custom_call" | custom-call | tf_op jit(solution)/shard_map/projections/pallas_call | solution.py:316
  61.6 2.5 %collective-permute-start = (bf16[128,128]{1,0:T(8,128)(2,1)}, bf16[128,128]{1,0:T(8,128)(2,1)S(1)}, u32[]{:S(2)}, u32[]{:S(2)}) collective-permute-start(bf16[128,128]{1,0:T(8,128)(2,1)} %get-tuple-element.9.refs_2_), channel_id=1, source_target_pairs={{0,16},{16,32},{32,48},{48,64},{64,80},{80,96},{96,112},{112,128},... | collective-permute-start | bytes 98312 | tf_op jit(solution)/shard_map/ppermute | solution.py:375
  64.1 3.0 %collective-permute-start.1 = (bf16[128,128]{1,0:T(8,128)(2,1)}, bf16[128,128]{1,0:T(8,128)(2,1)S(1)}, u32[]{:S(2)}, u32[]{:S(2)}) collective-permute-start(bf16[128,128]{1,0:T(8,128)(2,1)} %get-tuple-element.10.refs_1_), channel_id=1, source_target_pairs={{16,0},{32,16},{48,32},{64,48},{80,64},{96,80},{112,96},{128,112},... | collective-permute-start | bytes 98312 | tf_op jit(solution)/shard_map/ppermute | solution.py:376
  67.1 0.0 collective-permute-done.refs_0_
  67.1 0.0 copy-start.7
  67.1 2.9 %collective-permute-done.1.refs_3_ = bf16[128,128]{1,0:T(8,128)(2,1)S(1)} collective-permute-done((bf16[128,128]{1,0:T(8,128)(2,1)}, bf16[128,128]{1,0:T(8,128)(2,1)S(1)}, u32[]{:S(2)}, u32[]{:S(2)}) %collective-permute-start.1) | collective-permute-done | bytes 32800 | tf_op jit(solution)/shard_map/ppermute | solution.py:376
  69.9 0.0 copy-done.7
  70.0 0.6 copy-done.8
  70.6 3.2 %banded.1.mixed_ref = bf16[256,128]{1,0:T(8,128)(2,1)} custom-call(f32[2]{0:T(128)} %sink_ref.1, bf16[256,128]{1,0:T(8,128)(2,1)} %get-tuple-element.8.query_ref, bf16[128,128]{1,0:T(8,128)(2,1)} %copy-done.7, bf16[128,128]{1,0:T(8,128)(2,1)} %get-tuple-element.10.refs_1_, bf16[128,128]{1,0:T(8,128)(2,1)} %get-tuple-element.9.refs_2_, bf16[128,128]{1,0:T(8,128)(2,1)} %copy-done.8), custom_call_target="tpu_custom_call" | custom-call | tf_op jit(solution)/shard_map/banded/pallas_call | solution.py:359
  73.7 0.0 all-to-all-done.1.rows_ref
  73.7 0.0 collective-permute-done.4.refs_3_
  73.7 0.0 collective-permute-done.5.refs_4_
  73.7 6.4 %gated.1 = bf16[4,256,640]{2,1,0:T(8,128)(2,1)} custom-call(bf16[4,256,512]{2,1,0:T(8,128)(2,1)} %all-to-all-done.1.rows_ref, bf16[256,128]{1,0:T(8,128)(2,1)} %banded.1.mixed_ref, bf16[6144,128]{1,0:T(8,128)(2,1)} %copy-done, bf16[6144,128]{1,0:T(8,128)(2,1)} %copy-done.1, bf16[6144,128]{1,0:T(8,128)(2,1)} %collective-permute-done.3.refs_2_, ...), custom_call_target="tpu_custom_call" | custom-call | tf_op jit(solution)/shard_map/gated/pallas_call | solution.py:187
  80.1 26.5 %all_to_all.20.hidden_ref = bf16[4,256,640]{2,1,0:T(8,128)(2,1)} all-to-all(bf16[4,256,640]{2,1,0:T(8,128)(2,1)} %gated.1), channel_id=1, replica_groups=mesh['ep_0'=16,'ep_1'=2,'Y'=2,'h'=2,'X'=2,'p'=2] {'Y','X'}, dimensions={0} | all-to-all | bytes 2621440 | tf_op jit(solution)/shard_map/all_to_all | solution.py:25
  106.6 4.6 %lowered.1 = bf16[32,4,8,128]{3,2,1,0:T(8,128)(2,1)} custom-call(bf16[4,256,640]{2,1,0:T(8,128)(2,1)} %all_to_all.20.hidden_ref, bf16[6144,128]{1,0:T(8,128)(2,1)} %copy-done, bf16[6144,128]{1,0:T(8,128)(2,1)} %copy-done.1, bf16[6144,128]{1,0:T(8,128)(2,1)} %collective-permute-done.3.refs_2_, bf16[6144,128]{1,0:T(8,128)(2,1)} %collective-permute-done.4.refs_3_, ...), custom_call_target="tpu_custom_call" | custom-call | tf_op jit(solution)/shard_map/lowered/pallas_call | solution.py:229
  111.2 17.2 %all-to-all-start.3 = ((bf16[128,8,128]{2,1,0:T(8,128)(2,1)}), bf16[128,8,128]{2,1,0:T(8,128)(2,1)S(1)}, u32[]{:S(2)}, u32[]{:S(2)}) async-start(bf16[128,8,128]{2,1,0:T(8,128)(2,1)} %bitcast.14), calls=%async_computation.3 | async-start | bytes 524288 | tf_op jit(solution)/shard_map/all_to_all | solution.py:25
  128.5 1.0 slice.4.refs_0_
  129.5 3.3 %collective-permute-start.6 = (bf16[4,256,128]{2,1,0:T(8,128)(2,1)S(1)}, bf16[4,256,128]{2,1,0:T(8,128)(2,1)S(1)}, u32[]{:S(2)}, u32[]{:S(2)}) collective-permute-start(bf16[4,256,128]{2,1,0:T(8,128)(2,1)S(1)} %slice.4.refs_0_), channel_id=1, source_target_pairs={{0,1},{1,0},{4,5},{5,4},{2,3},{3,2},{6,7},{7,6},{8,9},{9,8},{12,13... | collective-permute-start | bytes 786440 | tf_op jit(solution)/shard_map/ppermute | solution.py:437
  132.7 3.1 %collective-permute-start.7 = (bf16[4,256,128]{2,1,0:T(8,128)(2,1)S(1)}, bf16[4,256,128]{2,1,0:T(8,128)(2,1)S(1)}, u32[]{:S(2)}, u32[]{:S(2)}) collective-permute-start(bf16[4,256,128]{2,1,0:T(8,128)(2,1)S(1)} %slice.4.refs_0_), channel_id=1, source_target_pairs={{0,4},{1,5},{4,0},{5,1},{2,6},{3,7},{6,2},{7,3},{8,12},{9,13},{12,... | collective-permute-start | bytes 786440 | tf_op jit(solution)/shard_map/ppermute | solution.py:437
  135.8 2.0 %collective-permute-start.8 = (bf16[4,256,128]{2,1,0:T(8,128)(2,1)S(1)}, bf16[4,256,128]{2,1,0:T(8,128)(2,1)S(1)}, u32[]{:S(2)}, u32[]{:S(2)}) collective-permute-start(bf16[4,256,128]{2,1,0:T(8,128)(2,1)S(1)} %slice.4.refs_0_), channel_id=1, source_target_pairs={{0,5},{1,4},{4,1},{5,0},{2,7},{3,6},{6,3},{7,2},{8,13},{9,12},{12,... | collective-permute-start | bytes 786440 | tf_op jit(solution)/shard_map/ppermute | solution.py:437
  137.9 0.6 divide_bitcast_fusion.chances_ref
  138.4 1.4 collective-permute-done.6.refs_1_
  139.8 9.6 %collective-permute-done.7.refs_2_ = bf16[4,256,128]{2,1,0:T(8,128)(2,1)S(1)} collective-permute-done((bf16[4,256,128]{2,1,0:T(8,128)(2,1)S(1)}, bf16[4,256,128]{2,1,0:T(8,128)(2,1)S(1)}, u32[]{:S(2)}, u32[]{:S(2)}) %collective-permute-start.7) | collective-permute-done | bytes 262176 | tf_op jit(solution)/shard_map/ppermute | solution.py:437
  149.4 0.0 collective-permute-done.8.refs_3_
  149.4 0.0 copy-done.4
  149.4 0.7 copy-done.5
  150.1 0.7 copy-done.6
  150.8 2.4 %projected.1 = bf16[256,128]{1,0:T(8,128)(2,1)} custom-call(bf16[4,256,128]{2,1,0:T(8,128)(2,1)} %copy-done.2, bf16[4,256,128]{2,1,0:T(8,128)(2,1)} %copy-done.4, bf16[4,256,128]{2,1,0:T(8,128)(2,1)} %copy-done.5, bf16[4,256,128]{2,1,0:T(8,128)(2,1)} %copy-done.6, bf16[2048,128]{1,0:T(8,128)(2,1)} %refs_4_.1), custom_call_target="tpu_custom_call" | custom-call | tf_op jit(solution)/shard_map/projected/pallas_call | solution.py:395
  153.3 0.0 all-to-all-done.3
  153.3 0.7 copy-done.3
  154.0 2.1 %combine.1 = bf16[128,128]{1,0:T(8,128)(2,1)} custom-call(bf16[1024,128]{1,0:T(8,128)(2,1)} %bitcast.16, s32[128,4]{1,0:T(8,128)} %get-tuple-element.11.target_ref, f32[4,128]{1,0:T(4,128)} %divide_bitcast_fusion.chances_ref), custom_call_target="tpu_custom_call" | custom-call | tf_op jit(solution)/shard_map/combine/pallas_call | solution.py:256
  (14 shorter events, 0.1 us)
Async XLA Ops:
  2.1 50.3 %copy-start = (bf16[6144,128]{1,0:T(8,128)(2,1)}, bf16[6144,128]{1,0:T(8,128)(2,1)S(1)}, u32[]{:S(2)}) copy-start(bf16[6144,128]{1,0:T(8,128)(2,1)S(1)} %pad_maximum_fusion.refs_0_) | copy-start | bytes 4718596
  2.1 24.9 %collective-permute-start.2 = (bf16[6144,128]{1,0:T(8,128)(2,1)S(1)}, bf16[6144,128]{1,0:T(8,128)(2,1)S(1)}, u32[]{:S(2)}, u32[]{:S(2)}) collective-permute-start(bf16[6144,128]{1,0:T(8,128)(2,1)S(1)} %pad_maximum_fusion.refs_0_), channel_id=1, source_target_pairs={{0,4},{1,16},{2,6},{3,18},{4,0},{5,20},{6,2},{7,22},{8,12},{9,24},... | collective-permute-start | bytes 4718600 | tf_op jit(solution)/shard_map/ppermute | solution.py:120
  6.6 43.4 %collective-permute-start.3 = (bf16[6144,128]{1,0:T(8,128)(2,1)S(1)}, bf16[6144,128]{1,0:T(8,128)(2,1)}, u32[]{:S(2)}, u32[]{:S(2)}) collective-permute-start(bf16[6144,128]{1,0:T(8,128)(2,1)S(1)} %pad_maximum_fusion.refs_0_), channel_id=1, source_target_pairs={{0,16},{1,4},{2,18},{3,6},{4,20},{5,0},{6,22},{7,2},{8,24},{9,12},... | collective-permute-start | bytes 4718600 | tf_op jit(solution)/shard_map/ppermute | solution.py:121
  11.7 39.7 %all-to-all-start = ((bf16[32,8,512]{2,1,0:T(8,128)(2,1)}), bf16[32,8,512]{2,1,0:T(8,128)(2,1)S(1)}, u32[]{:S(2)}, u32[]{:S(2)}) async-start(bf16[32,8,512]{2,1,0:T(8,128)(2,1)} %bitcast.22), calls=%async_computation | async-start | bytes 524288 | tf_op jit(solution)/shard_map/all_to_all | solution.py:25
  27.0 25.3 %copy-start.1 = (bf16[6144,128]{1,0:T(8,128)(2,1)}, bf16[6144,128]{1,0:T(8,128)(2,1)S(1)}, u32[]{:S(2)}) copy-start(bf16[6144,128]{1,0:T(8,128)(2,1)S(1)} %collective-permute-done.2.refs_1_) | copy-start | bytes 4718596
  27.0 46.7 %collective-permute-start.4 = (bf16[6144,128]{1,0:T(8,128)(2,1)S(1)}, bf16[6144,128]{1,0:T(8,128)(2,1)}, u32[]{:S(2)}, u32[]{:S(2)}) collective-permute-start(bf16[6144,128]{1,0:T(8,128)(2,1)S(1)} %collective-permute-done.2.refs_1_), channel_id=1, source_target_pairs={{0,16},{1,17},{2,18},{3,19},{4,20},{5,21},{6,22},{7,23},{8,24},{9,... | collective-permute-start | bytes 4718600 | tf_op jit(solution)/shard_map/ppermute | solution.py:122
  50.0 23.7 %collective-permute-start.5 = (bf16[6144,128]{1,0:T(8,128)(2,1)}, bf16[6144,128]{1,0:T(8,128)(2,1)}, u32[]{:S(2)}, u32[]{:S(2)}) collective-permute-start(bf16[6144,128]{1,0:T(8,128)(2,1)} %collective-permute-done.3.refs_2_), channel_id=1, source_target_pairs={{0,16},{2,18},{4,20},{6,22},{8,24},{10,26},{12,28},{14,30},{17,1},... | collective-permute-start | bytes 4718600 | tf_op jit(solution)/shard_map/ppermute | solution.py:123
  52.4 21.3 %all-to-all-start.1 = ((bf16[4,256,512]{2,1,0:T(8,128)(2,1)}), bf16[4,256,512]{2,1,0:T(8,128)(2,1)}, u32[]{:S(2)}, u32[]{:S(2)}) async-start(bf16[4,256,512]{2,1,0:T(8,128)(2,1)} %broadcast_in_dim.49), calls=%async_computation.1 | async-start | bytes 2097152 | tf_op jit(solution)/shard_map/all_to_all | solution.py:25
  61.6 5.5 %collective-permute-start = (bf16[128,128]{1,0:T(8,128)(2,1)}, bf16[128,128]{1,0:T(8,128)(2,1)S(1)}, u32[]{:S(2)}, u32[]{:S(2)}) collective-permute-start(bf16[128,128]{1,0:T(8,128)(2,1)} %get-tuple-element.9.refs_2_), channel_id=1, source_target_pairs={{0,16},{16,32},{32,48},{48,64},{64,80},{80,96},{96,112},{112,128},... | collective-permute-start | bytes 98312 | tf_op jit(solution)/shard_map/ppermute | solution.py:375
  64.1 5.8 %collective-permute-start.1 = (bf16[128,128]{1,0:T(8,128)(2,1)}, bf16[128,128]{1,0:T(8,128)(2,1)S(1)}, u32[]{:S(2)}, u32[]{:S(2)}) collective-permute-start(bf16[128,128]{1,0:T(8,128)(2,1)} %get-tuple-element.10.refs_1_), channel_id=1, source_target_pairs={{16,0},{32,16},{48,32},{64,48},{80,64},{96,80},{112,96},{128,112},... | collective-permute-start | bytes 98312 | tf_op jit(solution)/shard_map/ppermute | solution.py:376
  67.1 2.9 %copy-start.7 = (bf16[128,128]{1,0:T(8,128)(2,1)}, bf16[128,128]{1,0:T(8,128)(2,1)S(1)}, u32[]{:S(2)}) copy-start(bf16[128,128]{1,0:T(8,128)(2,1)S(1)} %collective-permute-done.refs_0_) | copy-start | bytes 98308
  69.9 0.6 copy-start.8
  106.6 21.8 %copy-start.9 = (f32[128,4]{0,1:T(4,128)S(1)}, f32[128,4]{0,1:T(4,128)}, u32[]{:S(2)}) copy-start(f32[128,4]{0,1:T(4,128)} %param.24) | copy-start | bytes 6148
  111.2 42.0 %all-to-all-start.3 = ((bf16[128,8,128]{2,1,0:T(8,128)(2,1)}), bf16[128,8,128]{2,1,0:T(8,128)(2,1)S(1)}, u32[]{:S(2)}, u32[]{:S(2)}) async-start(bf16[128,8,128]{2,1,0:T(8,128)(2,1)} %bitcast.14), calls=%async_computation.3 | async-start | bytes 524288 | tf_op jit(solution)/shard_map/all_to_all | solution.py:25
  129.4 20.0 %copy-start.2 = (bf16[4,256,128]{2,1,0:T(8,128)(2,1)}, bf16[4,256,128]{2,1,0:T(8,128)(2,1)S(1)}, u32[]{:S(2)}) copy-start(bf16[4,256,128]{2,1,0:T(8,128)(2,1)S(1)} %slice.4.refs_0_) | copy-start | bytes 786436
  129.5 10.4 %collective-permute-start.6 = (bf16[4,256,128]{2,1,0:T(8,128)(2,1)S(1)}, bf16[4,256,128]{2,1,0:T(8,128)(2,1)S(1)}, u32[]{:S(2)}, u32[]{:S(2)}) collective-permute-start(bf16[4,256,128]{2,1,0:T(8,128)(2,1)S(1)} %slice.4.refs_0_), channel_id=1, source_target_pairs={{0,1},{1,0},{4,5},{5,4},{2,3},{3,2},{6,7},{7,6},{8,9},{9,8},{12,13... | collective-permute-start | bytes 786440 | tf_op jit(solution)/shard_map/ppermute | solution.py:437
  132.7 16.7 %collective-permute-start.7 = (bf16[4,256,128]{2,1,0:T(8,128)(2,1)S(1)}, bf16[4,256,128]{2,1,0:T(8,128)(2,1)S(1)}, u32[]{:S(2)}, u32[]{:S(2)}) collective-permute-start(bf16[4,256,128]{2,1,0:T(8,128)(2,1)S(1)} %slice.4.refs_0_), channel_id=1, source_target_pairs={{0,4},{1,5},{4,0},{5,1},{2,6},{3,7},{6,2},{7,3},{8,12},{9,13},{12,... | collective-permute-start | bytes 786440 | tf_op jit(solution)/shard_map/ppermute | solution.py:437
  135.8 13.6 %collective-permute-start.8 = (bf16[4,256,128]{2,1,0:T(8,128)(2,1)S(1)}, bf16[4,256,128]{2,1,0:T(8,128)(2,1)S(1)}, u32[]{:S(2)}, u32[]{:S(2)}) collective-permute-start(bf16[4,256,128]{2,1,0:T(8,128)(2,1)S(1)} %slice.4.refs_0_), channel_id=1, source_target_pairs={{0,5},{1,4},{4,1},{5,0},{2,7},{3,6},{6,3},{7,2},{8,13},{9,12},{12,... | collective-permute-start | bytes 786440 | tf_op jit(solution)/shard_map/ppermute | solution.py:437
  139.8 9.6 %copy-start.4 = (bf16[4,256,128]{2,1,0:T(8,128)(2,1)}, bf16[4,256,128]{2,1,0:T(8,128)(2,1)S(1)}, u32[]{:S(2)}) copy-start(bf16[4,256,128]{2,1,0:T(8,128)(2,1)S(1)} %collective-permute-done.6.refs_1_) | copy-start | bytes 786436
  149.4 0.7 copy-start.5
  150.1 0.7 copy-start.6
  153.3 0.7 copy-start.3
where the time goes:
time: 157 us; the launch traced here: 156 us
  starting transfers between devices  82 us (52%)
  blocking collectives  26.5 us (17%)
  Pallas kernels  24.8 us (16%)
  waiting for transfers between devices  13.9 us (9%)
  local copies, waits for them, and re-layouts  4.74 us (3%)
  other arithmetic  3.36 us (2%)
    all_to_all x3, starting transfers between devices, swap(): return lax.all_to_all(pieces, axis, 0, 0, tiled=True)  36.9 us
    all_to_all x1, blocking collectives, swap(): return lax.all_to_all(pieces, axis, 0, 0, tiled=True)  26.5 us
    ppermute x1, starting transfers between devices, gather_shares(): third = lax.ppermute(first, axes, device_pairs(trade))  23 us
    ppermute x3, waiting for transfers between devices, shards(): lax.ppermute(heads, ('h', 'p'), [(i, i ^ k) for i in range(4)])  11 us
    ppermute x3, starting transfers between devices, shards(): lax.ppermute(heads, ('h', 'p'), [(i, i ^ k) for i in range(4)])  8.37 us
    pallas_call x1, Pallas kernels, gated(): pl.pallas_call(kernel, out_shape=jax.ShapeDtypeStruct((parts, n, 4 * u +...  6.4 us
    pallas_call x1, Pallas kernels, lowered(): pl.pallas_call(kernel, out_shape=jax.ShapeDtypeStruct((n // slots, 4, slo...  4.64 us
    ppermute x1, starting transfers between devices, gather_shares(): first = lax.ppermute(own, axes, device_pairs(outer))  4.5 us
  transfers between devices with their start and end apart: 12, of which 3 were waited for; matrix products, arithmetic and copies ran while one was open for 3% of the time, Pallas kernels for 7%

commit v1 on v0

--- a/solution.py
+++ b/solution.py
@@ -45,11 +45,21 @@
     return square.T
 
 
-def dispatch(rows, gain, routes, experts, slots, width):
+def dispatch(rows, gain, routes, weights, experts, slots, width):
     tokens = rows.shape[0]
     pairs = experts // 2
-
-    def kernel(rows_ref, gain_ref, routes_ref, out_ref, target_ref):
+    tall_rows, columns = weights[0].shape
+
+    def kernel(rows_ref, gain_ref, routes_ref, *refs):
+        weight_refs, (out_ref, target_ref, stacked_ref, sems) = refs[:3], refs[3:]
+        copies = [
+            pltpu.make_async_copy(
+                ref, stacked_ref.at[pl.ds(i * tall_rows, tall_rows)], sems.at[i]
+            )
+            for i, ref in enumerate(weight_refs)
+        ]
+        for copy in copies:
+            copy.start()
         block = 2 * lax.axis_index("Y") + lax.axis_index("X")
         values = rows_ref[...].astype(jnp.float32)
         scale = lax.rsqrt(jnp.mean(values * values, axis=-1, keepdims=True) + EPSILON)
@@ -82,18 +92,23 @@
         target_ref[...] = jnp.concatenate(
             [jnp.sum(mark * position, axis=1, keepdims=True) for mark in marks], axis=1
         ).astype(jnp.int32)
+        for copy in copies:
+            copy.wait()
 
     vmem = pl.BlockSpec(memory_space=pltpu.VMEM)
+    anywhere = pl.BlockSpec(memory_space=pl.ANY)
     return pl.pallas_call(
         kernel,
         out_shape=(
             jax.ShapeDtypeStruct((experts * slots, width), jnp.bfloat16),
             jax.ShapeDtypeStruct((tokens, TOP_K), jnp.int32),
+            jax.ShapeDtypeStruct((3 * tall_rows, columns), jnp.bfloat16),
         ),
-        in_specs=[vmem] * 3,
-        out_specs=(vmem, vmem),
+        in_specs=[vmem] * 3 + [anywhere] * 3,
+        out_specs=(vmem, vmem, anywhere),
+        scratch_shapes=[pltpu.SemaphoreType.DMA((3,))],
         name="dispatch",
-    )(rows, gain[None, :], routes.T)
+    )(rows, gain[None, :], routes.T, *weights)
 
 
 def device_pairs(where):
@@ -150,76 +165,118 @@
         pltpu.make_async_copy(there.at[rows], target, sem).start()
 
 
-def gated(rows, mixed, shares):
-    parts, n, k = rows.shape
+def gated(rows, shares, arrived):
+    parts, n, wide = rows.shape
     u = shares[0].shape[1]
-    j = mixed.shape[1]
+    k = 4 * u
+    j = wide - k
     whole = parts * k
 
-    def kernel(rows_ref, mixed_ref, *refs):
-        shares, (out_ref, weights_ref, sems) = refs[:5], refs[5:]
+    def kernel(rows_ref, _, *refs):
+        shares, refs = refs[:5], refs[5:]
+        out_ref, heads_ref, here_ref, weights_ref, hidden_ref, sems, row_sems, out_sems = refs
         native, order = share_order()
+        arrivals = [
+            pltpu.make_async_copy(
+                rows_ref.at[part, :, pl.ds(0, k)], here_ref.at[part], row_sems.at[part]
+            )
+            for part in range(parts)
+        ]
+        heads = pltpu.make_async_copy(
+            rows_ref.at[:, :, pl.ds(k, j)], heads_ref, row_sems.at[parts]
+        )
         targets = [
             (weights_ref.at[i, :, pl.ds(side * u, u)], sems.at[i, side])
             for i in range(4)
             for side in range(2)
         ]
-        for i in range(4):
+
+        def fetch(i):
             for side in range(2):
                 target, sem = targets[2 * i + side]
                 copy_share(native, shares, i, side * whole, whole, target, sem)
-        for copy in range(parts):
-            out_ref[copy, :, 4 * u :] = mixed_ref[...]
+
+        for part in range(parts):
+            arrivals[part].start()
+        for i in range(4):
+            fetch(i)
+        heads.start()
+        for part in range(parts):
+            arrivals[part].wait()
+        leaving = []
         for i in range(4):
             for side in range(2):
                 target, sem = targets[2 * i + side]
                 pltpu.make_async_copy(shares[1].at[pl.ds(0, whole)], target, sem).wait()
-            total = dot(rows_ref[0], weights_ref[i, :k, :])
+            total = dot(here_ref[0], weights_ref[i, :k, :])
             for part in range(1, parts):
-                total = total + dot(rows_ref[part], weights_ref[i, part * k : (part + 1) * k, :])
-            hidden = activate(total[:, :u], total[:, u:])
+                total = total + dot(here_ref[part], weights_ref[i, part * k : (part + 1) * k, :])
+            hidden_ref[i] = activate(total[:, :u], total[:, u:])
             lane = pl.multiple_of(order[i] * u, u)
             for copy in range(parts):
-                out_ref[copy, :, pl.ds(lane, u)] = hidden
-
-    vmem = pl.BlockSpec(memory_space=pltpu.VMEM)
+                out = out_ref.at[copy, :, pl.ds(lane, u)]
+                leaving.append(
+                    pltpu.make_async_copy(hidden_ref.at[i], out, out_sems.at[i, copy])
+                )
+                leaving[-1].start()
+        for copy in leaving:
+            copy.wait()
+        heads.wait()
+
     anywhere = pl.BlockSpec(memory_space=pl.ANY)
     return pl.pallas_call(
         kernel,
-        out_shape=jax.ShapeDtypeStruct((parts, n, 4 * u + j), jnp.bfloat16),
-        in_specs=[vmem, vmem] + [anywhere] * 5,
-        out_specs=vmem,
+        out_shape=(
+            jax.ShapeDtypeStruct((parts, n, 4 * u), jnp.bfloat16),
+            jax.ShapeDtypeStruct((parts, n, j), jnp.bfloat16),
+        ),
+        in_specs=[anywhere] * 7,
+        out_specs=(anywhere, anywhere),
         scratch_shapes=[
+            pltpu.VMEM((parts, n, k), jnp.bfloat16),
             pltpu.VMEM((4, whole, 2 * u), jnp.bfloat16),
+            pltpu.VMEM((4, n, u), jnp.bfloat16),
             pltpu.SemaphoreType.DMA((4, 2)),
+            pltpu.SemaphoreType.DMA((parts + 1,)),
+            pltpu.SemaphoreType.DMA((4, parts)),
         ],
         name="gated",
-    )(rows, mixed, *shares)
+    )(rows, arrived, *shares)
 
 
 def lowered(hidden, shares, slots):
-    parts, n, _ = hidden.shape
+    parts, n, k = hidden.shape
     f = shares[0].shape[1]
-    k = 4 * f
     whole = parts * k
     half = k // 2
 
     def kernel(hidden_ref, *refs):
-        shares, (out_ref, weights_ref, sems) = refs[:5], refs[5:]
+        shares, (out_ref, here_ref, weights_ref, sems, row_sems) = refs[:5], refs[5:]
         native, order = share_order()
         targets = [
             (weights_ref.at[i // 2, :, pl.ds((i % 2) * f, f)], sems.at[i]) for i in range(4)
         ]
-        for i in range(4):
+        arrivals = [
+            pltpu.make_async_copy(hidden_ref.at[part], here_ref.at[part], row_sems.at[part])
+            for part in range(parts)
+        ]
+        for i in range(2):
+            copy_share(native, shares, i, 2 * whole, whole, *targets[i])
+        for part in range(parts):
+            arrivals[part].start()
+        for i in range(2, 4):
             copy_share(native, shares, i, 2 * whole, whole, *targets[i])
         for pair in range(2):
             for i in (2 * pair, 2 * pair + 1):
                 pltpu.make_async_copy(shares[1].at[pl.ds(0, whole)], *targets[i]).wait()
             total = jnp.zeros((n, 2 * f), jnp.float32)
-            for Y, X, h in itertools.product(range(2), repeat=3):
-                unit = (8 * Y + 4 * h + 2 * X) * f
-                piece = hidden_ref[2 * Y + X, :, h * half : (h + 1) * half]
-                total = total + dot(piece, weights_ref[pair, unit : unit + half, :])
+            for Y, X in itertools.product(range(2), repeat=2):
+                if pair == 0:
+                    arrivals[2 * Y + X].wait()
+                for h in range(2):
+                    unit = (8 * Y + 4 * h + 2 * X) * f
+                    piece = here_ref[2 * Y + X, :, h * half : (h + 1) * half]
+                    total = total + dot(piece, weights_ref[pair, unit : unit + half, :])
             rounded = total.astype(jnp.bfloat16).reshape(n // slots, slots, 2 * f)
             out_ref[:, order[2 * pair]] = rounded[:, :, :f]
             out_ref[:, order[2 * pair + 1]] = rounded[:, :, f:]
@@ -229,11 +286,13 @@
     return pl.pallas_call(
         kernel,
         out_shape=jax.ShapeDtypeStruct((n // slots, 4, slots, f), jnp.bfloat16),
-        in_specs=[vmem] + [anywhere] * 5,
+        in_specs=[anywhere] * 6,
         out_specs=vmem,
         scratch_shapes=[
+            pltpu.VMEM((parts, n, k), jnp.bfloat16),
             pltpu.VMEM((2, whole, 2 * f), jnp.bfloat16),
             pltpu.SemaphoreType.DMA((4,)),
+            pltpu.SemaphoreType.DMA((parts,)),
         ],
         name="lowered",
     )(hidden, *shares)
@@ -246,10 +305,14 @@
     def kernel(results_ref, target_ref, chances_ref, out_ref):
         chances = tall(chances_ref[...])
         lane = lax.broadcasted_iota(jnp.int32, (tokens, slots), 1)
+        chosen = [
+            (target_ref[:, k : k + 1] == lane).astype(jnp.float32).astype(jnp.bfloat16)
+            for k in range(TOP_K)
+        ]
+        picked = dot(jnp.concatenate(chosen, axis=0), results_ref[...])
         total = jnp.zeros((tokens, f), jnp.float32)
         for k in range(TOP_K):
-            chosen = (target_ref[:, k : k + 1] == lane).astype(jnp.float32).astype(jnp.bfloat16)
-            total = total + dot(chosen, results_ref[...]) * chances[:, k : k + 1]
+            total = total + picked[k * tokens : (k + 1) * tokens] * chances[:, k : k + 1]
         out_ref[...] = total.astype(jnp.bfloat16)
 
     vmem = pl.BlockSpec(memory_space=pltpu.VMEM)
@@ -421,23 +484,26 @@
     rows_here, features = expert_input.shape
     slots = 2 * rows_here * TOP_K // experts // 4
     width = features // 4
-    own = jnp.concatenate([gate_weight[0], up_weight[0], down_weight[0]], axis=0)
+    weights = (gate_weight[0], up_weight[0], down_weight[0])
+    outgoing, target, own = dispatch(
+        expert_input, expert_gain, routes, weights, experts, slots, width
+    )
     shares = gather_shares(own)
-    outgoing, target = dispatch(expert_input, expert_gain, routes, experts, slots, width)
     received = swap(outgoing.reshape(experts, slots, width), EP)
     mixed = attention(mixer_input, mixer_gain, query_weight, key_weight, value_weight, sink_logit)
-    rows = spread(received.reshape(experts * slots, width), ("Y", "X"))
-    inner = gated(rows, mixed, shares)
-    beside = swap(inner, ("Y", "X"))
-    chances = jax.nn.softmax(route_logits.T, axis=0)
-    result = lowered(beside, shares, slots)
-    returned = swap(result.reshape(4 * experts, slots, -1), (*EP, "h", "p"))
-    heads = beside[:, :, width:]
+    beside = jnp.concatenate([received.reshape(experts * slots, width), mixed], axis=1)
+    rows = spread(beside, ("Y", "X"))
+    arrived = shares[3][:8] + shares[4][:8]
+    inner, heads = gated(rows, shares, arrived)
+    hidden = swap(inner, ("Y", "X"))
     heads = [heads] + [
         lax.ppermute(heads, ("h", "p"), [(i, i ^ k) for i in range(4)])
         for k in range(1, 4)
     ]
+    result = lowered(hidden, shares, slots)
+    returned = swap(result.reshape(4 * experts, slots, -1), (*EP, "h", "p"))
     mixer_output = projected(heads, output_weight)
+    chances = jax.nn.softmax(route_logits.T, axis=0)
     expert_output = combine(
         returned.reshape(experts * 4 * slots, -1), target, chances
     )

time: 157 us -> 219 us (1.39)
  Pallas kernels: 24.8 us -> 74.7 us
  waiting for transfers between devices: 13.9 us -> 31.3 us
  blocking collectives: 26.5 us -> 21.7 us
    pallas_call x1, Pallas kernels: 2.5 us -> 50.6 us  [dispatch(): pl.pallas_call(kernel, out_shape=(jax.ShapeDtypeStruct((experts * slots,...]
    all_to_all x3, waiting for transfers between devices: 0.01 us -> 16.5 us  [swap(): return lax.all_to_all(pieces, axis, 0, 0, tiled=True)]
    all_to_all x1, blocking collectives: 26.5 us -> 21.7 us  [swap(): return lax.all_to_all(pieces, axis, 0, 0, tiled=True)]
    pallas_call x1, Pallas kernels: 6.4 us -> 9.31 us  [gated(): pl.pallas_call(kernel, out_shape=(jax.ShapeDtypeStruct((parts, n, 4 * u),...]
  transfers between devices with their start and end apart: 12 -> 12, of which waited for: 3 -> 5; matrix products, arithmetic and copies ran while one was open for 3% -> 2% of each run, Pallas kernels for 7% -> 4%
where the time goes in v1:
time: 219 us
  starting transfers between devices  82.7 us (38%)
  Pallas kernels  74.7 us (34%)
  waiting for transfers between devices  31.3 us (14%)
  blocking collectives  21.7 us (10%)
  local copies, waits for them, and re-layouts  3.89 us (2%)
  other arithmetic  3.47 us (2%)
    pallas_call x1, Pallas kernels, dispatch(): pl.pallas_call(kernel, out_shape=(jax.ShapeDtypeStruct((experts * slots,...  50.6 us
    all_to_all x3, starting transfers between devices, swap(): return lax.all_to_all(pieces, axis, 0, 0, tiled=True)  36.6 us
    ppermute x1, starting transfers between devices, gather_shares(): third = lax.ppermute(first, axes, device_pairs(trade))  25 us
    all_to_all x1, blocking collectives, swap(): return lax.all_to_all(pieces, axis, 0, 0, tiled=True)  21.7 us
    all_to_all x3, waiting for transfers between devices, swap(): return lax.all_to_all(pieces, axis, 0, 0, tiled=True)  16.5 us
    ppermute x3, waiting for transfers between devices, shards(): lax.ppermute(heads, ('h', 'p'), [(i, i ^ k) for i in range(4)])  11.1 us
    pallas_call x1, Pallas kernels, gated(): pl.pallas_call(kernel, out_shape=(jax.ShapeDtypeStruct((parts, n, 4 * u),...  9.31 us
    ppermute x3, starting transfers between devices, shards(): lax.ppermute(heads, ('h', 'p'), [(i, i ^ k) for i in range(4)])  8.37 us
  transfers between devices with their start and end apart: 12, of which 5 were waited for; matrix products, arithmetic and copies ran while one was open for 2% of the time, Pallas kernels for 4%

profile of v1, /device:TPU:1, one launch (start us, length us, event | category | flops | bytes accessed | tf_op | source)
XLA Modules:
  0.0 218.5 jit_solution(4423693478002600982)
XLA Ops:
  0.6 50.6 %dispatch.1 = (bf16[256,512]{1,0:T(8,128)(2,1)}, s32[128,4]{1,0:T(8,128)}, bf16[6144,128]{1,0:T(8,128)(2,1)}) custom-call(bf16[128,2048]{1,0:T(8,128)(2,1)} %rows_ref.2, f32[1,2048]{1,0:T(1,128)} %bitcast.23, s32[4,128]{1,0:T(4,128)} %bitcast.25, bf16[2048,128]{1,0:T(8,128)(2,1)} %bitcast.17, bf16[2048,128]{1,0:T(8,128)(2,1)} %bitcast.18, ...), custom_call_target="tpu_custom_call" | custom-call | tf_op jit(solution)/shard_map/dispatch/pallas_call | solution.py:100
  51.2 4.5 %collective-permute-start.2 = (bf16[6144,128]{1,0:T(8,128)(2,1)}, bf16[6144,128]{1,0:T(8,128)(2,1)}, u32[]{:S(2)}, u32[]{:S(2)}) collective-permute-start(bf16[6144,128]{1,0:T(8,128)(2,1)} %get-tuple-element.14.refs_0_), channel_id=1, source_target_pairs={{0,4},{1,16},{2,6},{3,18},{4,0},{5,20},{6,2},{7,22},{8,12},{9,24},... | collective-permute-start | bytes 4718600 | tf_op jit(solution)/shard_map/ppermute | solution.py:135
  55.7 2.5 %collective-permute-start.4 = (bf16[6144,128]{1,0:T(8,128)(2,1)}, bf16[6144,128]{1,0:T(8,128)(2,1)}, u32[]{:S(2)}, u32[]{:S(2)}) collective-permute-start(bf16[6144,128]{1,0:T(8,128)(2,1)} %get-tuple-element.14.refs_0_), channel_id=1, source_target_pairs={{0,16},{1,4},{2,18},{3,6},{4,20},{5,0},{6,22},{7,2},{8,24},{9,12},... | collective-permute-start | bytes 4718600 | tf_op jit(solution)/shard_map/ppermute | solution.py:136
  58.2 15.4 %all-to-all-start = ((bf16[32,8,512]{2,1,0:T(8,128)(2,1)}), bf16[32,8,512]{2,1,0:T(8,128)(2,1)S(1)}, u32[]{:S(2)}, u32[]{:S(2)}) async-start(bf16[32,8,512]{2,1,0:T(8,128)(2,1)} %bitcast.22), calls=%async_computation | async-start | bytes 524288 | tf_op jit(solution)/shard_map/all_to_all | solution.py:25
  73.6 0.8 collective-permute-done.2.refs_1_
  74.4 25.0 %collective-permute-start.3 = (bf16[6144,128]{1,0:T(8,128)(2,1)}, bf16[6144,128]{1,0:T(8,128)(2,1)S(1)}, u32[]{:S(2)}, u32[]{:S(2)}) collective-permute-start(bf16[6144,128]{1,0:T(8,128)(2,1)} %collective-permute-done.2.refs_1_), channel_id=1, source_target_pairs={{0,16},{1,17},{2,18},{3,19},{4,20},{5,21},{6,22},{7,23},{8,24},{9,... | collective-permute-start | bytes 4718600 | tf_op jit(solution)/shard_map/ppermute | solution.py:137
  99.4 0.0 collective-permute-done.4.refs_2_
  99.4 1.3 collective-permute-start.5
  100.8 1.3 sine_multiply_fusion
  102.1 3.6 %projections.1 = (bf16[256,128]{1,0:T(8,128)(2,1)}, bf16[128,128]{1,0:T(8,128)(2,1)}, bf16[128,128]{1,0:T(8,128)(2,1)}) custom-call(bf16[256,2048]{1,0:T(8,128)(2,1)} %rows_ref.3, f32[1,2048]{1,0:T(1,128)} %bitcast.24, bf16[2048,128]{1,0:T(8,128)(2,1)} %query_ref.1, bf16[64,2048]{1,0:T(8,128)(2,1)} %bitcast.20, bf16[64,2048]{1,0:T(8,128)(2,1)} %bitcast.21, ...), custom_call_target="tpu_custom_call" | custom-call | tf_op jit(solution)/shard_map/projections/pallas_call | solution.py:379
  105.7 1.9 collective-permute-start
  107.6 2.5 %collective-permute-start.1 = (bf16[128,128]{1,0:T(8,128)(2,1)}, bf16[128,128]{1,0:T(8,128)(2,1)S(1)}, u32[]{:S(2)}, u32[]{:S(2)}) collective-permute-start(bf16[128,128]{1,0:T(8,128)(2,1)} %get-tuple-element.13.refs_1_), channel_id=1, source_target_pairs={{16,0},{32,16},{48,32},{64,48},{80,64},{96,80},{112,96},{128,112},... | collective-permute-start | bytes 98312 | tf_op jit(solution)/shard_map/ppermute | solution.py:439
  110.1 0.0 collective-permute-done.refs_0_
  110.1 0.0 copy-start.7
  110.1 2.9 %collective-permute-done.1.refs_3_ = bf16[128,128]{1,0:T(8,128)(2,1)S(1)} collective-permute-done((bf16[128,128]{1,0:T(8,128)(2,1)}, bf16[128,128]{1,0:T(8,128)(2,1)S(1)}, u32[]{:S(2)}, u32[]{:S(2)}) %collective-permute-start.1) | collective-permute-done | bytes 32800 | tf_op jit(solution)/shard_map/ppermute | solution.py:439
  113.0 0.0 copy-done.7
  113.0 0.6 copy-done.8
  113.6 3.1 %banded.1 = bf16[256,128]{1,0:T(8,128)(2,1)} custom-call(f32[2]{0:T(128)} %sink_ref.1, bf16[256,128]{1,0:T(8,128)(2,1)} %get-tuple-element.11.query_ref, bf16[128,128]{1,0:T(8,128)(2,1)} %copy-done.7, bf16[128,128]{1,0:T(8,128)(2,1)} %get-tuple-element.13.refs_1_, bf16[128,128]{1,0:T(8,128)(2,1)} %get-tuple-element.12.refs_2_, bf16[128,128]{1,0:T(8,128)(2,1)} %copy-done.8), custom_call_target="tpu_custom_call" | custom-call | tf_op jit(solution)/shard_map/banded/pallas_call | solution.py:422
  116.8 0.0 all-to-all-done
  116.8 0.9 pad_maximum_fusion
  117.6 1.2 broadcast_in_dim.53
  118.8 4.3 %all-to-all-start.1 = ((bf16[4,256,640]{2,1,0:T(8,128)(2,1)}), bf16[4,256,640]{2,1,0:T(8,128)(2,1)}, u32[]{:S(2)}, u32[]{:S(2)}) async-start(bf16[4,256,640]{2,1,0:T(8,128)(2,1)} %broadcast_in_dim.53), calls=%async_computation.1 | async-start | bytes 2621440 | tf_op jit(solution)/shard_map/all_to_all | solution.py:25
  123.1 0.0 collective-permute-done.3.refs_3_
  123.2 0.0 copy-start
  123.2 0.0 collective-permute-done.5.refs_4_
  123.2 0.0 copy-start.1
  123.2 0.6 slice_add_fusion._
  123.8 16.5 %all-to-all-done.1.rows_ref = bf16[4,256,640]{2,1,0:T(8,128)(2,1)} async-done(((bf16[4,256,640]{2,1,0:T(8,128)(2,1)}), bf16[4,256,640]{2,1,0:T(8,128)(2,1)}, u32[]{:S(2)}, u32[]{:S(2)}) %all-to-all-start.1) | async-done | bytes 1310752 | tf_op jit(solution)/shard_map/all_to_all | solution.py:25
  140.3 0.0 copy-done
  140.3 0.0 copy-done.1
  140.3 9.3 %gated.1 = (bf16[4,256,512]{2,1,0:T(8,128)(2,1)}, bf16[4,256,128]{2,1,0:T(8,128)(2,1)}) custom-call(bf16[4,256,640]{2,1,0:T(8,128)(2,1)} %all-to-all-done.1.rows_ref, bf16[8,128]{1,0:T(8,128)(2,1)} %slice_add_fusion._, bf16[6144,128]{1,0:T(8,128)(2,1)} %get-tuple-element.14.refs_0_, bf16[6144,128]{1,0:T(8,128)(2,1)} %collective-permute-done.2.refs_1_, ...), custom_call_target="tpu_custom_call" | custom-call | tf_op jit(solution)/shard_map/gated/pallas_call | solution.py:227
  149.7 21.7 %all_to_all.20.hidden_ref = bf16[4,256,512]{2,1,0:T(8,128)(2,1)} all-to-all(bf16[4,256,512]{2,1,0:T(8,128)(2,1)} %get-tuple-element.16), channel_id=1, replica_groups=mesh['ep_0'=16,'ep_1'=2,'Y'=2,'h'=2,'X'=2,'p'=2] {'Y','X'}, dimensions={0} | all-to-all | bytes 2097152 | tf_op jit(solution)/shard_map/all_to_all | solution.py:25
  171.3 3.6 %lowered.1 = bf16[32,4,8,128]{3,2,1,0:T(8,128)(2,1)} custom-call(bf16[4,256,512]{2,1,0:T(8,128)(2,1)} %all_to_all.20.hidden_ref, bf16[6144,128]{1,0:T(8,128)(2,1)} %get-tuple-element.14.refs_0_, bf16[6144,128]{1,0:T(8,128)(2,1)} %collective-permute-done.2.refs_1_, bf16[6144,128]{1,0:T(8,128)(2,1)} %collective-permute-done.4.refs_2_, ...), custom_call_target="tpu_custom_call" | custom-call | tf_op jit(solution)/shard_map/lowered/pallas_call | solution.py:286
  174.9 16.9 %all-to-all-start.3 = ((bf16[128,8,128]{2,1,0:T(8,128)(2,1)}), bf16[128,8,128]{2,1,0:T(8,128)(2,1)S(1)}, u32[]{:S(2)}, u32[]{:S(2)}) async-start(bf16[128,8,128]{2,1,0:T(8,128)(2,1)} %bitcast.14), calls=%async_computation.3 | async-start | bytes 524288 | tf_op jit(solution)/shard_map/all_to_all | solution.py:25
  191.7 0.0 copy-done.9
  191.8 3.3 %collective-permute-start.6 = (bf16[4,256,128]{2,1,0:T(8,128)(2,1)S(1)}, bf16[4,256,128]{2,1,0:T(8,128)(2,1)S(1)}, u32[]{:S(2)}, u32[]{:S(2)}) collective-permute-start(bf16[4,256,128]{2,1,0:T(8,128)(2,1)S(1)} %copy-done.3), channel_id=1, source_target_pairs={{0,1},{1,0},{4,5},{5,4},{2,3},{3,2},{6,7},{7,6},{8,9},{9,8},{12,13... | collective-permute-start | bytes 786440 | tf_op jit(solution)/shard_map/ppermute | solution.py:500
  195.1 3.1 %collective-permute-start.7 = (bf16[4,256,128]{2,1,0:T(8,128)(2,1)S(1)}, bf16[4,256,128]{2,1,0:T(8,128)(2,1)S(1)}, u32[]{:S(2)}, u32[]{:S(2)}) collective-permute-start(bf16[4,256,128]{2,1,0:T(8,128)(2,1)S(1)} %copy-done.3), channel_id=1, source_target_pairs={{0,4},{1,5},{4,0},{5,1},{2,6},{3,7},{6,2},{7,3},{8,12},{9,13},{12,... | collective-permute-start | bytes 786440 | tf_op jit(solution)/shard_map/ppermute | solution.py:500
  198.2 2.0 collective-permute-start.8
  200.2 0.6 divide_bitcast_fusion.chances_ref
  200.8 1.2 collective-permute-done.6.refs_1_
  202.0 9.9 %collective-permute-done.7.refs_2_ = bf16[4,256,128]{2,1,0:T(8,128)(2,1)S(1)} collective-permute-done((bf16[4,256,128]{2,1,0:T(8,128)(2,1)S(1)}, bf16[4,256,128]{2,1,0:T(8,128)(2,1)S(1)}, u32[]{:S(2)}, u32[]{:S(2)}) %collective-permute-start.7) | collective-permute-done | bytes 262176 | tf_op jit(solution)/shard_map/ppermute | solution.py:500
  211.9 0.0 collective-permute-done.8.refs_3_
  211.9 0.7 copy-done.5
  212.6 0.7 copy-done.6
  213.3 2.4 %projected.1 = bf16[256,128]{1,0:T(8,128)(2,1)} custom-call(bf16[4,256,128]{2,1,0:T(8,128)(2,1)} %get-tuple-element.15.refs_0_, bf16[4,256,128]{2,1,0:T(8,128)(2,1)} %copy-done.4, bf16[4,256,128]{2,1,0:T(8,128)(2,1)} %copy-done.5, bf16[4,256,128]{2,1,0:T(8,128)(2,1)} %copy-done.6, bf16[2048,128]{1,0:T(8,128)(2,1)} %refs_4_.1), custom_call_target="tpu_custom_call" | custom-call | tf_op jit(solution)/shard_map/projected/pallas_call | solution.py:458
  215.7 0.0 all-to-all-done.3
  215.7 0.7 copy-done.2
  216.4 2.1 combine.1
  (14 shorter events, 0.1 us)
Async XLA Ops:
  51.2 23.2 %collective-permute-start.2 = (bf16[6144,128]{1,0:T(8,128)(2,1)}, bf16[6144,128]{1,0:T(8,128)(2,1)}, u32[]{:S(2)}, u32[]{:S(2)}) collective-permute-start(bf16[6144,128]{1,0:T(8,128)(2,1)} %get-tuple-element.14.refs_0_), channel_id=1, source_target_pairs={{0,4},{1,16},{2,6},{3,18},{4,0},{5,20},{6,2},{7,22},{8,12},{9,24},... | collective-permute-start | bytes 4718600 | tf_op jit(solution)/shard_map/ppermute | solution.py:135
  55.7 43.7 %collective-permute-start.4 = (bf16[6144,128]{1,0:T(8,128)(2,1)}, bf16[6144,128]{1,0:T(8,128)(2,1)}, u32[]{:S(2)}, u32[]{:S(2)}) collective-permute-start(bf16[6144,128]{1,0:T(8,128)(2,1)} %get-tuple-element.14.refs_0_), channel_id=1, source_target_pairs={{0,16},{1,4},{2,18},{3,6},{4,20},{5,0},{6,22},{7,2},{8,24},{9,12},... | collective-permute-start | bytes 4718600 | tf_op jit(solution)/shard_map/ppermute | solution.py:136
  58.2 58.5 %all-to-all-start = ((bf16[32,8,512]{2,1,0:T(8,128)(2,1)}), bf16[32,8,512]{2,1,0:T(8,128)(2,1)S(1)}, u32[]{:S(2)}, u32[]{:S(2)}) async-start(bf16[32,8,512]{2,1,0:T(8,128)(2,1)} %bitcast.22), calls=%async_computation | async-start | bytes 524288 | tf_op jit(solution)/shard_map/all_to_all | solution.py:25
  74.4 48.8 %collective-permute-start.3 = (bf16[6144,128]{1,0:T(8,128)(2,1)}, bf16[6144,128]{1,0:T(8,128)(2,1)S(1)}, u32[]{:S(2)}, u32[]{:S(2)}) collective-permute-start(bf16[6144,128]{1,0:T(8,128)(2,1)} %collective-permute-done.2.refs_1_), channel_id=1, source_target_pairs={{0,16},{1,17},{2,18},{3,19},{4,20},{5,21},{6,22},{7,23},{8,24},{9,... | collective-permute-start | bytes 4718600 | tf_op jit(solution)/shard_map/ppermute | solution.py:137
  99.4 23.7 %collective-permute-start.5 = (bf16[6144,128]{1,0:T(8,128)(2,1)}, bf16[6144,128]{1,0:T(8,128)(2,1)S(1)}, u32[]{:S(2)}, u32[]{:S(2)}) collective-permute-start(bf16[6144,128]{1,0:T(8,128)(2,1)} %collective-permute-done.4.refs_2_), channel_id=1, source_target_pairs={{0,16},{2,18},{4,20},{6,22},{8,24},{10,26},{12,28},{14,30},{17,1},... | collective-permute-start | bytes 4718600 | tf_op jit(solution)/shard_map/ppermute | solution.py:138
  105.7 4.4 %collective-permute-start = (bf16[128,128]{1,0:T(8,128)(2,1)}, bf16[128,128]{1,0:T(8,128)(2,1)S(1)}, u32[]{:S(2)}, u32[]{:S(2)}) collective-permute-start(bf16[128,128]{1,0:T(8,128)(2,1)} %get-tuple-element.12.refs_2_), channel_id=1, source_target_pairs={{0,16},{16,32},{32,48},{48,64},{64,80},{80,96},{96,112},{112,128},... | collective-permute-start | bytes 98312 | tf_op jit(solution)/shard_map/ppermute | solution.py:438
  107.6 5.4 %collective-permute-start.1 = (bf16[128,128]{1,0:T(8,128)(2,1)}, bf16[128,128]{1,0:T(8,128)(2,1)S(1)}, u32[]{:S(2)}, u32[]{:S(2)}) collective-permute-start(bf16[128,128]{1,0:T(8,128)(2,1)} %get-tuple-element.13.refs_1_), channel_id=1, source_target_pairs={{16,0},{32,16},{48,32},{64,48},{80,64},{96,80},{112,96},{128,112},... | collective-permute-start | bytes 98312 | tf_op jit(solution)/shard_map/ppermute | solution.py:439
  110.1 2.9 %copy-start.7 = (bf16[128,128]{1,0:T(8,128)(2,1)}, bf16[128,128]{1,0:T(8,128)(2,1)S(1)}, u32[]{:S(2)}) copy-start(bf16[128,128]{1,0:T(8,128)(2,1)S(1)} %collective-permute-done.refs_0_) | copy-start | bytes 98308
  113.0 0.6 copy-start.8
  118.8 21.5 %all-to-all-start.1 = ((bf16[4,256,640]{2,1,0:T(8,128)(2,1)}), bf16[4,256,640]{2,1,0:T(8,128)(2,1)}, u32[]{:S(2)}, u32[]{:S(2)}) async-start(bf16[4,256,640]{2,1,0:T(8,128)(2,1)} %broadcast_in_dim.53), calls=%async_computation.1 | async-start | bytes 2621440 | tf_op jit(solution)/shard_map/all_to_all | solution.py:25
  123.2 17.2 %copy-start = (bf16[6144,128]{1,0:T(8,128)(2,1)}, bf16[6144,128]{1,0:T(8,128)(2,1)S(1)}, u32[]{:S(2)}) copy-start(bf16[6144,128]{1,0:T(8,128)(2,1)S(1)} %collective-permute-done.3.refs_3_) | copy-start | bytes 4718596
  123.2 17.2 %copy-start.1 = (bf16[6144,128]{1,0:T(8,128)(2,1)}, bf16[6144,128]{1,0:T(8,128)(2,1)S(1)}, u32[]{:S(2)}) copy-start(bf16[6144,128]{1,0:T(8,128)(2,1)S(1)} %collective-permute-done.5.refs_4_) | copy-start | bytes 4718596
  171.3 20.4 %copy-start.9 = (f32[128,4]{0,1:T(4,128)S(1)}, f32[128,4]{0,1:T(4,128)}, u32[]{:S(2)}) copy-start(f32[128,4]{0,1:T(4,128)} %param.24) | copy-start | bytes 6148
  171.3 20.5 %copy-start.3 = (bf16[4,256,128]{2,1,0:T(8,128)(2,1)S(1)}, bf16[4,256,128]{2,1,0:T(8,128)(2,1)}, u32[]{:S(2)}) copy-start(bf16[4,256,128]{2,1,0:T(8,128)(2,1)} %get-tuple-element.15.refs_0_) | copy-start | bytes 786436
  174.9 40.8 %all-to-all-start.3 = ((bf16[128,8,128]{2,1,0:T(8,128)(2,1)}), bf16[128,8,128]{2,1,0:T(8,128)(2,1)S(1)}, u32[]{:S(2)}, u32[]{:S(2)}) async-start(bf16[128,8,128]{2,1,0:T(8,128)(2,1)} %bitcast.14), calls=%async_computation.3 | async-start | bytes 524288 | tf_op jit(solution)/shard_map/all_to_all | solution.py:25
  191.8 10.2 %collective-permute-start.6 = (bf16[4,256,128]{2,1,0:T(8,128)(2,1)S(1)}, bf16[4,256,128]{2,1,0:T(8,128)(2,1)S(1)}, u32[]{:S(2)}, u32[]{:S(2)}) collective-permute-start(bf16[4,256,128]{2,1,0:T(8,128)(2,1)S(1)} %copy-done.3), channel_id=1, source_target_pairs={{0,1},{1,0},{4,5},{5,4},{2,3},{3,2},{6,7},{7,6},{8,9},{9,8},{12,13... | collective-permute-start | bytes 786440 | tf_op jit(solution)/shard_map/ppermute | solution.py:500
  195.1 16.8 %collective-permute-start.7 = (bf16[4,256,128]{2,1,0:T(8,128)(2,1)S(1)}, bf16[4,256,128]{2,1,0:T(8,128)(2,1)S(1)}, u32[]{:S(2)}, u32[]{:S(2)}) collective-permute-start(bf16[4,256,128]{2,1,0:T(8,128)(2,1)S(1)} %copy-done.3), channel_id=1, source_target_pairs={{0,4},{1,5},{4,0},{5,1},{2,6},{3,7},{6,2},{7,3},{8,12},{9,13},{12,... | collective-permute-start | bytes 786440 | tf_op jit(solution)/shard_map/ppermute | solution.py:500
  198.2 13.7 %collective-permute-start.8 = (bf16[4,256,128]{2,1,0:T(8,128)(2,1)S(1)}, bf16[4,256,128]{2,1,0:T(8,128)(2,1)S(1)}, u32[]{:S(2)}, u32[]{:S(2)}) collective-permute-start(bf16[4,256,128]{2,1,0:T(8,128)(2,1)S(1)} %copy-done.3), channel_id=1, source_target_pairs={{0,5},{1,4},{4,1},{5,0},{2,7},{3,6},{6,3},{7,2},{8,13},{9,12},{12,... | collective-permute-start | bytes 786440 | tf_op jit(solution)/shard_map/ppermute | solution.py:500
  202.0 9.9 %copy-start.4 = (bf16[4,256,128]{2,1,0:T(8,128)(2,1)}, bf16[4,256,128]{2,1,0:T(8,128)(2,1)S(1)}, u32[]{:S(2)}) copy-start(bf16[4,256,128]{2,1,0:T(8,128)(2,1)S(1)} %collective-permute-done.6.refs_1_) | copy-start | bytes 786436
  211.9 0.7 copy-start.5
  212.6 0.7 copy-start.6
  215.7 0.7 copy-start.2

commit v2 on v1

--- a/solution.py
+++ b/solution.py
@@ -51,18 +51,25 @@
     tall_rows, columns = weights[0].shape
 
     def kernel(rows_ref, gain_ref, routes_ref, *refs):
-        weight_refs, (out_ref, target_ref, stacked_ref, sems) = refs[:3], refs[3:]
-        copies = [
+        weight_refs, (out_ref, target_ref, stacked_ref, held_ref, sems) = refs[:3], refs[3:]
+        arriving = [
+            pltpu.make_async_copy(ref, held_ref.at[i], sems.at[i])
+            for i, ref in enumerate(weight_refs)
+        ]
+        leaving = [
             pltpu.make_async_copy(
-                ref, stacked_ref.at[pl.ds(i * tall_rows, tall_rows)], sems.at[i]
+                held_ref.at[i], stacked_ref.at[pl.ds(i * tall_rows, tall_rows)], sems.at[3 + i]
             )
-            for i, ref in enumerate(weight_refs)
-        ]
-        for copy in copies:
+            for i in range(3)
+        ]
+        for copy in arriving:
             copy.start()
         block = 2 * lax.axis_index("Y") + lax.axis_index("X")
         values = rows_ref[...].astype(jnp.float32)
         scale = lax.rsqrt(jnp.mean(values * values, axis=-1, keepdims=True) + EPSILON)
+        for come, go in zip(arriving, leaving):
+            come.wait()
+            go.start()
         start = pl.multiple_of(block * width, width)
         own = rows_ref[:, pl.ds(start, width)].astype(jnp.float32)
         normed = (own * scale * gain_ref[:, pl.ds(start, width)]).astype(jnp.bfloat16)
@@ -92,7 +99,7 @@
         target_ref[...] = jnp.concatenate(
             [jnp.sum(mark * position, axis=1, keepdims=True) for mark in marks], axis=1
         ).astype(jnp.int32)
-        for copy in copies:
+        for copy in leaving:
             copy.wait()
 
     vmem = pl.BlockSpec(memory_space=pltpu.VMEM)
@@ -106,7 +113,10 @@
         ),
         in_specs=[vmem] * 3 + [anywhere] * 3,
         out_specs=(vmem, vmem, anywhere),
-        scratch_shapes=[pltpu.SemaphoreType.DMA((3,))],
+        scratch_shapes=[
+            pltpu.VMEM((3, tall_rows, columns), jnp.bfloat16),
+            pltpu.SemaphoreType.DMA((6,)),
+        ],
         name="dispatch",
     )(rows, gain[None, :], routes.T, *weights)
 
@@ -177,13 +187,11 @@
         out_ref, heads_ref, here_ref, weights_ref, hidden_ref, sems, row_sems, out_sems = refs
         native, order = share_order()
         arrivals = [
-            pltpu.make_async_copy(
-                rows_ref.at[part, :, pl.ds(0, k)], here_ref.at[part], row_sems.at[part]
-            )
+            pltpu.make_async_copy(rows_ref.at[part], here_ref.at[part], row_sems.at[part])
             for part in range(parts)
         ]
         heads = pltpu.make_async_copy(
-            rows_ref.at[:, :, pl.ds(k, j)], heads_ref, row_sems.at[parts]
+            here_ref.at[:, :, pl.ds(k, j)], heads_ref, row_sems.at[parts]
         )
         targets = [
             (weights_ref.at[i, :, pl.ds(side * u, u)], sems.at[i, side])
@@ -200,17 +208,18 @@
             arrivals[part].start()
         for i in range(4):
             fetch(i)
-        heads.start()
         for part in range(parts):
             arrivals[part].wait()
+        heads.start()
         leaving = []
         for i in range(4):
             for side in range(2):
                 target, sem = targets[2 * i + side]
                 pltpu.make_async_copy(shares[1].at[pl.ds(0, whole)], target, sem).wait()
-            total = dot(here_ref[0], weights_ref[i, :k, :])
+            total = dot(here_ref[0, :, :k], weights_ref[i, :k, :])
             for part in range(1, parts):
-                total = total + dot(here_ref[part], weights_ref[i, part * k : (part + 1) * k, :])
+                piece = here_ref[part, :, :k]
+                total = total + dot(piece, weights_ref[i, part * k : (part + 1) * k, :])
             hidden_ref[i] = activate(total[:, :u], total[:, u:])
             lane = pl.multiple_of(order[i] * u, u)
             for copy in range(parts):
@@ -233,7 +242,7 @@
         in_specs=[anywhere] * 7,
         out_specs=(anywhere, anywhere),
         scratch_shapes=[
-            pltpu.VMEM((parts, n, k), jnp.bfloat16),
+            pltpu.VMEM((parts, n, wide), jnp.bfloat16),
             pltpu.VMEM((4, whole, 2 * u), jnp.bfloat16),
             pltpu.VMEM((4, n, u), jnp.bfloat16),
             pltpu.SemaphoreType.DMA((4, 2)),

time: 219 us -> 170 us (0.78)
  Pallas kernels: 74.7 us -> 25.1 us
    pallas_call x1, Pallas kernels: 50.6 us -> 4.04 us  [dispatch(): pl.pallas_call(kernel, out_shape=(jax.ShapeDtypeStruct((experts * slots,...]
    pallas_call x1, Pallas kernels: 9.31 us -> 6.2 us  [gated(): pl.pallas_call(kernel, out_shape=(jax.ShapeDtypeStruct((parts, n, 4 * u),...]
  transfers between devices with their start and end apart: 12 -> 12, of which waited for: 5 -> 5; matrix products, arithmetic and copies ran while one was open for 2% -> 3% of each run, Pallas kernels for 4% -> 5%
where the time goes in v2:
time: 170 us; the launch traced here: 169 us
  starting transfers between devices  82.6 us (49%)
  waiting for transfers between devices  31.3 us (18%)
  Pallas kernels  25.1 us (15%)
  blocking collectives  21.7 us (13%)
  local copies, waits for them, and re-layouts  3.89 us (2%)
  other arithmetic  3.47 us (2%)
    all_to_all x3, starting transfers between devices, swap(): return lax.all_to_all(pieces, axis, 0, 0, tiled=True)  36.5 us
    ppermute x1, starting transfers between devices, gather_shares(): third = lax.ppermute(first, axes, device_pairs(trade))  25 us
    all_to_all x1, blocking collectives, swap(): return lax.all_to_all(pieces, axis, 0, 0, tiled=True)  21.7 us
    all_to_all x3, waiting for transfers between devices, swap(): return lax.all_to_all(pieces, axis, 0, 0, tiled=True)  16.5 us
    ppermute x3, waiting for transfers between devices, shards(): lax.ppermute(heads, ('h', 'p'), [(i, i ^ k) for i in range(4)])  11.1 us
    ppermute x3, starting transfers between devices, shards(): lax.ppermute(heads, ('h', 'p'), [(i, i ^ k) for i in range(4)])  8.37 us
    pallas_call x1, Pallas kernels, gated(): pl.pallas_call(kernel, out_shape=(jax.ShapeDtypeStruct((parts, n, 4 * u),...  6.2 us
    ppermute x1, starting transfers between devices, gather_shares(): first = lax.ppermute(own, axes, device_pairs(outer))  4.5 us
  transfers between devices with their start and end apart: 12, of which 5 were waited for; matrix products, arithmetic and copies ran while one was open for 3% of the time, Pallas kernels for 5%

profile of v2, /device:TPU:1, one launch (start us, length us, event | category | flops | bytes accessed | tf_op | source)
XLA Modules:
  0.0 168.9 jit_solution(15015815433171363616)
XLA Ops:
  0.6 4.0 %dispatch.1 = (bf16[256,512]{1,0:T(8,128)(2,1)}, s32[128,4]{1,0:T(8,128)}, bf16[6144,128]{1,0:T(8,128)(2,1)}) custom-call(bf16[128,2048]{1,0:T(8,128)(2,1)} %rows_ref.2, f32[1,2048]{1,0:T(1,128)} %bitcast.23, s32[4,128]{1,0:T(4,128)} %bitcast.25, bf16[2048,128]{1,0:T(8,128)(2,1)} %bitcast.17, bf16[2048,128]{1,0:T(8,128)(2,1)} %bitcast.18, ...), custom_call_target="tpu_custom_call" | custom-call | tf_op jit(solution)/shard_map/dispatch/pallas_call | solution.py:107
  4.7 4.5 %collective-permute-start.2 = (bf16[6144,128]{1,0:T(8,128)(2,1)}, bf16[6144,128]{1,0:T(8,128)(2,1)}, u32[]{:S(2)}, u32[]{:S(2)}) collective-permute-start(bf16[6144,128]{1,0:T(8,128)(2,1)} %get-tuple-element.14.refs_0_), channel_id=1, source_target_pairs={{0,4},{1,16},{2,6},{3,18},{4,0},{5,20},{6,2},{7,22},{8,12},{9,24},... | collective-permute-start | bytes 4718600 | tf_op jit(solution)/shard_map/ppermute | solution.py:145
  9.2 2.5 %collective-permute-start.4 = (bf16[6144,128]{1,0:T(8,128)(2,1)}, bf16[6144,128]{1,0:T(8,128)(2,1)}, u32[]{:S(2)}, u32[]{:S(2)}) collective-permute-start(bf16[6144,128]{1,0:T(8,128)(2,1)} %get-tuple-element.14.refs_0_), channel_id=1, source_target_pairs={{0,16},{1,4},{2,18},{3,6},{4,20},{5,0},{6,22},{7,2},{8,24},{9,12},... | collective-permute-start | bytes 4718600 | tf_op jit(solution)/shard_map/ppermute | solution.py:146
  11.7 15.4 %all-to-all-start = ((bf16[32,8,512]{2,1,0:T(8,128)(2,1)}), bf16[32,8,512]{2,1,0:T(8,128)(2,1)S(1)}, u32[]{:S(2)}, u32[]{:S(2)}) async-start(bf16[32,8,512]{2,1,0:T(8,128)(2,1)} %bitcast.22), calls=%async_computation | async-start | bytes 524288 | tf_op jit(solution)/shard_map/all_to_all | solution.py:25
  27.1 0.8 collective-permute-done.2.refs_1_
  27.9 25.0 %collective-permute-start.3 = (bf16[6144,128]{1,0:T(8,128)(2,1)}, bf16[6144,128]{1,0:T(8,128)(2,1)S(1)}, u32[]{:S(2)}, u32[]{:S(2)}) collective-permute-start(bf16[6144,128]{1,0:T(8,128)(2,1)} %collective-permute-done.2.refs_1_), channel_id=1, source_target_pairs={{0,16},{1,17},{2,18},{3,19},{4,20},{5,21},{6,22},{7,23},{8,24},{9,... | collective-permute-start | bytes 4718600 | tf_op jit(solution)/shard_map/ppermute | solution.py:147
  52.9 0.0 collective-permute-done.4.refs_2_
  52.9 1.3 collective-permute-start.5
  54.3 1.3 sine_multiply_fusion
  55.6 3.6 %projections.1 = (bf16[256,128]{1,0:T(8,128)(2,1)}, bf16[128,128]{1,0:T(8,128)(2,1)}, bf16[128,128]{1,0:T(8,128)(2,1)}) custom-call(bf16[256,2048]{1,0:T(8,128)(2,1)} %rows_ref.3, f32[1,2048]{1,0:T(1,128)} %bitcast.24, bf16[2048,128]{1,0:T(8,128)(2,1)} %query_ref.1, bf16[64,2048]{1,0:T(8,128)(2,1)} %bitcast.20, bf16[64,2048]{1,0:T(8,128)(2,1)} %bitcast.21, ...), custom_call_target="tpu_custom_call" | custom-call | tf_op jit(solution)/shard_map/projections/pallas_call | solution.py:388
  59.1 1.9 %collective-permute-start = (bf16[128,128]{1,0:T(8,128)(2,1)}, bf16[128,128]{1,0:T(8,128)(2,1)S(1)}, u32[]{:S(2)}, u32[]{:S(2)}) collective-permute-start(bf16[128,128]{1,0:T(8,128)(2,1)} %get-tuple-element.12.refs_2_), channel_id=1, source_target_pairs={{0,16},{16,32},{32,48},{48,64},{64,80},{80,96},{96,112},{112,128},... | collective-permute-start | bytes 98312 | tf_op jit(solution)/shard_map/ppermute | solution.py:447
  61.1 2.5 %collective-permute-start.1 = (bf16[128,128]{1,0:T(8,128)(2,1)}, bf16[128,128]{1,0:T(8,128)(2,1)S(1)}, u32[]{:S(2)}, u32[]{:S(2)}) collective-permute-start(bf16[128,128]{1,0:T(8,128)(2,1)} %get-tuple-element.13.refs_1_), channel_id=1, source_target_pairs={{16,0},{32,16},{48,32},{64,48},{80,64},{96,80},{112,96},{128,112},... | collective-permute-start | bytes 98312 | tf_op jit(solution)/shard_map/ppermute | solution.py:448
  63.6 0.0 collective-permute-done.refs_0_
  63.6 0.0 copy-start.7
  63.6 2.9 %collective-permute-done.1.refs_3_ = bf16[128,128]{1,0:T(8,128)(2,1)S(1)} collective-permute-done((bf16[128,128]{1,0:T(8,128)(2,1)}, bf16[128,128]{1,0:T(8,128)(2,1)S(1)}, u32[]{:S(2)}, u32[]{:S(2)}) %collective-permute-start.1) | collective-permute-done | bytes 32800 | tf_op jit(solution)/shard_map/ppermute | solution.py:448
  66.5 0.0 copy-done.7
  66.5 0.6 copy-done.8
  67.1 3.1 %banded.1 = bf16[256,128]{1,0:T(8,128)(2,1)} custom-call(f32[2]{0:T(128)} %sink_ref.1, bf16[256,128]{1,0:T(8,128)(2,1)} %get-tuple-element.11.query_ref, bf16[128,128]{1,0:T(8,128)(2,1)} %copy-done.7, bf16[128,128]{1,0:T(8,128)(2,1)} %get-tuple-element.13.refs_1_, bf16[128,128]{1,0:T(8,128)(2,1)} %get-tuple-element.12.refs_2_, bf16[128,128]{1,0:T(8,128)(2,1)} %copy-done.8), custom_call_target="tpu_custom_call" | custom-call | tf_op jit(solution)/shard_map/banded/pallas_call | solution.py:431
  70.3 0.0 all-to-all-done
  70.3 0.9 pad_maximum_fusion
  71.1 1.2 broadcast_in_dim.53
  72.3 4.3 %all-to-all-start.1 = ((bf16[4,256,640]{2,1,0:T(8,128)(2,1)}), bf16[4,256,640]{2,1,0:T(8,128)(2,1)}, u32[]{:S(2)}, u32[]{:S(2)}) async-start(bf16[4,256,640]{2,1,0:T(8,128)(2,1)} %broadcast_in_dim.53), calls=%async_computation.1 | async-start | bytes 2621440 | tf_op jit(solution)/shard_map/all_to_all | solution.py:25
  76.6 0.0 collective-permute-done.3.refs_3_
  76.6 0.0 copy-start
  76.7 0.0 collective-permute-done.5.refs_4_
  76.7 0.0 copy-start.1
  76.7 0.6 slice_add_fusion._
  77.3 16.5 %all-to-all-done.1.rows_ref = bf16[4,256,640]{2,1,0:T(8,128)(2,1)} async-done(((bf16[4,256,640]{2,1,0:T(8,128)(2,1)}), bf16[4,256,640]{2,1,0:T(8,128)(2,1)}, u32[]{:S(2)}, u32[]{:S(2)}) %all-to-all-start.1) | async-done | bytes 1310752 | tf_op jit(solution)/shard_map/all_to_all | solution.py:25
  93.8 0.0 copy-done
  93.8 0.0 copy-done.1
  93.8 6.2 %gated.1 = (bf16[4,256,512]{2,1,0:T(8,128)(2,1)}, bf16[4,256,128]{2,1,0:T(8,128)(2,1)}) custom-call(bf16[4,256,640]{2,1,0:T(8,128)(2,1)} %all-to-all-done.1.rows_ref, bf16[8,128]{1,0:T(8,128)(2,1)} %slice_add_fusion._, bf16[6144,128]{1,0:T(8,128)(2,1)} %get-tuple-element.14.refs_0_, bf16[6144,128]{1,0:T(8,128)(2,1)} %collective-permute-done.2.refs_1_, ...), custom_call_target="tpu_custom_call" | custom-call | tf_op jit(solution)/shard_map/gated/pallas_call | solution.py:236
  100.0 21.7 %all_to_all.20.hidden_ref = bf16[4,256,512]{2,1,0:T(8,128)(2,1)} all-to-all(bf16[4,256,512]{2,1,0:T(8,128)(2,1)} %get-tuple-element.16), channel_id=1, replica_groups=mesh['ep_0'=16,'ep_1'=2,'Y'=2,'h'=2,'X'=2,'p'=2] {'Y','X'}, dimensions={0} | all-to-all | bytes 2097152 | tf_op jit(solution)/shard_map/all_to_all | solution.py:25
  121.7 3.6 %lowered.1 = bf16[32,4,8,128]{3,2,1,0:T(8,128)(2,1)} custom-call(bf16[4,256,512]{2,1,0:T(8,128)(2,1)} %all_to_all.20.hidden_ref, bf16[6144,128]{1,0:T(8,128)(2,1)} %get-tuple-element.14.refs_0_, bf16[6144,128]{1,0:T(8,128)(2,1)} %collective-permute-done.2.refs_1_, bf16[6144,128]{1,0:T(8,128)(2,1)} %collective-permute-done.4.refs_2_, ...), custom_call_target="tpu_custom_call" | custom-call | tf_op jit(solution)/shard_map/lowered/pallas_call | solution.py:295
  125.3 16.8 %all-to-all-start.3 = ((bf16[128,8,128]{2,1,0:T(8,128)(2,1)}), bf16[128,8,128]{2,1,0:T(8,128)(2,1)S(1)}, u32[]{:S(2)}, u32[]{:S(2)}) async-start(bf16[128,8,128]{2,1,0:T(8,128)(2,1)} %bitcast.14), calls=%async_computation.3 | async-start | bytes 524288 | tf_op jit(solution)/shard_map/all_to_all | solution.py:25
  142.2 0.0 copy-done.3
  142.2 3.3 %collective-permute-start.6 = (bf16[4,256,128]{2,1,0:T(8,128)(2,1)S(1)}, bf16[4,256,128]{2,1,0:T(8,128)(2,1)S(1)}, u32[]{:S(2)}, u32[]{:S(2)}) collective-permute-start(bf16[4,256,128]{2,1,0:T(8,128)(2,1)S(1)} %copy-done.3), channel_id=1, source_target_pairs={{0,1},{1,0},{4,5},{5,4},{2,3},{3,2},{6,7},{7,6},{8,9},{9,8},{12,13... | collective-permute-start | bytes 786440 | tf_op jit(solution)/shard_map/ppermute | solution.py:509
  145.4 3.1 %collective-permute-start.7 = (bf16[4,256,128]{2,1,0:T(8,128)(2,1)S(1)}, bf16[4,256,128]{2,1,0:T(8,128)(2,1)S(1)}, u32[]{:S(2)}, u32[]{:S(2)}) collective-permute-start(bf16[4,256,128]{2,1,0:T(8,128)(2,1)S(1)} %copy-done.3), channel_id=1, source_target_pairs={{0,4},{1,5},{4,0},{5,1},{2,6},{3,7},{6,2},{7,3},{8,12},{9,13},{12,... | collective-permute-start | bytes 786440 | tf_op jit(solution)/shard_map/ppermute | solution.py:509
  148.5 2.0 %collective-permute-start.8 = (bf16[4,256,128]{2,1,0:T(8,128)(2,1)S(1)}, bf16[4,256,128]{2,1,0:T(8,128)(2,1)S(1)}, u32[]{:S(2)}, u32[]{:S(2)}) collective-permute-start(bf16[4,256,128]{2,1,0:T(8,128)(2,1)S(1)} %copy-done.3), channel_id=1, source_target_pairs={{0,5},{1,4},{4,1},{5,0},{2,7},{3,6},{6,3},{7,2},{8,13},{9,12},{12,... | collective-permute-start | bytes 786440 | tf_op jit(solution)/shard_map/ppermute | solution.py:509
  150.6 0.6 divide_bitcast_fusion.chances_ref
  151.2 1.2 collective-permute-done.6.refs_1_
  152.4 9.9 %collective-permute-done.7.refs_2_ = bf16[4,256,128]{2,1,0:T(8,128)(2,1)S(1)} collective-permute-done((bf16[4,256,128]{2,1,0:T(8,128)(2,1)S(1)}, bf16[4,256,128]{2,1,0:T(8,128)(2,1)S(1)}, u32[]{:S(2)}, u32[]{:S(2)}) %collective-permute-start.7) | collective-permute-done | bytes 262176 | tf_op jit(solution)/shard_map/ppermute | solution.py:509
  162.3 0.0 collective-permute-done.8.refs_3_
  162.3 0.7 copy-done.5
  163.0 0.7 copy-done.6
  163.7 2.4 %projected.1 = bf16[256,128]{1,0:T(8,128)(2,1)} custom-call(bf16[4,256,128]{2,1,0:T(8,128)(2,1)} %get-tuple-element.15.refs_0_, bf16[4,256,128]{2,1,0:T(8,128)(2,1)} %copy-done.4, bf16[4,256,128]{2,1,0:T(8,128)(2,1)} %copy-done.5, bf16[4,256,128]{2,1,0:T(8,128)(2,1)} %copy-done.6, bf16[2048,128]{1,0:T(8,128)(2,1)} %refs_4_.1), custom_call_target="tpu_custom_call" | custom-call | tf_op jit(solution)/shard_map/projected/pallas_call | solution.py:467
  166.1 0.0 all-to-all-done.3
  166.1 0.7 copy-done.2
  166.8 2.1 %combine.1 = bf16[128,128]{1,0:T(8,128)(2,1)} custom-call(bf16[1024,128]{1,0:T(8,128)(2,1)} %bitcast.16, s32[128,4]{1,0:T(8,128)} %get-tuple-element.17.target_ref, f32[4,128]{1,0:T(4,128)} %divide_bitcast_fusion.chances_ref), custom_call_target="tpu_custom_call" | custom-call | tf_op jit(solution)/shard_map/combine/pallas_call | solution.py:328
  (14 shorter events, 0.1 us)
Async XLA Ops:
  4.7 23.2 %collective-permute-start.2 = (bf16[6144,128]{1,0:T(8,128)(2,1)}, bf16[6144,128]{1,0:T(8,128)(2,1)}, u32[]{:S(2)}, u32[]{:S(2)}) collective-permute-start(bf16[6144,128]{1,0:T(8,128)(2,1)} %get-tuple-element.14.refs_0_), channel_id=1, source_target_pairs={{0,4},{1,16},{2,6},{3,18},{4,0},{5,20},{6,2},{7,22},{8,12},{9,24},... | collective-permute-start | bytes 4718600 | tf_op jit(solution)/shard_map/ppermute | solution.py:145
  9.2 43.7 %collective-permute-start.4 = (bf16[6144,128]{1,0:T(8,128)(2,1)}, bf16[6144,128]{1,0:T(8,128)(2,1)}, u32[]{:S(2)}, u32[]{:S(2)}) collective-permute-start(bf16[6144,128]{1,0:T(8,128)(2,1)} %get-tuple-element.14.refs_0_), channel_id=1, source_target_pairs={{0,16},{1,4},{2,18},{3,6},{4,20},{5,0},{6,22},{7,2},{8,24},{9,12},... | collective-permute-start | bytes 4718600 | tf_op jit(solution)/shard_map/ppermute | solution.py:146
  11.7 58.5 %all-to-all-start = ((bf16[32,8,512]{2,1,0:T(8,128)(2,1)}), bf16[32,8,512]{2,1,0:T(8,128)(2,1)S(1)}, u32[]{:S(2)}, u32[]{:S(2)}) async-start(bf16[32,8,512]{2,1,0:T(8,128)(2,1)} %bitcast.22), calls=%async_computation | async-start | bytes 524288 | tf_op jit(solution)/shard_map/all_to_all | solution.py:25
  27.9 48.8 %collective-permute-start.3 = (bf16[6144,128]{1,0:T(8,128)(2,1)}, bf16[6144,128]{1,0:T(8,128)(2,1)S(1)}, u32[]{:S(2)}, u32[]{:S(2)}) collective-permute-start(bf16[6144,128]{1,0:T(8,128)(2,1)} %collective-permute-done.2.refs_1_), channel_id=1, source_target_pairs={{0,16},{1,17},{2,18},{3,19},{4,20},{5,21},{6,22},{7,23},{8,24},{9,... | collective-permute-start | bytes 4718600 | tf_op jit(solution)/shard_map/ppermute | solution.py:147
  52.9 23.7 %collective-permute-start.5 = (bf16[6144,128]{1,0:T(8,128)(2,1)}, bf16[6144,128]{1,0:T(8,128)(2,1)S(1)}, u32[]{:S(2)}, u32[]{:S(2)}) collective-permute-start(bf16[6144,128]{1,0:T(8,128)(2,1)} %collective-permute-done.4.refs_2_), channel_id=1, source_target_pairs={{0,16},{2,18},{4,20},{6,22},{8,24},{10,26},{12,28},{14,30},{17,1},... | collective-permute-start | bytes 4718600 | tf_op jit(solution)/shard_map/ppermute | solution.py:148
  59.1 4.4 %collective-permute-start = (bf16[128,128]{1,0:T(8,128)(2,1)}, bf16[128,128]{1,0:T(8,128)(2,1)S(1)}, u32[]{:S(2)}, u32[]{:S(2)}) collective-permute-start(bf16[128,128]{1,0:T(8,128)(2,1)} %get-tuple-element.12.refs_2_), channel_id=1, source_target_pairs={{0,16},{16,32},{32,48},{48,64},{64,80},{80,96},{96,112},{112,128},... | collective-permute-start | bytes 98312 | tf_op jit(solution)/shard_map/ppermute | solution.py:447
  61.1 5.4 %collective-permute-start.1 = (bf16[128,128]{1,0:T(8,128)(2,1)}, bf16[128,128]{1,0:T(8,128)(2,1)S(1)}, u32[]{:S(2)}, u32[]{:S(2)}) collective-permute-start(bf16[128,128]{1,0:T(8,128)(2,1)} %get-tuple-element.13.refs_1_), channel_id=1, source_target_pairs={{16,0},{32,16},{48,32},{64,48},{80,64},{96,80},{112,96},{128,112},... | collective-permute-start | bytes 98312 | tf_op jit(solution)/shard_map/ppermute | solution.py:448
  63.6 2.9 %copy-start.7 = (bf16[128,128]{1,0:T(8,128)(2,1)}, bf16[128,128]{1,0:T(8,128)(2,1)S(1)}, u32[]{:S(2)}) copy-start(bf16[128,128]{1,0:T(8,128)(2,1)S(1)} %collective-permute-done.refs_0_) | copy-start | bytes 98308
  66.5 0.6 copy-start.8
  72.3 21.5 %all-to-all-start.1 = ((bf16[4,256,640]{2,1,0:T(8,128)(2,1)}), bf16[4,256,640]{2,1,0:T(8,128)(2,1)}, u32[]{:S(2)}, u32[]{:S(2)}) async-start(bf16[4,256,640]{2,1,0:T(8,128)(2,1)} %broadcast_in_dim.53), calls=%async_computation.1 | async-start | bytes 2621440 | tf_op jit(solution)/shard_map/all_to_all | solution.py:25
  76.6 17.2 %copy-start = (bf16[6144,128]{1,0:T(8,128)(2,1)}, bf16[6144,128]{1,0:T(8,128)(2,1)S(1)}, u32[]{:S(2)}) copy-start(bf16[6144,128]{1,0:T(8,128)(2,1)S(1)} %collective-permute-done.3.refs_3_) | copy-start | bytes 4718596
  76.7 17.2 %copy-start.1 = (bf16[6144,128]{1,0:T(8,128)(2,1)}, bf16[6144,128]{1,0:T(8,128)(2,1)S(1)}, u32[]{:S(2)}) copy-start(bf16[6144,128]{1,0:T(8,128)(2,1)S(1)} %collective-permute-done.5.refs_4_) | copy-start | bytes 4718596
  121.7 20.4 %copy-start.9 = (f32[128,4]{0,1:T(4,128)S(1)}, f32[128,4]{0,1:T(4,128)}, u32[]{:S(2)}) copy-start(f32[128,4]{0,1:T(4,128)} %param.24) | copy-start | bytes 6148
  121.7 20.5 %copy-start.3 = (bf16[4,256,128]{2,1,0:T(8,128)(2,1)S(1)}, bf16[4,256,128]{2,1,0:T(8,128)(2,1)}, u32[]{:S(2)}) copy-start(bf16[4,256,128]{2,1,0:T(8,128)(2,1)} %get-tuple-element.15.refs_0_) | copy-start | bytes 786436
  125.3 40.8 %all-to-all-start.3 = ((bf16[128,8,128]{2,1,0:T(8,128)(2,1)}), bf16[128,8,128]{2,1,0:T(8,128)(2,1)S(1)}, u32[]{:S(2)}, u32[]{:S(2)}) async-start(bf16[128,8,128]{2,1,0:T(8,128)(2,1)} %bitcast.14), calls=%async_computation.3 | async-start | bytes 524288 | tf_op jit(solution)/shard_map/all_to_all | solution.py:25
  142.2 10.2 %collective-permute-start.6 = (bf16[4,256,128]{2,1,0:T(8,128)(2,1)S(1)}, bf16[4,256,128]{2,1,0:T(8,128)(2,1)S(1)}, u32[]{:S(2)}, u32[]{:S(2)}) collective-permute-start(bf16[4,256,128]{2,1,0:T(8,128)(2,1)S(1)} %copy-done.3), channel_id=1, source_target_pairs={{0,1},{1,0},{4,5},{5,4},{2,3},{3,2},{6,7},{7,6},{8,9},{9,8},{12,13... | collective-permute-start | bytes 786440 | tf_op jit(solution)/shard_map/ppermute | solution.py:509
  145.4 16.8 %collective-permute-start.7 = (bf16[4,256,128]{2,1,0:T(8,128)(2,1)S(1)}, bf16[4,256,128]{2,1,0:T(8,128)(2,1)S(1)}, u32[]{:S(2)}, u32[]{:S(2)}) collective-permute-start(bf16[4,256,128]{2,1,0:T(8,128)(2,1)S(1)} %copy-done.3), channel_id=1, source_target_pairs={{0,4},{1,5},{4,0},{5,1},{2,6},{3,7},{6,2},{7,3},{8,12},{9,13},{12,... | collective-permute-start | bytes 786440 | tf_op jit(solution)/shard_map/ppermute | solution.py:509
  148.5 13.7 %collective-permute-start.8 = (bf16[4,256,128]{2,1,0:T(8,128)(2,1)S(1)}, bf16[4,256,128]{2,1,0:T(8,128)(2,1)S(1)}, u32[]{:S(2)}, u32[]{:S(2)}) collective-permute-start(bf16[4,256,128]{2,1,0:T(8,128)(2,1)S(1)} %copy-done.3), channel_id=1, source_target_pairs={{0,5},{1,4},{4,1},{5,0},{2,7},{3,6},{6,3},{7,2},{8,13},{9,12},{12,... | collective-permute-start | bytes 786440 | tf_op jit(solution)/shard_map/ppermute | solution.py:509
  152.4 9.9 %copy-start.4 = (bf16[4,256,128]{2,1,0:T(8,128)(2,1)}, bf16[4,256,128]{2,1,0:T(8,128)(2,1)S(1)}, u32[]{:S(2)}) copy-start(bf16[4,256,128]{2,1,0:T(8,128)(2,1)S(1)} %collective-permute-done.6.refs_1_) | copy-start | bytes 786436
  162.3 0.7 copy-start.5
  163.0 0.7 copy-start.6
  166.1 0.7 copy-start.2

commit v3 on v2

--- a/solution.py
+++ b/solution.py
@@ -51,7 +51,10 @@
     tall_rows, columns = weights[0].shape
 
     def kernel(rows_ref, gain_ref, routes_ref, *refs):
-        weight_refs, (out_ref, target_ref, stacked_ref, held_ref, sems) = refs[:3], refs[3:]
+        weight_refs, refs = refs[:3], refs[3:]
+        out_ref, target_ref, stacked_ref, held_ref, here_ref, sems = refs
+        rows_copy = pltpu.make_async_copy(rows_ref, here_ref, sems.at[6])
+        rows_copy.start()
         arriving = [
             pltpu.make_async_copy(ref, held_ref.at[i], sems.at[i])
             for i, ref in enumerate(weight_refs)
@@ -65,13 +68,14 @@
         for copy in arriving:
             copy.start()
         block = 2 * lax.axis_index("Y") + lax.axis_index("X")
-        values = rows_ref[...].astype(jnp.float32)
-        scale = lax.rsqrt(jnp.mean(values * values, axis=-1, keepdims=True) + EPSILON)
+        rows_copy.wait()
         for come, go in zip(arriving, leaving):
             come.wait()
             go.start()
+        values = here_ref[...].astype(jnp.float32)
+        scale = lax.rsqrt(jnp.mean(values * values, axis=-1, keepdims=True) + EPSILON)
         start = pl.multiple_of(block * width, width)
-        own = rows_ref[:, pl.ds(start, width)].astype(jnp.float32)
+        own = here_ref[:, pl.ds(start, width)].astype(jnp.float32)
         normed = (own * scale * gain_ref[:, pl.ds(start, width)]).astype(jnp.bfloat16)
         first = lax.broadcasted_iota(jnp.int32, (tokens, tokens), 0)
         second = lax.broadcasted_iota(jnp.int32, (tokens, tokens), 1)
@@ -111,11 +115,12 @@
             jax.ShapeDtypeStruct((tokens, TOP_K), jnp.int32),
             jax.ShapeDtypeStruct((3 * tall_rows, columns), jnp.bfloat16),
         ),
-        in_specs=[vmem] * 3 + [anywhere] * 3,
+        in_specs=[anywhere] + [vmem] * 2 + [anywhere] * 3,
         out_specs=(vmem, vmem, anywhere),
         scratch_shapes=[
             pltpu.VMEM((3, tall_rows, columns), jnp.bfloat16),
-            pltpu.SemaphoreType.DMA((6,)),
+            pltpu.VMEM(rows.shape, rows.dtype),
+            pltpu.SemaphoreType.DMA((7,)),
         ],
         name="dispatch",
     )(rows, gain[None, :], routes.T, *weights)
@@ -175,92 +180,83 @@
         pltpu.make_async_copy(there.at[rows], target, sem).start()
 
 
-def gated(rows, shares, arrived):
-    parts, n, wide = rows.shape
+def gated(rows, mixed, shares, arrived):
+    parts, n, k = rows.shape
     u = shares[0].shape[1]
-    k = 4 * u
-    j = wide - k
+    j = mixed.shape[1]
     whole = parts * k
 
-    def kernel(rows_ref, _, *refs):
+    def kernel(rows_ref, mixed_ref, _, *refs):
         shares, refs = refs[:5], refs[5:]
-        out_ref, heads_ref, here_ref, weights_ref, hidden_ref, sems, row_sems, out_sems = refs
+        out_ref, here_ref, weights_ref, hidden_ref, sems, row_sems, out_sems = refs
         native, order = share_order()
         arrivals = [
             pltpu.make_async_copy(rows_ref.at[part], here_ref.at[part], row_sems.at[part])
             for part in range(parts)
         ]
-        heads = pltpu.make_async_copy(
-            here_ref.at[:, :, pl.ds(k, j)], heads_ref, row_sems.at[parts]
+        arrivals.append(
+            pltpu.make_async_copy(
+                mixed_ref, hidden_ref.at[:, pl.ds(4 * u, j)], row_sems.at[parts]
+            )
         )
         targets = [
             (weights_ref.at[i, :, pl.ds(side * u, u)], sems.at[i, side])
             for i in range(4)
             for side in range(2)
         ]
-
-        def fetch(i):
-            for side in range(2):
-                target, sem = targets[2 * i + side]
-                copy_share(native, shares, i, side * whole, whole, target, sem)
-
-        for part in range(parts):
-            arrivals[part].start()
-        for i in range(4):
-            fetch(i)
-        for part in range(parts):
-            arrivals[part].wait()
-        heads.start()
-        leaving = []
+        for copy in arrivals:
+            copy.start()
         for i in range(4):
             for side in range(2):
-                target, sem = targets[2 * i + side]
-                pltpu.make_async_copy(shares[1].at[pl.ds(0, whole)], target, sem).wait()
-            total = dot(here_ref[0, :, :k], weights_ref[i, :k, :])
+                copy_share(native, shares, i, side * whole, whole, *targets[2 * i + side])
+        for copy in arrivals:
+            copy.wait()
+        for target in targets:
+            pltpu.make_async_copy(shares[1].at[pl.ds(0, whole)], *target).wait()
+        for i in range(4):
+            total = dot(here_ref[0], weights_ref[i, :k, :])
             for part in range(1, parts):
-                piece = here_ref[part, :, :k]
-                total = total + dot(piece, weights_ref[i, part * k : (part + 1) * k, :])
-            hidden_ref[i] = activate(total[:, :u], total[:, u:])
+                total = total + dot(here_ref[part], weights_ref[i, part * k : (part + 1) * k, :])
             lane = pl.multiple_of(order[i] * u, u)
-            for copy in range(parts):
-                out = out_ref.at[copy, :, pl.ds(lane, u)]
-                leaving.append(
-                    pltpu.make_async_copy(hidden_ref.at[i], out, out_sems.at[i, copy])
-                )
-                leaving[-1].start()
+            hidden_ref[:, pl.ds(lane, u)] = activate(total[:, :u], total[:, u:])
+        leaving = [
+            pltpu.make_async_copy(hidden_ref, out_ref.at[copy], out_sems.at[copy])
+            for copy in range(parts)
+        ]
+        for copy in leaving:
+            copy.start()
         for copy in leaving:
             copy.wait()
-        heads.wait()
 
     anywhere = pl.BlockSpec(memory_space=pl.ANY)
     return pl.pallas_call(
         kernel,
-        out_shape=(
-            jax.ShapeDtypeStruct((parts, n, 4 * u), jnp.bfloat16),
-            jax.ShapeDtypeStruct((parts, n, j), jnp.bfloat16),
-        ),
-        in_specs=[anywhere] * 7,
-        out_specs=(anywhere, anywhere),
+        out_shape=jax.ShapeDtypeStruct((parts, n, 4 * u + j), jnp.bfloat16),
+        in_specs=[anywhere] * 8,
+        out_specs=anywhere,
         scratch_shapes=[
-            pltpu.VMEM((parts, n, wide), jnp.bfloat16),
+            pltpu.VMEM((parts, n, k), jnp.bfloat16),
             pltpu.VMEM((4, whole, 2 * u), jnp.bfloat16),
-            pltpu.VMEM((4, n, u), jnp.bfloat16),
+            pltpu.VMEM((n, 4 * u + j), jnp.bfloat16),
             pltpu.SemaphoreType.DMA((4, 2)),
             pltpu.SemaphoreType.DMA((parts + 1,)),
-            pltpu.SemaphoreType.DMA((4, parts)),
+            pltpu.SemaphoreType.DMA((parts,)),
         ],
         name="gated",
-    )(rows, arrived, *shares)
+    )(rows, mixed, arrived, *shares)
 
 
 def lowered(hidden, shares, slots):
-    parts, n, k = hidden.shape
+    parts, n, wide = hidden.shape
     f = shares[0].shape[1]
+    k = 4 * f
+    j = wide - k
     whole = parts * k
     half = k // 2
 
     def kernel(hidden_ref, *refs):
-        shares, (out_ref, here_ref, weights_ref, sems, row_sems) = refs[:5], refs[5:]
+        shares, refs = refs[:5], refs[5:]
+        out_ref, heads_ref, here_ref, weights_ref, sems, row_sems = refs
         native, order = share_order()
         targets = [
             (weights_ref.at[i // 2, :, pl.ds((i % 2) * f, f)], sems.at[i]) for i in range(4)
@@ -269,39 +265,44 @@
             pltpu.make_async_copy(hidden_ref.at[part], here_ref.at[part], row_sems.at[part])
             for part in range(parts)
         ]
-        for i in range(2):
+        heads = pltpu.make_async_copy(
+            here_ref.at[:, :, pl.ds(k, j)], heads_ref, row_sems.at[parts]
+        )
+        for copy in arrivals:
+            copy.start()
+        for i in range(4):
             copy_share(native, shares, i, 2 * whole, whole, *targets[i])
-        for part in range(parts):
-            arrivals[part].start()
-        for i in range(2, 4):
-            copy_share(native, shares, i, 2 * whole, whole, *targets[i])
+        for copy in arrivals:
+            copy.wait()
+        heads.start()
+        for target in targets:
+            pltpu.make_async_copy(shares[1].at[pl.ds(0, whole)], *target).wait()
         for pair in range(2):
-            for i in (2 * pair, 2 * pair + 1):
-                pltpu.make_async_copy(shares[1].at[pl.ds(0, whole)], *targets[i]).wait()
             total = jnp.zeros((n, 2 * f), jnp.float32)
-            for Y, X in itertools.product(range(2), repeat=2):
-                if pair == 0:
-                    arrivals[2 * Y + X].wait()
-                for h in range(2):
-                    unit = (8 * Y + 4 * h + 2 * X) * f
-                    piece = here_ref[2 * Y + X, :, h * half : (h + 1) * half]
-                    total = total + dot(piece, weights_ref[pair, unit : unit + half, :])
+            for Y, X, h in itertools.product(range(2), repeat=3):
+                unit = (8 * Y + 4 * h + 2 * X) * f
+                piece = here_ref[2 * Y + X, :, h * half : (h + 1) * half]
+                total = total + dot(piece, weights_ref[pair, unit : unit + half, :])
             rounded = total.astype(jnp.bfloat16).reshape(n // slots, slots, 2 * f)
             out_ref[:, order[2 * pair]] = rounded[:, :, :f]
             out_ref[:, order[2 * pair + 1]] = rounded[:, :, f:]
+        heads.wait()
 
     vmem = pl.BlockSpec(memory_space=pltpu.VMEM)
     anywhere = pl.BlockSpec(memory_space=pl.ANY)
     return pl.pallas_call(
         kernel,
-        out_shape=jax.ShapeDtypeStruct((n // slots, 4, slots, f), jnp.bfloat16),
+        out_shape=(
+            jax.ShapeDtypeStruct((n // slots, 4, slots, f), jnp.bfloat16),
+            jax.ShapeDtypeStruct((parts, n, j), jnp.bfloat16),
+        ),
         in_specs=[anywhere] * 6,
-        out_specs=vmem,
+        out_specs=(vmem, anywhere),
         scratch_shapes=[
-            pltpu.VMEM((parts, n, k), jnp.bfloat16),
+            pltpu.VMEM((parts, n, wide), jnp.bfloat16),
             pltpu.VMEM((2, whole, 2 * f), jnp.bfloat16),
             pltpu.SemaphoreType.DMA((4,)),
-            pltpu.SemaphoreType.DMA((parts,)),
+            pltpu.SemaphoreType.DMA((parts + 1,)),
         ],
         name="lowered",
     )(hidden, *shares)
@@ -334,23 +335,24 @@
     )(results, target, chances)
 
 
-def rotary_tables(places, width):
+def rotary_tables(first, rows, width):
     quarter = HEAD_DIM // 4
     lane = jnp.arange(width, dtype=jnp.int32)
     frequency = BASE ** (-(lane % quarter).astype(jnp.float32) / quarter)
-    row = (places // GRID_W).astype(jnp.float32)[:, None]
-    column = (places % GRID_W).astype(jnp.float32)[:, None]
-    angle = jnp.where(lane % HEAD_DIM < HEAD_DIM // 2, row, column) * frequency
+    at = jnp.arange(GRID_W + rows, dtype=jnp.int32)
+    place = jnp.where(at < GRID_W, at, at - GRID_W + first)
+    angle = place.astype(jnp.float32)[:, None] * frequency
     sign = jnp.where(lane % (2 * quarter) < quarter, -1.0, 1.0)
     return jnp.cos(angle), jnp.sin(angle) * sign
 
 
-def projections(rows, gain, query_weight, key_weight, value_weight, places):
+def projections(rows, gain, query_weight, key_weight, value_weight):
     tokens, _ = rows.shape
     width = query_weight.shape[1]
     half = width // 2
     quarter = HEAD_DIM // 4
-    cosine, sine = rotary_tables(places, width)
+    spans = tokens // GRID_W
+    cosine, sine = rotary_tables(lax.axis_index(EP) * spans, spans, width)
 
     def kernel(
         rows_ref, gain_ref, query_ref, key_ref, value_ref, cos_ref, sin_ref, out_ref, *pair_refs
@@ -358,15 +360,25 @@
         values = rows_ref[...].astype(jnp.float32)
         scale = lax.rsqrt(jnp.mean(values * values, axis=-1, keepdims=True) + EPSILON)
         normed = (values * scale * gain_ref[...]).astype(jnp.bfloat16)
-        lane = lax.broadcasted_iota(jnp.int32, (tokens, width), 1) % (2 * quarter)
+        lane = lax.broadcasted_iota(jnp.int32, (tokens, width), 1)
+        near = lane % (2 * quarter) < quarter
+        by_row = lax.broadcasted_iota(jnp.int32, (GRID_W, width), 1) % HEAD_DIM < HEAD_DIM // 2
+
+        def table(ref):
+            columns = ref[:GRID_W, :]
+            parts = [
+                jnp.where(by_row, ref[GRID_W + i : GRID_W + i + 1, :], columns)
+                for i in range(spans)
+            ]
+            return jnp.concatenate(parts, axis=0)
+
+        cos, sin = table(cos_ref), table(sin_ref)
 
         def turned(a):
             partner = jnp.where(
-                lane < quarter,
-                pltpu.roll(a, width - quarter, 1),
-                pltpu.roll(a, quarter, 1),
+                near, pltpu.roll(a, width - quarter, 1), pltpu.roll(a, quarter, 1)
             )
-            return (a * cos_ref[...] + partner * sin_ref[...]).astype(jnp.bfloat16)
+            return (a * cos + partner * sin).astype(jnp.bfloat16)
 
         def flipped(weight_ref):
             return lax.dot_general(
@@ -376,11 +388,7 @@
         out_ref[...] = turned(dot(normed, query_ref[...]))
         keys, mine = flipped(key_ref), flipped(value_ref)
         both = jnp.concatenate([keys, mine], axis=1)
-        rounded = jnp.where(
-            lax.broadcasted_iota(jnp.int32, (tokens, width), 1) < half,
-            turned(both),
-            both.astype(jnp.bfloat16),
-        )
+        rounded = jnp.where(lane < half, turned(both), both.astype(jnp.bfloat16))
         for i, ref in enumerate(pair_refs):
             ref[...] = rounded[i * WINDOW : (i + 1) * WINDOW]
 
@@ -438,11 +446,7 @@
 
 
 def attention(mixer_input, mixer_gain, query_weight, key_weight, value_weight, sink_logit):
-    tokens = mixer_input.shape[0]
-    places = lax.axis_index(EP) * tokens + jnp.arange(tokens, dtype=jnp.int32)
-    query, *pieces = projections(
-        mixer_input, mixer_gain, query_weight, key_weight, value_weight, places
-    )
+    query, *pieces = projections(mixer_input, mixer_gain, query_weight, key_weight, value_weight)
     up = [(i, i + 1) for i in range(lax.axis_size(EP) - 1)]
     before = lax.ppermute(pieces[-1], EP, up)
     after = lax.ppermute(pieces[0], EP, [(j, i) for i, j in up])
@@ -500,17 +504,16 @@
     shares = gather_shares(own)
     received = swap(outgoing.reshape(experts, slots, width), EP)
     mixed = attention(mixer_input, mixer_gain, query_weight, key_weight, value_weight, sink_logit)
-    beside = jnp.concatenate([received.reshape(experts * slots, width), mixed], axis=1)
-    rows = spread(beside, ("Y", "X"))
+    rows = spread(received.reshape(experts * slots, width), ("Y", "X"))
     arrived = shares[3][:8] + shares[4][:8]
-    inner, heads = gated(rows, shares, arrived)
+    inner = gated(rows, mixed, shares, arrived)
     hidden = swap(inner, ("Y", "X"))
+    result, heads = lowered(hidden, shares, slots)
+    returned = swap(result.reshape(4 * experts, slots, -1), (*EP, "h", "p"))
     heads = [heads] + [
         lax.ppermute(heads, ("h", "p"), [(i, i ^ k) for i in range(4)])
         for k in range(1, 4)
     ]
-    result = lowered(hidden, shares, slots)
-    returned = swap(result.reshape(4 * experts, slots, -1), (*EP, "h", "p"))
     mixer_output = projected(heads, output_weight)
     chances = jax.nn.softmax(route_logits.T, axis=0)
     expert_output = combine(

time: 170 us -> 156 us (0.918)
  waiting for transfers between devices: 31.3 us -> 15.4 us
  blocking collectives: 21.7 us -> 26 us
  Pallas kernels: 25.1 us -> 23.4 us
    all_to_all x3, waiting for transfers between devices: 16.5 us -> 0.01 us  [swap(): return lax.all_to_all(pieces, axis, 0, 0, tiled=True)]
    all_to_all x1, blocking collectives: 21.7 us -> 26 us  [swap(): return lax.all_to_all(pieces, axis, 0, 0, tiled=True)]
    unnamed x20 -> x18, local copies, waits for them, and re-layouts: 2.71 us -> 3.68 us
  transfers between devices with their start and end apart: 12 -> 12, of which waited for: 5 -> 4; matrix products, arithmetic and copies ran while one was open for 3% -> 2% of each run, Pallas kernels for 5% -> 6%
where the time goes in v3:
time: 156 us; the launch traced here: 155 us
  starting transfers between devices  83 us (53%)
  blocking collectives  26 us (17%)
  Pallas kernels  23.4 us (15%)
  waiting for transfers between devices  15.4 us (10%)
  local copies, waits for them, and re-layouts  4.72 us (3%)
  other arithmetic  2.07 us (1%)
    all_to_all x3, starting transfers between devices, swap(): return lax.all_to_all(pieces, axis, 0, 0, tiled=True)  36.9 us
    all_to_all x1, blocking collectives, swap(): return lax.all_to_all(pieces, axis, 0, 0, tiled=True)  26 us
    ppermute x1, starting transfers between devices, gather_shares(): third = lax.ppermute(first, axes, device_pairs(trade))  25 us
    ppermute x3, waiting for transfers between devices, shards(): lax.ppermute(heads, ('h', 'p'), [(i, i ^ k) for i in range(4)])  11.3 us
    ppermute x3, starting transfers between devices, shards(): lax.ppermute(heads, ('h', 'p'), [(i, i ^ k) for i in range(4)])  8.37 us
    pallas_call x1, Pallas kernels, gated(): pl.pallas_call(kernel, out_shape=jax.ShapeDtypeStruct((parts, n, 4 * u +...  4.97 us
    ppermute x1, starting transfers between devices, gather_shares(): first = lax.ppermute(own, axes, device_pairs(outer))  4.5 us
    pallas_call x1, Pallas kernels, dispatch(): pl.pallas_call(kernel, out_shape=(jax.ShapeDtypeStruct((experts * slots,...  3.84 us
  transfers between devices with their start and end apart: 12, of which 4 were waited for; matrix products, arithmetic and copies ran while one was open for 2% of the time, Pallas kernels for 6%

profile of v3, /device:TPU:1, one launch (start us, length us, event | category | flops | bytes accessed | tf_op | source)
XLA Modules:
  0.0 155.4 jit_solution(16619835234770976235)
XLA Ops:
  0.6 3.8 %dispatch.1 = (bf16[256,512]{1,0:T(8,128)(2,1)}, s32[128,4]{1,0:T(8,128)}, bf16[6144,128]{1,0:T(8,128)(2,1)}) custom-call(bf16[128,2048]{1,0:T(8,128)(2,1)} %rows_ref.2, f32[1,2048]{1,0:T(1,128)} %bitcast.23, s32[4,128]{1,0:T(4,128)} %bitcast.25, bf16[2048,128]{1,0:T(8,128)(2,1)} %bitcast.16, bf16[2048,128]{1,0:T(8,128)(2,1)} %bitcast.17, ...), custom_call_target="tpu_custom_call" | custom-call | tf_op jit(solution)/shard_map/dispatch/pallas_call | solution.py:111
  4.5 4.5 %collective-permute-start.2 = (bf16[6144,128]{1,0:T(8,128)(2,1)}, bf16[6144,128]{1,0:T(8,128)(2,1)}, u32[]{:S(2)}, u32[]{:S(2)}) collective-permute-start(bf16[6144,128]{1,0:T(8,128)(2,1)} %get-tuple-element.14.refs_0_), channel_id=1, source_target_pairs={{0,4},{1,16},{2,6},{3,18},{4,0},{5,20},{6,2},{7,22},{8,12},{9,24},... | collective-permute-start | bytes 4718600 | tf_op jit(solution)/shard_map/ppermute | solution.py:150
  9.0 2.5 %collective-permute-start.4 = (bf16[6144,128]{1,0:T(8,128)(2,1)}, bf16[6144,128]{1,0:T(8,128)(2,1)}, u32[]{:S(2)}, u32[]{:S(2)}) collective-permute-start(bf16[6144,128]{1,0:T(8,128)(2,1)} %get-tuple-element.14.refs_0_), channel_id=1, source_target_pairs={{0,16},{1,4},{2,18},{3,6},{4,20},{5,0},{6,22},{7,2},{8,24},{9,12},... | collective-permute-start | bytes 4718600 | tf_op jit(solution)/shard_map/ppermute | solution.py:151
  11.5 15.4 %all-to-all-start = ((bf16[32,8,512]{2,1,0:T(8,128)(2,1)}), bf16[32,8,512]{2,1,0:T(8,128)(2,1)S(1)}, u32[]{:S(2)}, u32[]{:S(2)}) async-start(bf16[32,8,512]{2,1,0:T(8,128)(2,1)} %bitcast.22), calls=%async_computation | async-start | bytes 524288 | tf_op jit(solution)/shard_map/all_to_all | solution.py:25
  26.9 0.8 collective-permute-done.2.refs_1_
  27.7 25.0 %collective-permute-start.3 = (bf16[6144,128]{1,0:T(8,128)(2,1)}, bf16[6144,128]{1,0:T(8,128)(2,1)S(1)}, u32[]{:S(2)}, u32[]{:S(2)}) collective-permute-start(bf16[6144,128]{1,0:T(8,128)(2,1)} %collective-permute-done.2.refs_1_), channel_id=1, source_target_pairs={{0,16},{1,17},{2,18},{3,19},{4,20},{5,21},{6,22},{7,23},{8,24},{9,... | collective-permute-start | bytes 4718600 | tf_op jit(solution)/shard_map/ppermute | solution.py:152
  52.7 0.0 collective-permute-done.4.refs_2_
  52.7 1.3 collective-permute-start.5
  54.0 0.0 all-to-all-done
  54.0 1.0 broadcast_in_dim.28
  55.1 4.3 %all-to-all-start.1 = ((bf16[4,256,512]{2,1,0:T(8,128)(2,1)}), bf16[4,256,512]{2,1,0:T(8,128)(2,1)}, u32[]{:S(2)}, u32[]{:S(2)}) async-start(bf16[4,256,512]{2,1,0:T(8,128)(2,1)} %broadcast_in_dim.28), calls=%async_computation.1 | async-start | bytes 2097152 | tf_op jit(solution)/shard_map/all_to_all | solution.py:25
  59.4 0.8 fusion
  60.2 3.5 %projections.1 = (bf16[256,128]{1,0:T(8,128)(2,1)}, bf16[128,128]{1,0:T(8,128)(2,1)}, bf16[128,128]{1,0:T(8,128)(2,1)}) custom-call(bf16[256,2048]{1,0:T(8,128)(2,1)} %rows_ref.3, f32[1,2048]{1,0:T(1,128)} %bitcast.24, bf16[2048,128]{1,0:T(8,128)(2,1)} %query_ref.1, bf16[64,2048]{1,0:T(8,128)(2,1)} %bitcast.19, bf16[64,2048]{1,0:T(8,128)(2,1)} %bitcast.20, ...), custom_call_target="tpu_custom_call" | custom-call | tf_op jit(solution)/shard_map/projections/pallas_call | solution.py:396
  63.7 1.9 %collective-permute-start = (bf16[128,128]{1,0:T(8,128)(2,1)}, bf16[128,128]{1,0:T(8,128)(2,1)S(1)}, u32[]{:S(2)}, u32[]{:S(2)}) collective-permute-start(bf16[128,128]{1,0:T(8,128)(2,1)} %get-tuple-element.12.refs_2_), channel_id=1, source_target_pairs={{0,16},{16,32},{32,48},{48,64},{64,80},{80,96},{96,112},{112,128},... | collective-permute-start | bytes 98312 | tf_op jit(solution)/shard_map/ppermute | solution.py:451
  65.6 2.5 %collective-permute-start.1 = (bf16[128,128]{1,0:T(8,128)(2,1)}, bf16[128,128]{1,0:T(8,128)(2,1)S(1)}, u32[]{:S(2)}, u32[]{:S(2)}) collective-permute-start(bf16[128,128]{1,0:T(8,128)(2,1)} %get-tuple-element.13.refs_1_), channel_id=1, source_target_pairs={{16,0},{32,16},{48,32},{64,48},{80,64},{96,80},{112,96},{128,112},... | collective-permute-start | bytes 98312 | tf_op jit(solution)/shard_map/ppermute | solution.py:452
  68.2 0.0 collective-permute-done.refs_0_
  68.2 0.0 copy-start.6
  68.2 3.3 %collective-permute-done.1.refs_3_ = bf16[128,128]{1,0:T(8,128)(2,1)S(1)} collective-permute-done((bf16[128,128]{1,0:T(8,128)(2,1)}, bf16[128,128]{1,0:T(8,128)(2,1)S(1)}, u32[]{:S(2)}, u32[]{:S(2)}) %collective-permute-start.1) | collective-permute-done | bytes 32800 | tf_op jit(solution)/shard_map/ppermute | solution.py:452
  71.5 0.0 copy-start.7
  71.5 0.0 copy-done.6
  71.5 0.6 copy-done.7
  72.1 3.1 %banded.1.mixed_ref = bf16[256,128]{1,0:T(8,128)(2,1)} custom-call(f32[2]{0:T(128)} %sink_ref.1, bf16[256,128]{1,0:T(8,128)(2,1)} %get-tuple-element.11.query_ref, bf16[128,128]{1,0:T(8,128)(2,1)} %copy-done.6, bf16[128,128]{1,0:T(8,128)(2,1)} %get-tuple-element.13.refs_1_, bf16[128,128]{1,0:T(8,128)(2,1)} %get-tuple-element.12.refs_2_, ...), custom_call_target="tpu_custom_call" | custom-call | tf_op jit(solution)/shard_map/banded/pallas_call | solution.py:439
  75.2 0.0 collective-permute-done.3.refs_3_
  75.2 0.0 collective-permute-done.5.refs_4_
  75.3 0.0 copy-start.1
  75.3 0.6 slice_add_fusion._
  75.9 0.0 all-to-all-done.1.rows_ref
  75.9 0.5 copy-done
  76.4 0.5 copy-done.1
  76.9 5.0 %gated.1 = bf16[4,256,640]{2,1,0:T(8,128)(2,1)} custom-call(bf16[4,256,512]{2,1,0:T(8,128)(2,1)} %all-to-all-done.1.rows_ref, bf16[256,128]{1,0:T(8,128)(2,1)} %banded.1.mixed_ref, bf16[8,128]{1,0:T(8,128)(2,1)} %slice_add_fusion._, bf16[6144,128]{1,0:T(8,128)(2,1)} %get-tuple-element.14.refs_0_, bf16[6144,128]{1,0:T(8,128)(2,1)} %collective-permute-done.2.refs_1_, ...), custom_call_target="tpu_custom_call" | custom-call | tf_op jit(solution)/shard_map/gated/pallas_call | solution.py:232
  81.9 26.0 %all_to_all.20.hidden_ref = bf16[4,256,640]{2,1,0:T(8,128)(2,1)} all-to-all(bf16[4,256,640]{2,1,0:T(8,128)(2,1)} %gated.1), channel_id=1, replica_groups=mesh['ep_0'=16,'ep_1'=2,'Y'=2,'h'=2,'X'=2,'p'=2] {'Y','X'}, dimensions={0} | all-to-all | bytes 2621440 | tf_op jit(solution)/shard_map/all_to_all | solution.py:25
  107.9 3.4 %lowered.1 = (bf16[32,4,8,128]{3,2,1,0:T(8,128)(2,1)}, bf16[4,256,128]{2,1,0:T(8,128)(2,1)}) custom-call(bf16[4,256,640]{2,1,0:T(8,128)(2,1)} %all_to_all.20.hidden_ref, bf16[6144,128]{1,0:T(8,128)(2,1)} %get-tuple-element.14.refs_0_, bf16[6144,128]{1,0:T(8,128)(2,1)} %collective-permute-done.2.refs_1_, bf16[6144,128]{1,0:T(8,128)(2,1)} %collective-permute-done.4.refs_2_, ...), custom_call_target="tpu_custom_call" | custom-call | tf_op jit(solution)/shard_map/lowered/pallas_call | solution.py:293
  111.3 17.2 %all-to-all-start.3 = ((bf16[128,8,128]{2,1,0:T(8,128)(2,1)}), bf16[128,8,128]{2,1,0:T(8,128)(2,1)S(1)}, u32[]{:S(2)}, u32[]{:S(2)}) async-start(bf16[128,8,128]{2,1,0:T(8,128)(2,1)} %bitcast.21), calls=%async_computation.3 | async-start | bytes 524288 | tf_op jit(solution)/shard_map/all_to_all | solution.py:25
  128.5 0.0 copy-done.8
  128.5 3.3 %collective-permute-start.6 = (bf16[4,256,128]{2,1,0:T(8,128)(2,1)}, bf16[4,256,128]{2,1,0:T(8,128)(2,1)S(1)}, u32[]{:S(2)}, u32[]{:S(2)}) collective-permute-start(bf16[4,256,128]{2,1,0:T(8,128)(2,1)} %get-tuple-element.15.refs_0_), channel_id=1, source_target_pairs={{0,1},{1,0},{4,5},{5,4},{2,3},{3,2},{6,7},{7,6},{8,9},{9,8},{12,13... | collective-permute-start | bytes 786440 | tf_op jit(solution)/shard_map/ppermute | solution.py:514
  131.8 3.1 %collective-permute-start.7 = (bf16[4,256,128]{2,1,0:T(8,128)(2,1)}, bf16[4,256,128]{2,1,0:T(8,128)(2,1)S(1)}, u32[]{:S(2)}, u32[]{:S(2)}) collective-permute-start(bf16[4,256,128]{2,1,0:T(8,128)(2,1)} %get-tuple-element.15.refs_0_), channel_id=1, source_target_pairs={{0,4},{1,5},{4,0},{5,1},{2,6},{3,7},{6,2},{7,3},{8,12},{9,13},{12,... | collective-permute-start | bytes 786440 | tf_op jit(solution)/shard_map/ppermute | solution.py:514
  134.9 2.0 %collective-permute-start.8 = (bf16[4,256,128]{2,1,0:T(8,128)(2,1)}, bf16[4,256,128]{2,1,0:T(8,128)(2,1)S(1)}, u32[]{:S(2)}, u32[]{:S(2)}) collective-permute-start(bf16[4,256,128]{2,1,0:T(8,128)(2,1)} %get-tuple-element.15.refs_0_), channel_id=1, source_target_pairs={{0,5},{1,4},{4,1},{5,0},{2,7},{3,6},{6,3},{7,2},{8,13},{9,12},{12,... | collective-permute-start | bytes 786440 | tf_op jit(solution)/shard_map/ppermute | solution.py:514
  136.9 0.5 divide_bitcast_fusion.chances_ref
  137.5 1.5 collective-permute-done.6.refs_1_
  139.0 9.8 %collective-permute-done.7.refs_2_ = bf16[4,256,128]{2,1,0:T(8,128)(2,1)S(1)} collective-permute-done((bf16[4,256,128]{2,1,0:T(8,128)(2,1)}, bf16[4,256,128]{2,1,0:T(8,128)(2,1)S(1)}, u32[]{:S(2)}, u32[]{:S(2)}) %collective-permute-start.7) | collective-permute-done | bytes 262176 | tf_op jit(solution)/shard_map/ppermute | solution.py:514
  148.8 0.0 collective-permute-done.8.refs_3_
  148.8 0.0 copy-done.3
  148.8 0.7 copy-done.4
  149.5 0.7 copy-done.5
  150.1 2.4 %projected.1 = bf16[256,128]{1,0:T(8,128)(2,1)} custom-call(bf16[4,256,128]{2,1,0:T(8,128)(2,1)} %get-tuple-element.15.refs_0_, bf16[4,256,128]{2,1,0:T(8,128)(2,1)} %copy-done.3, bf16[4,256,128]{2,1,0:T(8,128)(2,1)} %copy-done.4, bf16[4,256,128]{2,1,0:T(8,128)(2,1)} %copy-done.5, bf16[2048,128]{1,0:T(8,128)(2,1)} %refs_4_.1), custom_call_target="tpu_custom_call" | custom-call | tf_op jit(solution)/shard_map/projected/pallas_call | solution.py:471
  152.6 0.0 all-to-all-done.3
  152.6 0.7 copy-done.2
  153.3 2.1 %combine.1 = bf16[128,128]{1,0:T(8,128)(2,1)} custom-call(bf16[1024,128]{1,0:T(8,128)(2,1)} %bitcast.15, s32[128,4]{1,0:T(8,128)} %get-tuple-element.17.target_ref, f32[4,128]{1,0:T(4,128)} %divide_bitcast_fusion.chances_ref), custom_call_target="tpu_custom_call" | custom-call | tf_op jit(solution)/shard_map/combine/pallas_call | solution.py:329
  (10 shorter events, 0.1 us)
Async XLA Ops:
  4.5 23.2 %collective-permute-start.2 = (bf16[6144,128]{1,0:T(8,128)(2,1)}, bf16[6144,128]{1,0:T(8,128)(2,1)}, u32[]{:S(2)}, u32[]{:S(2)}) collective-permute-start(bf16[6144,128]{1,0:T(8,128)(2,1)} %get-tuple-element.14.refs_0_), channel_id=1, source_target_pairs={{0,4},{1,16},{2,6},{3,18},{4,0},{5,20},{6,2},{7,22},{8,12},{9,24},... | collective-permute-start | bytes 4718600 | tf_op jit(solution)/shard_map/ppermute | solution.py:150
  9.0 43.7 %collective-permute-start.4 = (bf16[6144,128]{1,0:T(8,128)(2,1)}, bf16[6144,128]{1,0:T(8,128)(2,1)}, u32[]{:S(2)}, u32[]{:S(2)}) collective-permute-start(bf16[6144,128]{1,0:T(8,128)(2,1)} %get-tuple-element.14.refs_0_), channel_id=1, source_target_pairs={{0,16},{1,4},{2,18},{3,6},{4,20},{5,0},{6,22},{7,2},{8,24},{9,12},... | collective-permute-start | bytes 4718600 | tf_op jit(solution)/shard_map/ppermute | solution.py:151
  11.5 42.5 %all-to-all-start = ((bf16[32,8,512]{2,1,0:T(8,128)(2,1)}), bf16[32,8,512]{2,1,0:T(8,128)(2,1)S(1)}, u32[]{:S(2)}, u32[]{:S(2)}) async-start(bf16[32,8,512]{2,1,0:T(8,128)(2,1)} %bitcast.22), calls=%async_computation | async-start | bytes 524288 | tf_op jit(solution)/shard_map/all_to_all | solution.py:25
  27.7 47.6 %collective-permute-start.3 = (bf16[6144,128]{1,0:T(8,128)(2,1)}, bf16[6144,128]{1,0:T(8,128)(2,1)S(1)}, u32[]{:S(2)}, u32[]{:S(2)}) collective-permute-start(bf16[6144,128]{1,0:T(8,128)(2,1)} %collective-permute-done.2.refs_1_), channel_id=1, source_target_pairs={{0,16},{1,17},{2,18},{3,19},{4,20},{5,21},{6,22},{7,23},{8,24},{9,... | collective-permute-start | bytes 4718600 | tf_op jit(solution)/shard_map/ppermute | solution.py:152
  52.7 22.5 %collective-permute-start.5 = (bf16[6144,128]{1,0:T(8,128)(2,1)}, bf16[6144,128]{1,0:T(8,128)(2,1)S(1)}, u32[]{:S(2)}, u32[]{:S(2)}) collective-permute-start(bf16[6144,128]{1,0:T(8,128)(2,1)} %collective-permute-done.4.refs_2_), channel_id=1, source_target_pairs={{0,16},{2,18},{4,20},{6,22},{8,24},{10,26},{12,28},{14,30},{17,1},... | collective-permute-start | bytes 4718600 | tf_op jit(solution)/shard_map/ppermute | solution.py:153
  55.1 20.8 %all-to-all-start.1 = ((bf16[4,256,512]{2,1,0:T(8,128)(2,1)}), bf16[4,256,512]{2,1,0:T(8,128)(2,1)}, u32[]{:S(2)}, u32[]{:S(2)}) async-start(bf16[4,256,512]{2,1,0:T(8,128)(2,1)} %broadcast_in_dim.28), calls=%async_computation.1 | async-start | bytes 2097152 | tf_op jit(solution)/shard_map/all_to_all | solution.py:25
  63.7 4.4 %collective-permute-start = (bf16[128,128]{1,0:T(8,128)(2,1)}, bf16[128,128]{1,0:T(8,128)(2,1)S(1)}, u32[]{:S(2)}, u32[]{:S(2)}) collective-permute-start(bf16[128,128]{1,0:T(8,128)(2,1)} %get-tuple-element.12.refs_2_), channel_id=1, source_target_pairs={{0,16},{16,32},{32,48},{48,64},{64,80},{80,96},{96,112},{112,128},... | collective-permute-start | bytes 98312 | tf_op jit(solution)/shard_map/ppermute | solution.py:451
  65.6 5.8 %collective-permute-start.1 = (bf16[128,128]{1,0:T(8,128)(2,1)}, bf16[128,128]{1,0:T(8,128)(2,1)S(1)}, u32[]{:S(2)}, u32[]{:S(2)}) collective-permute-start(bf16[128,128]{1,0:T(8,128)(2,1)} %get-tuple-element.13.refs_1_), channel_id=1, source_target_pairs={{16,0},{32,16},{48,32},{64,48},{80,64},{96,80},{112,96},{128,112},... | collective-permute-start | bytes 98312 | tf_op jit(solution)/shard_map/ppermute | solution.py:452
  68.2 3.3 %copy-start.6 = (bf16[128,128]{1,0:T(8,128)(2,1)}, bf16[128,128]{1,0:T(8,128)(2,1)S(1)}, u32[]{:S(2)}) copy-start(bf16[128,128]{1,0:T(8,128)(2,1)S(1)} %collective-permute-done.refs_0_) | copy-start | bytes 98308
  71.5 0.6 copy-start.7
  75.2 1.2 copy-start
  75.3 1.6 %copy-start.1 = (bf16[6144,128]{1,0:T(8,128)(2,1)}, bf16[6144,128]{1,0:T(8,128)(2,1)S(1)}, u32[]{:S(2)}) copy-start(bf16[6144,128]{1,0:T(8,128)(2,1)S(1)} %collective-permute-done.5.refs_4_) | copy-start | bytes 4718596
  107.9 20.6 %copy-start.8 = (f32[128,4]{0,1:T(4,128)S(1)}, f32[128,4]{0,1:T(4,128)}, u32[]{:S(2)}) copy-start(f32[128,4]{0,1:T(4,128)} %param.24) | copy-start | bytes 6148
  111.3 41.3 %all-to-all-start.3 = ((bf16[128,8,128]{2,1,0:T(8,128)(2,1)}), bf16[128,8,128]{2,1,0:T(8,128)(2,1)S(1)}, u32[]{:S(2)}, u32[]{:S(2)}) async-start(bf16[128,8,128]{2,1,0:T(8,128)(2,1)} %bitcast.21), calls=%async_computation.3 | async-start | bytes 524288 | tf_op jit(solution)/shard_map/all_to_all | solution.py:25
  128.5 10.5 %collective-permute-start.6 = (bf16[4,256,128]{2,1,0:T(8,128)(2,1)}, bf16[4,256,128]{2,1,0:T(8,128)(2,1)S(1)}, u32[]{:S(2)}, u32[]{:S(2)}) collective-permute-start(bf16[4,256,128]{2,1,0:T(8,128)(2,1)} %get-tuple-element.15.refs_0_), channel_id=1, source_target_pairs={{0,1},{1,0},{4,5},{5,4},{2,3},{3,2},{6,7},{7,6},{8,9},{9,8},{12,13... | collective-permute-start | bytes 786440 | tf_op jit(solution)/shard_map/ppermute | solution.py:514
  131.8 17.0 %collective-permute-start.7 = (bf16[4,256,128]{2,1,0:T(8,128)(2,1)}, bf16[4,256,128]{2,1,0:T(8,128)(2,1)S(1)}, u32[]{:S(2)}, u32[]{:S(2)}) collective-permute-start(bf16[4,256,128]{2,1,0:T(8,128)(2,1)} %get-tuple-element.15.refs_0_), channel_id=1, source_target_pairs={{0,4},{1,5},{4,0},{5,1},{2,6},{3,7},{6,2},{7,3},{8,12},{9,13},{12,... | collective-permute-start | bytes 786440 | tf_op jit(solution)/shard_map/ppermute | solution.py:514
  134.9 13.9 %collective-permute-start.8 = (bf16[4,256,128]{2,1,0:T(8,128)(2,1)}, bf16[4,256,128]{2,1,0:T(8,128)(2,1)S(1)}, u32[]{:S(2)}, u32[]{:S(2)}) collective-permute-start(bf16[4,256,128]{2,1,0:T(8,128)(2,1)} %get-tuple-element.15.refs_0_), channel_id=1, source_target_pairs={{0,5},{1,4},{4,1},{5,0},{2,7},{3,6},{6,3},{7,2},{8,13},{9,12},{12,... | collective-permute-start | bytes 786440 | tf_op jit(solution)/shard_map/ppermute | solution.py:514
  139.0 9.8 %copy-start.3 = (bf16[4,256,128]{2,1,0:T(8,128)(2,1)}, bf16[4,256,128]{2,1,0:T(8,128)(2,1)S(1)}, u32[]{:S(2)}) copy-start(bf16[4,256,128]{2,1,0:T(8,128)(2,1)S(1)} %collective-permute-done.6.refs_1_) | copy-start | bytes 786436
  148.8 0.7 copy-start.4
  149.5 0.7 copy-start.5
  152.6 0.7 copy-start.2

commit v4 on v3

--- a/solution.py
+++ b/solution.py
@@ -308,31 +308,28 @@
     )(hidden, *shares)
 
 
-def combine(results, target, chances):
-    slots, f = results.shape
+def selectors(target, logits, slots):
     tokens = target.shape[0]
 
-    def kernel(results_ref, target_ref, chances_ref, out_ref):
-        chances = tall(chances_ref[...])
+    def kernel(target_ref, logits_ref, out_ref):
+        chances = tall(jax.nn.softmax(logits_ref[...], axis=0))
         lane = lax.broadcasted_iota(jnp.int32, (tokens, slots), 1)
-        chosen = [
-            (target_ref[:, k : k + 1] == lane).astype(jnp.float32).astype(jnp.bfloat16)
-            for k in range(TOP_K)
-        ]
-        picked = dot(jnp.concatenate(chosen, axis=0), results_ref[...])
-        total = jnp.zeros((tokens, f), jnp.float32)
+        rest = jnp.zeros((tokens, slots), jnp.float32)
         for k in range(TOP_K):
-            total = total + picked[k * tokens : (k + 1) * tokens] * chances[:, k : k + 1]
-        out_ref[...] = total.astype(jnp.bfloat16)
+            rest = jnp.where(target_ref[:, k : k + 1] == lane, chances[:, k : k + 1], rest)
+        for part in range(3):
+            rounded = rest.astype(jnp.bfloat16)
+            out_ref[part * tokens : (part + 1) * tokens, :] = rounded
+            rest = rest - rounded.astype(jnp.float32)
 
     vmem = pl.BlockSpec(memory_space=pltpu.VMEM)
     return pl.pallas_call(
         kernel,
-        out_shape=jax.ShapeDtypeStruct((tokens, f), jnp.bfloat16),
-        in_specs=[vmem] * 3,
+        out_shape=jax.ShapeDtypeStruct((3 * tokens, slots), jnp.bfloat16),
+        in_specs=[vmem] * 2,
         out_specs=vmem,
-        name="combine",
-    )(results, target, chances)
+        name="selectors",
+    )(target, logits)
 
 
 def rotary_tables(first, rows, width):
@@ -453,28 +450,26 @@
     return banded(query, [before, *pieces, after], sink_logit)
 
 
-def projected(heads, weight):
-    _, n, j = heads[0].shape
-    f = weight.shape[1]
-
-    def kernel(*refs):
-        heads_refs, weight_ref, out_ref = refs[:4], refs[4], refs[5]
-        total = jnp.zeros((n, f), jnp.float32)
-        for k in range(4):
-            h, p = lax.axis_index("h") ^ (k // 2), lax.axis_index("p") ^ (k % 2)
-            for Y, X in itertools.product(range(2), repeat=2):
-                unit = pl.multiple_of((8 * Y + 4 * h + 2 * X + p) * j, j)
-                total = total + dot(heads_refs[k][2 * Y + X], weight_ref[pl.ds(unit, j), :])
-        out_ref[...] = total.astype(jnp.bfloat16)
+def partial_sums(heads, columns):
+    parts, n, _ = heads.shape
+    f = columns[0].shape[2]
+
+    def kernel(heads_ref, *refs):
+        columns_refs, out_refs = refs[:4], refs[4:]
+        for columns_ref, out_ref in zip(columns_refs, out_refs):
+            total = dot(heads_ref[0], columns_ref[0])
+            for part in range(1, parts):
+                total = total + dot(heads_ref[part], columns_ref[part])
+            out_ref[...] = total
 
     vmem = pl.BlockSpec(memory_space=pltpu.VMEM)
     return pl.pallas_call(
         kernel,
-        out_shape=jax.ShapeDtypeStruct((n, f), jnp.bfloat16),
+        out_shape=[jax.ShapeDtypeStruct((n, f), jnp.float32)] * 4,
         in_specs=[vmem] * 5,
-        out_specs=vmem,
-        name="projected",
-    )(*heads, weight)
+        out_specs=[vmem] * 4,
+        name="partial_sums",
+    )(heads, *columns)
 
 
 def shards(
@@ -510,15 +505,23 @@
     hidden = swap(inner, ("Y", "X"))
     result, heads = lowered(hidden, shares, slots)
     returned = swap(result.reshape(4 * experts, slots, -1), (*EP, "h", "p"))
-    heads = [heads] + [
-        lax.ppermute(heads, ("h", "p"), [(i, i ^ k) for i in range(4)])
-        for k in range(1, 4)
-    ]
-    mixer_output = projected(heads, output_weight)
-    chances = jax.nn.softmax(route_logits.T, axis=0)
-    expert_output = combine(
-        returned.reshape(experts * 4 * slots, -1), target, chances
-    )
+    around = [[(i, i ^ k) for i in range(4)] for k in range(4)]
+    size = mixed.shape[1]
+    blocks = output_weight.reshape(2, 2, 2, 2, size, -1)
+    columns = []
+    for k in range(4):
+        h, p = lax.axis_index("h") ^ (k // 2), lax.axis_index("p") ^ (k % 2)
+        piece = lax.dynamic_slice_in_dim(blocks, h, 1, 1)
+        piece = lax.dynamic_slice_in_dim(piece, p, 1, 3).reshape(4, size, -1)
+        columns.append(lax.ppermute(piece, ("h", "p"), around[k]) if k else piece)
+    own_sum, *sums = partial_sums(heads, columns)
+    for k in range(1, 4):
+        own_sum = own_sum + lax.ppermute(sums[k - 1], ("h", "p"), around[k])
+    mixer_output = own_sum.astype(jnp.bfloat16)
+    chances = selectors(target, route_logits.T, experts * 4 * slots)
+    parts = dot(chances, returned.reshape(experts * 4 * slots, -1))
+    parts = parts.reshape(3, rows_here, -1)
+    expert_output = (parts[0] + (parts[1] + parts[2])).astype(jnp.bfloat16)
     return (mixer_output, expert_output)
 
 

time: 156 us -> 164 us (1.051)
  starting transfers between devices: 83 us -> 91.3 us
  waiting for transfers between devices: 15.4 us -> 11.4 us
    ppermute x3 -> x6, starting transfers between devices: 8.37 us -> 16.7 us  [the longest x3 8.36 us: shards(): columns.append(lax.ppermute(piece, ('h', 'p'), around[k]) if k else piece)]
    ppermute x3 -> x6, waiting for transfers between devices: 11.3 us -> 7.3 us  [the longest x3 5.45 us: shards(): columns.append(lax.ppermute(piece, ('h', 'p'), around[k]) if k else piece)]
    convert_element_type x0 -> x2, other arithmetic: none -> 2.19 us  [the longest x1 1.56 us: shards(): mixer_output = own_sum.astype(jnp.bfloat16)]
    unnamed x18 -> x16, local copies, waits for them, and re-layouts: 3.68 us -> 2.28 us
  transfers between devices with their start and end apart: 12 -> 15, of which waited for: 4 -> 5; matrix products, arithmetic and copies ran while one was open for 2% -> 3% of each run, Pallas kernels for 6% -> 7%
where the time goes in v4:
time: 164 us; the launch traced here: 162 us
  starting transfers between devices  91.3 us (56%)
  blocking collectives  26 us (16%)
  Pallas kernels  23.6 us (14%)
  waiting for transfers between devices  11.4 us (7%)
  local copies, waits for them, and re-layouts  4.04 us (2%)
  other arithmetic  3.69 us (2%)
    all_to_all x3, starting transfers between devices, swap(): return lax.all_to_all(pieces, axis, 0, 0, tiled=True)  36.9 us
    all_to_all x1, blocking collectives, swap(): return lax.all_to_all(pieces, axis, 0, 0, tiled=True)  26 us
    ppermute x1, starting transfers between devices, gather_shares(): third = lax.ppermute(first, axes, device_pairs(trade))  25 us
    ppermute x3, starting transfers between devices, shards(): columns.append(lax.ppermute(piece, ('h', 'p'), around[k]) if k else piece)  8.36 us
    ppermute x3, starting transfers between devices, shards(): own_sum = own_sum + lax.ppermute(sums[k - 1], ('h', 'p'), around[k])  8.36 us
    ppermute x3, waiting for transfers between devices, shards(): columns.append(lax.ppermute(piece, ('h', 'p'), around[k]) if k else piece)  5.45 us
    pallas_call x1, Pallas kernels, gated(): pl.pallas_call(kernel, out_shape=jax.ShapeDtypeStruct((parts, n, 4 * u +...  5 us
    ppermute x1, starting transfers between devices, gather_shares(): first = lax.ppermute(own, axes, device_pairs(outer))  4.5 us
  transfers between devices with their start and end apart: 15, of which 5 were waited for; matrix products, arithmetic and copies ran while one was open for 3% of the time, Pallas kernels for 7%

profile of v4, /device:TPU:1, one launch (start us, length us, event | category | flops | bytes accessed | tf_op | source)
XLA Modules:
  0.0 162.5 jit_solution(15402407005926973704)
XLA Ops:
  0.6 3.9 %dispatch.1 = (bf16[256,512]{1,0:T(8,128)(2,1)}, s32[128,4]{1,0:T(8,128)}, bf16[6144,128]{1,0:T(8,128)(2,1)}) custom-call(bf16[128,2048]{1,0:T(8,128)(2,1)} %rows_ref.2, f32[1,2048]{1,0:T(1,128)} %bitcast.42, s32[4,128]{1,0:T(4,128)} %bitcast.44, bf16[2048,128]{1,0:T(8,128)(2,1)} %bitcast.30, bf16[2048,128]{1,0:T(8,128)(2,1)} %bitcast.31, ...), custom_call_target="tpu_custom_call" | custom-call | tf_op jit(solution)/shard_map/dispatch/pallas_call | solution.py:111
  4.5 4.5 %collective-permute-start.2 = (bf16[6144,128]{1,0:T(8,128)(2,1)}, bf16[6144,128]{1,0:T(8,128)(2,1)}, u32[]{:S(2)}, u32[]{:S(2)}) collective-permute-start(bf16[6144,128]{1,0:T(8,128)(2,1)} %get-tuple-element.18.refs_0_), channel_id=1, source_target_pairs={{0,4},{1,16},{2,6},{3,18},{4,0},{5,20},{6,2},{7,22},{8,12},{9,24},... | collective-permute-start | bytes 4718600 | tf_op jit(solution)/shard_map/ppermute | solution.py:150
  9.0 2.5 %collective-permute-start.4 = (bf16[6144,128]{1,0:T(8,128)(2,1)}, bf16[6144,128]{1,0:T(8,128)(2,1)}, u32[]{:S(2)}, u32[]{:S(2)}) collective-permute-start(bf16[6144,128]{1,0:T(8,128)(2,1)} %get-tuple-element.18.refs_0_), channel_id=1, source_target_pairs={{0,16},{1,4},{2,18},{3,6},{4,20},{5,0},{6,22},{7,2},{8,24},{9,12},... | collective-permute-start | bytes 4718600 | tf_op jit(solution)/shard_map/ppermute | solution.py:151
  11.6 15.4 %all-to-all-start = ((bf16[32,8,512]{2,1,0:T(8,128)(2,1)}), bf16[32,8,512]{2,1,0:T(8,128)(2,1)S(1)}, u32[]{:S(2)}, u32[]{:S(2)}) async-start(bf16[32,8,512]{2,1,0:T(8,128)(2,1)} %bitcast.38), calls=%async_computation | async-start | bytes 524288 | tf_op jit(solution)/shard_map/all_to_all | solution.py:25
  26.9 0.8 collective-permute-done.2.refs_1_
  27.7 25.0 %collective-permute-start.3 = (bf16[6144,128]{1,0:T(8,128)(2,1)}, bf16[6144,128]{1,0:T(8,128)(2,1)S(1)}, u32[]{:S(2)}, u32[]{:S(2)}) collective-permute-start(bf16[6144,128]{1,0:T(8,128)(2,1)} %collective-permute-done.2.refs_1_), channel_id=1, source_target_pairs={{0,16},{1,17},{2,18},{3,19},{4,20},{5,21},{6,22},{7,23},{8,24},{9,... | collective-permute-start | bytes 4718600 | tf_op jit(solution)/shard_map/ppermute | solution.py:152
  52.7 0.0 collective-permute-done.4.refs_2_
  52.7 1.3 collective-permute-start.5
  54.0 0.0 all-to-all-done
  54.1 1.1 broadcast_in_dim.26
  55.1 4.3 %all-to-all-start.1 = ((bf16[4,256,512]{2,1,0:T(8,128)(2,1)}), bf16[4,256,512]{2,1,0:T(8,128)(2,1)}, u32[]{:S(2)}, u32[]{:S(2)}) async-start(bf16[4,256,512]{2,1,0:T(8,128)(2,1)} %broadcast_in_dim.26), calls=%async_computation.1 | async-start | bytes 2097152 | tf_op jit(solution)/shard_map/all_to_all | solution.py:25
  59.4 0.9 fusion.4
  60.3 3.5 %projections.1 = (bf16[256,128]{1,0:T(8,128)(2,1)}, bf16[128,128]{1,0:T(8,128)(2,1)}, bf16[128,128]{1,0:T(8,128)(2,1)}) custom-call(bf16[256,2048]{1,0:T(8,128)(2,1)} %rows_ref.3, f32[1,2048]{1,0:T(1,128)} %bitcast.43, bf16[2048,128]{1,0:T(8,128)(2,1)} %query_ref.1, bf16[64,2048]{1,0:T(8,128)(2,1)} %bitcast.35, bf16[64,2048]{1,0:T(8,128)(2,1)} %bitcast.36, ...), custom_call_target="tpu_custom_call" | custom-call | tf_op jit(solution)/shard_map/projections/pallas_call | solution.py:393
  63.8 1.9 %collective-permute-start = (bf16[128,128]{1,0:T(8,128)(2,1)}, bf16[128,128]{1,0:T(8,128)(2,1)S(1)}, u32[]{:S(2)}, u32[]{:S(2)}) collective-permute-start(bf16[128,128]{1,0:T(8,128)(2,1)} %get-tuple-element.16.refs_2_), channel_id=1, source_target_pairs={{0,16},{16,32},{32,48},{48,64},{64,80},{80,96},{96,112},{112,128},... | collective-permute-start | bytes 98312 | tf_op jit(solution)/shard_map/ppermute | solution.py:448
  65.7 2.5 %collective-permute-start.1 = (bf16[128,128]{1,0:T(8,128)(2,1)}, bf16[128,128]{1,0:T(8,128)(2,1)S(1)}, u32[]{:S(2)}, u32[]{:S(2)}) collective-permute-start(bf16[128,128]{1,0:T(8,128)(2,1)} %get-tuple-element.17.refs_1_), channel_id=1, source_target_pairs={{16,0},{32,16},{48,32},{64,48},{80,64},{96,80},{112,96},{128,112},... | collective-permute-start | bytes 98312 | tf_op jit(solution)/shard_map/ppermute | solution.py:449
  68.2 0.0 collective-permute-done.refs_0_
  68.2 3.3 %collective-permute-done.1.refs_3_ = bf16[128,128]{1,0:T(8,128)(2,1)S(1)} collective-permute-done((bf16[128,128]{1,0:T(8,128)(2,1)}, bf16[128,128]{1,0:T(8,128)(2,1)S(1)}, u32[]{:S(2)}, u32[]{:S(2)}) %collective-permute-start.1) | collective-permute-done | bytes 32800 | tf_op jit(solution)/shard_map/ppermute | solution.py:449
  71.6 0.6 copy-done.7
  72.2 3.2 %banded.1.mixed_ref = bf16[256,128]{1,0:T(8,128)(2,1)} custom-call(f32[2]{0:T(128)} %sink_ref.1, bf16[256,128]{1,0:T(8,128)(2,1)} %get-tuple-element.15.query_ref, bf16[128,128]{1,0:T(8,128)(2,1)} %copy-done.6, bf16[128,128]{1,0:T(8,128)(2,1)} %get-tuple-element.17.refs_1_, bf16[128,128]{1,0:T(8,128)(2,1)} %get-tuple-element.16.refs_2_, ...), custom_call_target="tpu_custom_call" | custom-call | tf_op jit(solution)/shard_map/banded/pallas_call | solution.py:436
  75.3 0.0 collective-permute-done.3.refs_3_
  75.3 0.0 collective-permute-done.5.refs_4_
  75.3 0.6 slice_add_fusion.1._
  76.0 0.0 all-to-all-done.1.rows_ref
  76.0 0.5 copy-done
  76.5 0.5 copy-done.1
  77.0 5.0 %gated.1 = bf16[4,256,640]{2,1,0:T(8,128)(2,1)} custom-call(bf16[4,256,512]{2,1,0:T(8,128)(2,1)} %all-to-all-done.1.rows_ref, bf16[256,128]{1,0:T(8,128)(2,1)} %banded.1.mixed_ref, bf16[8,128]{1,0:T(8,128)(2,1)} %slice_add_fusion.1._, bf16[6144,128]{1,0:T(8,128)(2,1)} %get-tuple-element.18.refs_0_, bf16[6144,128]{1,0:T(8,128)(2,1)} %collective-permute-done.2.refs_1_, ...), custom_call_target="tpu_custom_call" | custom-call | tf_op jit(solution)/shard_map/gated/pallas_call | solution.py:232
  82.0 26.0 %all_to_all.20.hidden_ref = bf16[4,256,640]{2,1,0:T(8,128)(2,1)} all-to-all(bf16[4,256,640]{2,1,0:T(8,128)(2,1)} %gated.1), channel_id=1, replica_groups=mesh['ep_0'=16,'ep_1'=2,'Y'=2,'h'=2,'X'=2,'p'=2] {'Y','X'}, dimensions={0} | all-to-all | bytes 2621440 | tf_op jit(solution)/shard_map/all_to_all | solution.py:25
  108.0 3.5 %lowered.1 = (bf16[32,4,8,128]{3,2,1,0:T(8,128)(2,1)}, bf16[4,256,128]{2,1,0:T(8,128)(2,1)}) custom-call(bf16[4,256,640]{2,1,0:T(8,128)(2,1)} %all_to_all.20.hidden_ref, bf16[6144,128]{1,0:T(8,128)(2,1)} %get-tuple-element.18.refs_0_, bf16[6144,128]{1,0:T(8,128)(2,1)} %collective-permute-done.2.refs_1_, bf16[6144,128]{1,0:T(8,128)(2,1)} %collective-permute-done.4.refs_2_, ...), custom_call_target="tpu_custom_call" | custom-call | tf_op jit(solution)/shard_map/lowered/pallas_call | solution.py:293
  111.5 17.2 %all-to-all-start.3 = ((bf16[128,8,128]{2,1,0:T(8,128)(2,1)}), bf16[128,8,128]{2,1,0:T(8,128)(2,1)S(1)}, u32[]{:S(2)}, u32[]{:S(2)}) async-start(bf16[128,8,128]{2,1,0:T(8,128)(2,1)} %bitcast.37), calls=%async_computation.3 | async-start | bytes 524288 | tf_op jit(solution)/shard_map/all_to_all | solution.py:25
  128.7 0.7 constant_dynamic-slice_fusion
  129.4 3.2 %collective-permute-start.6 = (bf16[4,128,128]{2,1,0:T(8,128)(2,1)S(1)}, bf16[4,128,128]{2,1,0:T(8,128)(2,1)S(1)}, u32[]{:S(2)}, u32[]{:S(2)}) collective-permute-start(bf16[4,128,128]{2,1,0:T(8,128)(2,1)S(1)} %bitcast.41), channel_id=1, source_target_pairs={{0,1},{1,0},{4,5},{5,4},{2,3},{3,2},{6,7},{7,6},{8,9},{9,8},{12,13... | collective-permute-start | bytes 393224 | tf_op jit(solution)/shard_map/ppermute | solution.py:516
  132.7 3.1 %collective-permute-start.7 = (bf16[4,128,128]{2,1,0:T(8,128)(2,1)S(1)}, bf16[4,128,128]{2,1,0:T(8,128)(2,1)S(1)}, u32[]{:S(2)}, u32[]{:S(2)}) collective-permute-start(bf16[4,128,128]{2,1,0:T(8,128)(2,1)S(1)} %bitcast.40), channel_id=1, source_target_pairs={{0,4},{1,5},{4,0},{5,1},{2,6},{3,7},{6,2},{7,3},{8,12},{9,13},{12,... | collective-permute-start | bytes 393224 | tf_op jit(solution)/shard_map/ppermute | solution.py:516
  135.8 2.0 %collective-permute-start.8 = (bf16[4,128,128]{2,1,0:T(8,128)(2,1)S(1)}, bf16[4,128,128]{2,1,0:T(8,128)(2,1)S(1)}, u32[]{:S(2)}, u32[]{:S(2)}) collective-permute-start(bf16[4,128,128]{2,1,0:T(8,128)(2,1)S(1)} %bitcast.39), channel_id=1, source_target_pairs={{0,5},{1,4},{4,1},{5,0},{2,7},{3,6},{6,3},{7,2},{8,13},{9,12},{12,... | collective-permute-start | bytes 393224 | tf_op jit(solution)/shard_map/ppermute | solution.py:516
  137.8 0.0 collective-permute-done.6.refs_1_
  137.8 2.0 %collective-permute-done.7.refs_2_ = bf16[4,128,128]{2,1,0:T(8,128)(2,1)S(1)} collective-permute-done((bf16[4,128,128]{2,1,0:T(8,128)(2,1)S(1)}, bf16[4,128,128]{2,1,0:T(8,128)(2,1)S(1)}, u32[]{:S(2)}, u32[]{:S(2)}) %collective-permute-start.7) | collective-permute-done | bytes 131104 | tf_op jit(solution)/shard_map/ppermute | solution.py:516
  139.9 3.4 %collective-permute-done.8.refs_3_ = bf16[4,128,128]{2,1,0:T(8,128)(2,1)S(1)} collective-permute-done((bf16[4,128,128]{2,1,0:T(8,128)(2,1)S(1)}, bf16[4,128,128]{2,1,0:T(8,128)(2,1)S(1)}, u32[]{:S(2)}, u32[]{:S(2)}) %collective-permute-start.8) | collective-permute-done | bytes 131104 | tf_op jit(solution)/shard_map/ppermute | solution.py:516
  143.3 0.7 copy-done.5
  144.0 2.3 %partial_sums.1 = (f32[256,128]{1,0:T(8,128)}, f32[256,128]{1,0:T(8,128)}, f32[256,128]{1,0:T(8,128)}, f32[256,128]{1,0:T(8,128)}) custom-call(bf16[4,256,128]{2,1,0:T(8,128)(2,1)} %get-tuple-element.19.heads_ref, bf16[4,128,128]{2,1,0:T(8,128)(2,1)} %bitcast.34, bf16[4,128,128]{2,1,0:T(8,128)(2,1)} %copy-done.3, bf16[4,128,128]{2,1,0:T(8,128)(2,1)} %copy-done.4, ...), custom_call_target="tpu_custom_call" | custom-call | tf_op jit(solution)/shard_map/partial_sums/pallas_call | solution.py:466
  146.2 2.2 %collective-permute-start.10 = (f32[256,128]{1,0:T(8,128)}, f32[256,128]{1,0:T(8,128)S(1)}, u32[]{:S(2)}, u32[]{:S(2)}) collective-permute-start(f32[256,128]{1,0:T(8,128)} %get-tuple-element.22), channel_id=1, source_target_pairs={{0,4},{1,5},{4,0},{5,1},{2,6},{3,7},{6,2},{7,3},{8,12},{9,13},{12,... | collective-permute-start | bytes 393224 | tf_op jit(solution)/shard_map/ppermute | solution.py:519
  148.4 3.0 %collective-permute-start.11 = (f32[256,128]{1,0:T(8,128)}, f32[256,128]{1,0:T(8,128)S(1)}, u32[]{:S(2)}, u32[]{:S(2)}) collective-permute-start(f32[256,128]{1,0:T(8,128)} %get-tuple-element.23), channel_id=1, source_target_pairs={{0,5},{1,4},{4,1},{5,0},{2,7},{3,6},{6,3},{7,2},{8,13},{9,12},{12,... | collective-permute-start | bytes 393224 | tf_op jit(solution)/shard_map/ppermute | solution.py:519
  151.5 3.1 %collective-permute-start.9 = (f32[256,128]{1,0:T(8,128)}, f32[256,128]{1,0:T(8,128)S(1)}, u32[]{:S(2)}, u32[]{:S(2)}) collective-permute-start(f32[256,128]{1,0:T(8,128)} %get-tuple-element.21), channel_id=1, source_target_pairs={{0,1},{1,0},{4,5},{5,4},{2,3},{3,2},{6,7},{7,6},{8,9},{9,8},{12,13... | collective-permute-start | bytes 393224 | tf_op jit(solution)/shard_map/ppermute | solution.py:519
  154.6 2.3 %selectors.1 = bf16[384,1024]{1,0:T(8,128)(2,1)} custom-call(s32[128,4]{1,0:T(8,128)} %get-tuple-element.24.target_ref, f32[4,128]{1,0:T(4,128)} %bitcast.45), custom_call_target="tpu_custom_call" | custom-call | tf_op jit(solution)/shard_map/selectors/pallas_call | solution.py:326
  156.9 0.0 collective-permute-done.10
  156.9 0.0 collective-permute-done.11
  156.9 1.8 %collective-permute-done.9 = f32[256,128]{1,0:T(8,128)S(1)} collective-permute-done((f32[256,128]{1,0:T(8,128)}, f32[256,128]{1,0:T(8,128)S(1)}, u32[]{:S(2)}, u32[]{:S(2)}) %collective-permute-start.9) | collective-permute-done | bytes 131104 | tf_op jit(solution)/shard_map/ppermute | solution.py:519
  158.8 1.6 add_convert_fusion
  160.3 1.5 fusion
  161.8 0.6 fusion.3
  (15 shorter events, 0.0 us)
Async XLA Ops:
  4.5 23.2 %collective-permute-start.2 = (bf16[6144,128]{1,0:T(8,128)(2,1)}, bf16[6144,128]{1,0:T(8,128)(2,1)}, u32[]{:S(2)}, u32[]{:S(2)}) collective-permute-start(bf16[6144,128]{1,0:T(8,128)(2,1)} %get-tuple-element.18.refs_0_), channel_id=1, source_target_pairs={{0,4},{1,16},{2,6},{3,18},{4,0},{5,20},{6,2},{7,22},{8,12},{9,24},... | collective-permute-start | bytes 4718600 | tf_op jit(solution)/shard_map/ppermute | solution.py:150
  9.0 43.7 %collective-permute-start.4 = (bf16[6144,128]{1,0:T(8,128)(2,1)}, bf16[6144,128]{1,0:T(8,128)(2,1)}, u32[]{:S(2)}, u32[]{:S(2)}) collective-permute-start(bf16[6144,128]{1,0:T(8,128)(2,1)} %get-tuple-element.18.refs_0_), channel_id=1, source_target_pairs={{0,16},{1,4},{2,18},{3,6},{4,20},{5,0},{6,22},{7,2},{8,24},{9,12},... | collective-permute-start | bytes 4718600 | tf_op jit(solution)/shard_map/ppermute | solution.py:151
  11.6 42.5 %all-to-all-start = ((bf16[32,8,512]{2,1,0:T(8,128)(2,1)}), bf16[32,8,512]{2,1,0:T(8,128)(2,1)S(1)}, u32[]{:S(2)}, u32[]{:S(2)}) async-start(bf16[32,8,512]{2,1,0:T(8,128)(2,1)} %bitcast.38), calls=%async_computation | async-start | bytes 524288 | tf_op jit(solution)/shard_map/all_to_all | solution.py:25
  27.7 47.6 %collective-permute-start.3 = (bf16[6144,128]{1,0:T(8,128)(2,1)}, bf16[6144,128]{1,0:T(8,128)(2,1)S(1)}, u32[]{:S(2)}, u32[]{:S(2)}) collective-permute-start(bf16[6144,128]{1,0:T(8,128)(2,1)} %collective-permute-done.2.refs_1_), channel_id=1, source_target_pairs={{0,16},{1,17},{2,18},{3,19},{4,20},{5,21},{6,22},{7,23},{8,24},{9,... | collective-permute-start | bytes 4718600 | tf_op jit(solution)/shard_map/ppermute | solution.py:152
  52.7 22.6 %collective-permute-start.5 = (bf16[6144,128]{1,0:T(8,128)(2,1)}, bf16[6144,128]{1,0:T(8,128)(2,1)S(1)}, u32[]{:S(2)}, u32[]{:S(2)}) collective-permute-start(bf16[6144,128]{1,0:T(8,128)(2,1)} %collective-permute-done.4.refs_2_), channel_id=1, source_target_pairs={{0,16},{2,18},{4,20},{6,22},{8,24},{10,26},{12,28},{14,30},{17,1},... | collective-permute-start | bytes 4718600 | tf_op jit(solution)/shard_map/ppermute | solution.py:153
  55.1 20.9 %all-to-all-start.1 = ((bf16[4,256,512]{2,1,0:T(8,128)(2,1)}), bf16[4,256,512]{2,1,0:T(8,128)(2,1)}, u32[]{:S(2)}, u32[]{:S(2)}) async-start(bf16[4,256,512]{2,1,0:T(8,128)(2,1)} %broadcast_in_dim.26), calls=%async_computation.1 | async-start | bytes 2097152 | tf_op jit(solution)/shard_map/all_to_all | solution.py:25
  63.8 4.4 %collective-permute-start = (bf16[128,128]{1,0:T(8,128)(2,1)}, bf16[128,128]{1,0:T(8,128)(2,1)S(1)}, u32[]{:S(2)}, u32[]{:S(2)}) collective-permute-start(bf16[128,128]{1,0:T(8,128)(2,1)} %get-tuple-element.16.refs_2_), channel_id=1, source_target_pairs={{0,16},{16,32},{32,48},{48,64},{64,80},{80,96},{96,112},{112,128},... | collective-permute-start | bytes 98312 | tf_op jit(solution)/shard_map/ppermute | solution.py:448
  65.7 5.8 %collective-permute-start.1 = (bf16[128,128]{1,0:T(8,128)(2,1)}, bf16[128,128]{1,0:T(8,128)(2,1)S(1)}, u32[]{:S(2)}, u32[]{:S(2)}) collective-permute-start(bf16[128,128]{1,0:T(8,128)(2,1)} %get-tuple-element.17.refs_1_), channel_id=1, source_target_pairs={{16,0},{32,16},{48,32},{64,48},{80,64},{96,80},{112,96},{128,112},... | collective-permute-start | bytes 98312 | tf_op jit(solution)/shard_map/ppermute | solution.py:449
  68.2 3.3 %copy-start.6 = (bf16[128,128]{1,0:T(8,128)(2,1)}, bf16[128,128]{1,0:T(8,128)(2,1)S(1)}, u32[]{:S(2)}) copy-start(bf16[128,128]{1,0:T(8,128)(2,1)S(1)} %collective-permute-done.refs_0_) | copy-start | bytes 98308
  71.6 0.6 copy-start.7
  75.3 1.2 copy-start
  75.3 1.6 %copy-start.1 = (bf16[6144,128]{1,0:T(8,128)(2,1)}, bf16[6144,128]{1,0:T(8,128)(2,1)S(1)}, u32[]{:S(2)}) copy-start(bf16[6144,128]{1,0:T(8,128)(2,1)S(1)} %collective-permute-done.5.refs_4_) | copy-start | bytes 4718596
  108.0 20.7 %copy-start.2 = (bf16[2048,128]{1,0:T(8,128)(2,1)S(1)}, bf16[2048,128]{1,0:T(8,128)(2,1)}, u32[]{:S(2)}) copy-start(bf16[2048,128]{1,0:T(8,128)(2,1)} %param.19) | copy-start | bytes 1572868
  111.5 48.9 %all-to-all-start.3 = ((bf16[128,8,128]{2,1,0:T(8,128)(2,1)}), bf16[128,8,128]{2,1,0:T(8,128)(2,1)S(1)}, u32[]{:S(2)}, u32[]{:S(2)}) async-start(bf16[128,8,128]{2,1,0:T(8,128)(2,1)} %bitcast.37), calls=%async_computation.3 | async-start | bytes 524288 | tf_op jit(solution)/shard_map/all_to_all | solution.py:25
  129.4 8.4 %collective-permute-start.6 = (bf16[4,128,128]{2,1,0:T(8,128)(2,1)S(1)}, bf16[4,128,128]{2,1,0:T(8,128)(2,1)S(1)}, u32[]{:S(2)}, u32[]{:S(2)}) collective-permute-start(bf16[4,128,128]{2,1,0:T(8,128)(2,1)S(1)} %bitcast.41), channel_id=1, source_target_pairs={{0,1},{1,0},{4,5},{5,4},{2,3},{3,2},{6,7},{7,6},{8,9},{9,8},{12,13... | collective-permute-start | bytes 393224 | tf_op jit(solution)/shard_map/ppermute | solution.py:516
  132.7 7.2 %collective-permute-start.7 = (bf16[4,128,128]{2,1,0:T(8,128)(2,1)S(1)}, bf16[4,128,128]{2,1,0:T(8,128)(2,1)S(1)}, u32[]{:S(2)}, u32[]{:S(2)}) collective-permute-start(bf16[4,128,128]{2,1,0:T(8,128)(2,1)S(1)} %bitcast.40), channel_id=1, source_target_pairs={{0,4},{1,5},{4,0},{5,1},{2,6},{3,7},{6,2},{7,3},{8,12},{9,13},{12,... | collective-permute-start | bytes 393224 | tf_op jit(solution)/shard_map/ppermute | solution.py:516
  135.8 7.5 %collective-permute-start.8 = (bf16[4,128,128]{2,1,0:T(8,128)(2,1)S(1)}, bf16[4,128,128]{2,1,0:T(8,128)(2,1)S(1)}, u32[]{:S(2)}, u32[]{:S(2)}) collective-permute-start(bf16[4,128,128]{2,1,0:T(8,128)(2,1)S(1)} %bitcast.39), channel_id=1, source_target_pairs={{0,5},{1,4},{4,1},{5,0},{2,7},{3,6},{6,3},{7,2},{8,13},{9,12},{12,... | collective-permute-start | bytes 393224 | tf_op jit(solution)/shard_map/ppermute | solution.py:516
  137.8 5.5 %copy-start.3 = (bf16[4,128,128]{2,1,0:T(8,128)(2,1)}, bf16[4,128,128]{2,1,0:T(8,128)(2,1)S(1)}, u32[]{:S(2)}) copy-start(bf16[4,128,128]{2,1,0:T(8,128)(2,1)S(1)} %collective-permute-done.6.refs_1_) | copy-start | bytes 393220
  139.9 3.4 %copy-start.4 = (bf16[4,128,128]{2,1,0:T(8,128)(2,1)}, bf16[4,128,128]{2,1,0:T(8,128)(2,1)S(1)}, u32[]{:S(2)}) copy-start(bf16[4,128,128]{2,1,0:T(8,128)(2,1)S(1)} %collective-permute-done.7.refs_2_) | copy-start | bytes 393220
  143.3 0.7 copy-start.5
  146.2 10.7 %collective-permute-start.10 = (f32[256,128]{1,0:T(8,128)}, f32[256,128]{1,0:T(8,128)S(1)}, u32[]{:S(2)}, u32[]{:S(2)}) collective-permute-start(f32[256,128]{1,0:T(8,128)} %get-tuple-element.22), channel_id=1, source_target_pairs={{0,4},{1,5},{4,0},{5,1},{2,6},{3,7},{6,2},{7,3},{8,12},{9,13},{12,... | collective-permute-start | bytes 393224 | tf_op jit(solution)/shard_map/ppermute | solution.py:519
  148.4 8.5 %collective-permute-start.11 = (f32[256,128]{1,0:T(8,128)}, f32[256,128]{1,0:T(8,128)S(1)}, u32[]{:S(2)}, u32[]{:S(2)}) collective-permute-start(f32[256,128]{1,0:T(8,128)} %get-tuple-element.23), channel_id=1, source_target_pairs={{0,5},{1,4},{4,1},{5,0},{2,7},{3,6},{6,3},{7,2},{8,13},{9,12},{12,... | collective-permute-start | bytes 393224 | tf_op jit(solution)/shard_map/ppermute | solution.py:519
  151.5 7.3 %collective-permute-start.9 = (f32[256,128]{1,0:T(8,128)}, f32[256,128]{1,0:T(8,128)S(1)}, u32[]{:S(2)}, u32[]{:S(2)}) collective-permute-start(f32[256,128]{1,0:T(8,128)} %get-tuple-element.21), channel_id=1, source_target_pairs={{0,1},{1,0},{4,5},{5,4},{2,3},{3,2},{6,7},{7,6},{8,9},{9,8},{12,13... | collective-permute-start | bytes 393224 | tf_op jit(solution)/shard_map/ppermute | solution.py:519

commit v5 on v4

--- a/solution.py
+++ b/solution.py
@@ -45,37 +45,16 @@
     return square.T
 
 
-def dispatch(rows, gain, routes, weights, experts, slots, width):
+def dispatch(rows, gain, routes, experts, slots, width):
     tokens = rows.shape[0]
     pairs = experts // 2
-    tall_rows, columns = weights[0].shape
-
-    def kernel(rows_ref, gain_ref, routes_ref, *refs):
-        weight_refs, refs = refs[:3], refs[3:]
-        out_ref, target_ref, stacked_ref, held_ref, here_ref, sems = refs
-        rows_copy = pltpu.make_async_copy(rows_ref, here_ref, sems.at[6])
-        rows_copy.start()
-        arriving = [
-            pltpu.make_async_copy(ref, held_ref.at[i], sems.at[i])
-            for i, ref in enumerate(weight_refs)
-        ]
-        leaving = [
-            pltpu.make_async_copy(
-                held_ref.at[i], stacked_ref.at[pl.ds(i * tall_rows, tall_rows)], sems.at[3 + i]
-            )
-            for i in range(3)
-        ]
-        for copy in arriving:
-            copy.start()
+
+    def kernel(rows_ref, gain_ref, routes_ref, out_ref, target_ref):
         block = 2 * lax.axis_index("Y") + lax.axis_index("X")
-        rows_copy.wait()
-        for come, go in zip(arriving, leaving):
-            come.wait()
-            go.start()
-        values = here_ref[...].astype(jnp.float32)
+        values = rows_ref[...].astype(jnp.float32)
         scale = lax.rsqrt(jnp.mean(values * values, axis=-1, keepdims=True) + EPSILON)
         start = pl.multiple_of(block * width, width)
-        own = here_ref[:, pl.ds(start, width)].astype(jnp.float32)
+        own = rows_ref[:, pl.ds(start, width)].astype(jnp.float32)
         normed = (own * scale * gain_ref[:, pl.ds(start, width)]).astype(jnp.bfloat16)
         first = lax.broadcasted_iota(jnp.int32, (tokens, tokens), 0)
         second = lax.broadcasted_iota(jnp.int32, (tokens, tokens), 1)
@@ -103,27 +82,18 @@
         target_ref[...] = jnp.concatenate(
             [jnp.sum(mark * position, axis=1, keepdims=True) for mark in marks], axis=1
         ).astype(jnp.int32)
-        for copy in leaving:
-            copy.wait()
 
     vmem = pl.BlockSpec(memory_space=pltpu.VMEM)
-    anywhere = pl.BlockSpec(memory_space=pl.ANY)
     return pl.pallas_call(
         kernel,
         out_shape=(
             jax.ShapeDtypeStruct((experts * slots, width), jnp.bfloat16),
             jax.ShapeDtypeStruct((tokens, TOP_K), jnp.int32),
-            jax.ShapeDtypeStruct((3 * tall_rows, columns), jnp.bfloat16),
         ),
-        in_specs=[anywhere] + [vmem] * 2 + [anywhere] * 3,
-        out_specs=(vmem, vmem, anywhere),
-        scratch_shapes=[
-            pltpu.VMEM((3, tall_rows, columns), jnp.bfloat16),
-            pltpu.VMEM(rows.shape, rows.dtype),
-            pltpu.SemaphoreType.DMA((7,)),
-        ],
+        in_specs=[vmem] * 3,
+        out_specs=(vmem, vmem),
         name="dispatch",
-    )(rows, gain[None, :], routes.T, *weights)
+    )(rows, gain[None, :], routes.T)
 
 
 def device_pairs(where):
@@ -246,7 +216,7 @@
     )(rows, mixed, arrived, *shares)
 
 
-def lowered(hidden, shares, slots):
+def lowered(hidden, shares, landed, slots):
     parts, n, wide = hidden.shape
     f = shares[0].shape[1]
     k = 4 * f
@@ -254,7 +224,7 @@
     whole = parts * k
     half = k // 2
 
-    def kernel(hidden_ref, *refs):
+    def kernel(hidden_ref, _, *refs):
         shares, refs = refs[:5], refs[5:]
         out_ref, heads_ref, here_ref, weights_ref, sems, row_sems = refs
         native, order = share_order()
@@ -271,7 +241,7 @@
         for copy in arrivals:
             copy.start()
         for i in range(4):
-            copy_share(native, shares, i, 2 * whole, whole, *targets[i])
+            copy_share(native, shares, i, 0, whole, *targets[i])
         for copy in arrivals:
             copy.wait()
         heads.start()
@@ -296,7 +266,7 @@
             jax.ShapeDtypeStruct((n // slots, 4, slots, f), jnp.bfloat16),
             jax.ShapeDtypeStruct((parts, n, j), jnp.bfloat16),
         ),
-        in_specs=[anywhere] * 6,
+        in_specs=[anywhere] * 7,
         out_specs=(vmem, anywhere),
         scratch_shapes=[
             pltpu.VMEM((parts, n, wide), jnp.bfloat16),
@@ -305,7 +275,7 @@
             pltpu.SemaphoreType.DMA((parts + 1,)),
         ],
         name="lowered",
-    )(hidden, *shares)
+    )(hidden, landed, *shares)
 
 
 def selectors(target, logits, slots):
@@ -492,18 +462,18 @@
     rows_here, features = expert_input.shape
     slots = 2 * rows_here * TOP_K // experts // 4
     width = features // 4
-    weights = (gate_weight[0], up_weight[0], down_weight[0])
-    outgoing, target, own = dispatch(
-        expert_input, expert_gain, routes, weights, experts, slots, width
-    )
-    shares = gather_shares(own)
+    outgoing, target = dispatch(expert_input, expert_gain, routes, experts, slots, width)
+    both = jnp.concatenate([gate_weight[0], up_weight[0]], axis=0)
+    shares = gather_shares(both)
+    down_shares = gather_shares(down_weight[0])
     received = swap(outgoing.reshape(experts, slots, width), EP)
     mixed = attention(mixer_input, mixer_gain, query_weight, key_weight, value_weight, sink_logit)
     rows = spread(received.reshape(experts * slots, width), ("Y", "X"))
     arrived = shares[3][:8] + shares[4][:8]
     inner = gated(rows, mixed, shares, arrived)
     hidden = swap(inner, ("Y", "X"))
-    result, heads = lowered(hidden, shares, slots)
+    landed = down_shares[3][:8] + down_shares[4][:8]
+    result, heads = lowered(hidden, down_shares, landed, slots)
     returned = swap(result.reshape(4 * experts, slots, -1), (*EP, "h", "p"))
     around = [[(i, i ^ k) for i in range(4)] for k in range(4)]
     size = mixed.shape[1]

time: 164 us -> 158 us (0.963)
  the two profiles are of different devices: /device:TPU:1 before, /device:TPU:16 now
where the time goes in v5:
time: 158 us; the launch traced here: 157 us
  starting transfers between devices  82.6 us (52%)
  waiting for transfers between devices  38.7 us (24%)
  Pallas kernels  22.2 us (14%)
  other arithmetic  6.21 us (4%)
  local copies, waits for them, and re-layouts  5.16 us (3%)
    all_to_all x4, starting transfers between devices, swap(): return lax.all_to_all(pieces, axis, 0, 0, tiled=True)  39.6 us
    all_to_all x4, waiting for transfers between devices, swap(): return lax.all_to_all(pieces, axis, 0, 0, tiled=True)  23.3 us
    ppermute x3, starting transfers between devices, shards(): columns.append(lax.ppermute(piece, ('h', 'p'), around[k]) if k else piece)  9.2 us
    ppermute x3, starting transfers between devices, shards(): own_sum = own_sum + lax.ppermute(sums[k - 1], ('h', 'p'), around[k])  9.2 us
    ppermute x2, starting transfers between devices, gather_shares(): first = lax.ppermute(own, axes, device_pairs(outer))  6.39 us
    ppermute x2, starting transfers between devices, gather_shares(): third = lax.ppermute(first, axes, device_pairs(trade))  5.94 us
    ppermute x3, waiting for transfers between devices, shards(): columns.append(lax.ppermute(piece, ('h', 'p'), around[k]) if k else piece)  5.43 us
    ppermute x2, starting transfers between devices, gather_shares(): fourth = lax.ppermute(second, axes, device_pairs(give))  5.35 us
  transfers between devices with their start and end apart: 20, of which 8 were waited for; matrix products, arithmetic and copies ran while one was open for 4% of the time, Pallas kernels for 12%

profile of v5, /device:TPU:16, one launch (start us, length us, event | category | flops | bytes accessed | tf_op | source)
XLA Modules:
  0.0 157.3 jit_solution(11636970411599731375)
XLA Ops:
  0.6 1.3 pad_maximum_fusion.refs_0_
  1.9 3.2 %collective-permute-start.2 = (bf16[4096,128]{1,0:T(8,128)(2,1)S(1)}, bf16[4096,128]{1,0:T(8,128)(2,1)}, u32[]{:S(2)}, u32[]{:S(2)}) collective-permute-start(bf16[4096,128]{1,0:T(8,128)(2,1)S(1)} %pad_maximum_fusion.refs_0_), channel_id=1, source_target_pairs={{0,4},{1,16},{2,6},{3,18},{4,0},{5,20},{6,2},{7,22},{8,12},{9,24},... | collective-permute-start | bytes 3145736 | tf_op jit(solution)/shard_map/ppermute | solution.py:120
  5.1 2.2 %collective-permute-start.4 = (bf16[4096,128]{1,0:T(8,128)(2,1)S(1)}, bf16[4096,128]{1,0:T(8,128)(2,1)}, u32[]{:S(2)}, u32[]{:S(2)}) collective-permute-start(bf16[4096,128]{1,0:T(8,128)(2,1)S(1)} %pad_maximum_fusion.refs_0_), channel_id=1, source_target_pairs={{0,16},{1,4},{2,18},{3,6},{4,20},{5,0},{6,22},{7,2},{8,24},{9,12},... | collective-permute-start | bytes 3145736 | tf_op jit(solution)/shard_map/ppermute | solution.py:121
  7.4 2.5 %dispatch.1 = (bf16[256,512]{1,0:T(8,128)(2,1)}, s32[128,4]{1,0:T(8,128)}) custom-call(bf16[128,2048]{1,0:T(8,128)(2,1)} %rows_ref.2, f32[1,2048]{1,0:T(1,128)} %bitcast.41, s32[4,128]{1,0:T(4,128)} %bitcast.43), custom_call_target="tpu_custom_call" | custom-call | tf_op jit(solution)/shard_map/dispatch/pallas_call | solution.py:87
  9.9 15.7 %all-to-all-start = ((bf16[32,8,512]{2,1,0:T(8,128)(2,1)}), bf16[32,8,512]{2,1,0:T(8,128)(2,1)S(1)}, u32[]{:S(2)}, u32[]{:S(2)}) async-start(bf16[32,8,512]{2,1,0:T(8,128)(2,1)} %bitcast.37), calls=%async_computation | async-start | bytes 524288 | tf_op jit(solution)/shard_map/all_to_all | solution.py:25
  25.6 3.1 %collective-permute-done.2.refs_1_ = bf16[4096,128]{1,0:T(8,128)(2,1)} collective-permute-done((bf16[4096,128]{1,0:T(8,128)(2,1)S(1)}, bf16[4096,128]{1,0:T(8,128)(2,1)}, u32[]{:S(2)}, u32[]{:S(2)}) %collective-permute-start.2) | collective-permute-done | bytes 1048608 | tf_op jit(solution)/shard_map/ppermute | solution.py:120
  28.7 1.9 %collective-permute-start.3 = (bf16[4096,128]{1,0:T(8,128)(2,1)}, bf16[4096,128]{1,0:T(8,128)(2,1)S(1)}, u32[]{:S(2)}, u32[]{:S(2)}) collective-permute-start(bf16[4096,128]{1,0:T(8,128)(2,1)} %collective-permute-done.2.refs_1_), channel_id=1, source_target_pairs={{0,16},{1,17},{2,18},{3,19},{4,20},{5,21},{6,22},{7,23},{8,24},{9,... | collective-permute-start | bytes 3145736 | tf_op jit(solution)/shard_map/ppermute | solution.py:122
  30.6 3.4 %collective-permute-start.5 = (bf16[4096,128]{1,0:T(8,128)(2,1)}, bf16[4096,128]{1,0:T(8,128)(2,1)}, u32[]{:S(2)}, u32[]{:S(2)}) collective-permute-start(bf16[4096,128]{1,0:T(8,128)(2,1)} %collective-permute-done.4.refs_2_), channel_id=1, source_target_pairs={{0,16},{2,18},{4,20},{6,22},{8,24},{10,26},{12,28},{14,30},{17,1},... | collective-permute-start | bytes 3145736 | tf_op jit(solution)/shard_map/ppermute | solution.py:123
  34.0 14.3 %all-to-all-done = bf16[32,8,512]{2,1,0:T(8,128)(2,1)S(1)} async-done(((bf16[32,8,512]{2,1,0:T(8,128)(2,1)}), bf16[32,8,512]{2,1,0:T(8,128)(2,1)S(1)}, u32[]{:S(2)}, u32[]{:S(2)}) %all-to-all-start) | async-done | bytes 262176 | tf_op jit(solution)/shard_map/all_to_all | solution.py:25
  48.3 1.1 broadcast_in_dim.26
  49.3 7.0 %all-to-all-start.1 = ((bf16[4,256,512]{2,1,0:T(8,128)(2,1)}), bf16[4,256,512]{2,1,0:T(8,128)(2,1)S(1)}, u32[]{:S(2)}, u32[]{:S(2)}) async-start(bf16[4,256,512]{2,1,0:T(8,128)(2,1)} %broadcast_in_dim.26), calls=%async_computation.1 | async-start | bytes 2097152 | tf_op jit(solution)/shard_map/all_to_all | solution.py:25
  56.3 0.9 fusion.4
  57.2 3.5 %projections.1 = (bf16[256,128]{1,0:T(8,128)(2,1)}, bf16[128,128]{1,0:T(8,128)(2,1)}, bf16[128,128]{1,0:T(8,128)(2,1)}) custom-call(bf16[256,2048]{1,0:T(8,128)(2,1)} %rows_ref.3, f32[1,2048]{1,0:T(1,128)} %bitcast.42, bf16[2048,128]{1,0:T(8,128)(2,1)} %query_ref.1, bf16[64,2048]{1,0:T(8,128)(2,1)} %bitcast.34, bf16[64,2048]{1,0:T(8,128)(2,1)} %bitcast.35, ...), custom_call_target="tpu_custom_call" | custom-call | tf_op jit(solution)/shard_map/projections/pallas_call | solution.py:363
  60.7 1.3 collective-permute-start
  62.0 3.2 %collective-permute-start.6 = (bf16[2048,128]{1,0:T(8,128)(2,1)}, bf16[2048,128]{1,0:T(8,128)(2,1)}, u32[]{:S(2)}, u32[]{:S(2)}) collective-permute-start(bf16[2048,128]{1,0:T(8,128)(2,1)} %bitcast.9.refs_0_), channel_id=1, source_target_pairs={{0,4},{1,16},{2,6},{3,18},{4,0},{5,20},{6,2},{7,22},{8,12},{9,24},... | collective-permute-start | bytes 1572872 | tf_op jit(solution)/shard_map/ppermute | solution.py:120
  65.2 2.1 %collective-permute-start.8 = (bf16[2048,128]{1,0:T(8,128)(2,1)}, bf16[2048,128]{1,0:T(8,128)(2,1)}, u32[]{:S(2)}, u32[]{:S(2)}) collective-permute-start(bf16[2048,128]{1,0:T(8,128)(2,1)} %bitcast.9.refs_0_), channel_id=1, source_target_pairs={{0,16},{1,4},{2,18},{3,6},{4,20},{5,0},{6,22},{7,2},{8,24},{9,12},... | collective-permute-start | bytes 1572872 | tf_op jit(solution)/shard_map/ppermute | solution.py:121
  67.3 1.3 collective-permute-start.1
  68.6 3.1 %collective-permute-done.1.refs_3_ = bf16[128,128]{1,0:T(8,128)(2,1)S(1)} collective-permute-done((bf16[128,128]{1,0:T(8,128)(2,1)}, bf16[128,128]{1,0:T(8,128)(2,1)S(1)}, u32[]{:S(2)}, u32[]{:S(2)}) %collective-permute-start.1) | collective-permute-done | bytes 32800 | tf_op jit(solution)/shard_map/ppermute | solution.py:419
  71.7 0.6 copy-done.11
  72.3 3.2 %banded.1.mixed_ref = bf16[256,128]{1,0:T(8,128)(2,1)} custom-call(f32[2]{0:T(128)} %sink_ref.1, bf16[256,128]{1,0:T(8,128)(2,1)} %get-tuple-element.14.query_ref, bf16[128,128]{1,0:T(8,128)(2,1)} %copy-done.10, bf16[128,128]{1,0:T(8,128)(2,1)} %get-tuple-element.16.refs_1_, bf16[128,128]{1,0:T(8,128)(2,1)} %get-tuple-element.15.refs_2_, ...), custom_call_target="tpu_custom_call" | custom-call | tf_op jit(solution)/shard_map/banded/pallas_call | solution.py:406
  75.5 1.3 slice_add_fusion.2._
  76.8 1.0 copy-done.2
  77.8 5.0 %gated.1 = bf16[4,256,640]{2,1,0:T(8,128)(2,1)} custom-call(bf16[4,256,512]{2,1,0:T(8,128)(2,1)} %copy-done.2, bf16[256,128]{1,0:T(8,128)(2,1)} %banded.1.mixed_ref, bf16[8,128]{1,0:T(8,128)(2,1)} %slice_add_fusion.2._, bf16[4096,128]{1,0:T(8,128)(2,1)} %copy-done.1, bf16[4096,128]{1,0:T(8,128)(2,1)} %collective-permute-done.2.refs_1_, ...), custom_call_target="tpu_custom_call" | custom-call | tf_op jit(solution)/shard_map/gated/pallas_call | solution.py:202
  82.8 7.8 %all-to-all-start.2 = ((bf16[4,256,640]{2,1,0:T(8,128)(2,1)}), bf16[4,256,640]{2,1,0:T(8,128)(2,1)S(1)}, u32[]{:S(2)}, u32[]{:S(2)}) async-start(bf16[4,256,640]{2,1,0:T(8,128)(2,1)} %gated.1), calls=%async_computation.2 | async-start | bytes 2621440 | tf_op jit(solution)/shard_map/all_to_all | solution.py:25
  90.6 4.0 %collective-permute-start.7 = (bf16[2048,128]{1,0:T(8,128)(2,1)}, bf16[2048,128]{1,0:T(8,128)(2,1)S(1)}, u32[]{:S(2)}, u32[]{:S(2)}) collective-permute-start(bf16[2048,128]{1,0:T(8,128)(2,1)} %collective-permute-done.6.refs_1_), channel_id=1, source_target_pairs={{0,16},{1,17},{2,18},{3,19},{4,20},{5,21},{6,22},{7,23},{8,24},{9,... | collective-permute-start | bytes 1572872 | tf_op jit(solution)/shard_map/ppermute | solution.py:122
  94.6 1.9 %collective-permute-start.9 = (bf16[2048,128]{1,0:T(8,128)(2,1)}, bf16[2048,128]{1,0:T(8,128)(2,1)S(1)}, u32[]{:S(2)}, u32[]{:S(2)}) collective-permute-start(bf16[2048,128]{1,0:T(8,128)(2,1)} %collective-permute-done.8.refs_2_), channel_id=1, source_target_pairs={{0,16},{2,18},{4,20},{6,22},{8,24},{10,26},{12,28},{14,30},{17,1},... | collective-permute-start | bytes 1572872 | tf_op jit(solution)/shard_map/ppermute | solution.py:123
  96.6 1.7 %collective-permute-done.9.refs_4_ = bf16[2048,128]{1,0:T(8,128)(2,1)S(1)} collective-permute-done((bf16[2048,128]{1,0:T(8,128)(2,1)}, bf16[2048,128]{1,0:T(8,128)(2,1)S(1)}, u32[]{:S(2)}, u32[]{:S(2)}) %collective-permute-start.9) | collective-permute-done | bytes 524320 | tf_op jit(solution)/shard_map/ppermute | solution.py:123
  98.3 0.6 slice_add_fusion.1._
  98.9 9.0 %all-to-all-done.2.hidden_ref = bf16[4,256,640]{2,1,0:T(8,128)(2,1)S(1)} async-done(((bf16[4,256,640]{2,1,0:T(8,128)(2,1)}), bf16[4,256,640]{2,1,0:T(8,128)(2,1)S(1)}, u32[]{:S(2)}, u32[]{:S(2)}) %all-to-all-start.2) | async-done | bytes 1310752 | tf_op jit(solution)/shard_map/all_to_all | solution.py:25
  108.0 1.1 copy-done
  109.1 3.4 %lowered.1 = (bf16[32,4,8,128]{3,2,1,0:T(8,128)(2,1)}, bf16[4,256,128]{2,1,0:T(8,128)(2,1)}) custom-call(bf16[4,256,640]{2,1,0:T(8,128)(2,1)} %copy-done, bf16[8,128]{1,0:T(8,128)(2,1)} %slice_add_fusion.1._, bf16[2048,128]{1,0:T(8,128)(2,1)} %bitcast.9.refs_0_, bf16[2048,128]{1,0:T(8,128)(2,1)} %collective-permute-done.6.refs_1_, ...), custom_call_target="tpu_custom_call" | custom-call | tf_op jit(solution)/shard_map/lowered/pallas_call | solution.py:263
  112.5 9.1 %all-to-all-start.3 = ((bf16[128,8,128]{2,1,0:T(8,128)(2,1)}), bf16[128,8,128]{2,1,0:T(8,128)(2,1)S(1)}, u32[]{:S(2)}, u32[]{:S(2)}) async-start(bf16[128,8,128]{2,1,0:T(8,128)(2,1)} %bitcast.36), calls=%async_computation.3 | async-start | bytes 524288 | tf_op jit(solution)/shard_map/all_to_all | solution.py:25
  121.7 0.7 constant_dynamic-slice_fusion
  122.4 3.0 %collective-permute-start.10 = (bf16[4,128,128]{2,1,0:T(8,128)(2,1)S(1)}, bf16[4,128,128]{2,1,0:T(8,128)(2,1)S(1)}, u32[]{:S(2)}, u32[]{:S(2)}) collective-permute-start(bf16[4,128,128]{2,1,0:T(8,128)(2,1)S(1)} %bitcast.40), channel_id=1, source_target_pairs={{0,1},{1,0},{4,5},{5,4},{2,3},{3,2},{6,7},{7,6},{8,9},{9,8},{12,13... | collective-permute-start | bytes 393224 | tf_op jit(solution)/shard_map/ppermute | solution.py:486
  125.4 3.4 %collective-permute-start.11 = (bf16[4,128,128]{2,1,0:T(8,128)(2,1)S(1)}, bf16[4,128,128]{2,1,0:T(8,128)(2,1)S(1)}, u32[]{:S(2)}, u32[]{:S(2)}) collective-permute-start(bf16[4,128,128]{2,1,0:T(8,128)(2,1)S(1)} %bitcast.39), channel_id=1, source_target_pairs={{0,4},{1,5},{4,0},{5,1},{2,6},{3,7},{6,2},{7,3},{8,12},{9,13},{12,... | collective-permute-start | bytes 393224 | tf_op jit(solution)/shard_map/ppermute | solution.py:486
  128.8 2.8 %collective-permute-start.12 = (bf16[4,128,128]{2,1,0:T(8,128)(2,1)S(1)}, bf16[4,128,128]{2,1,0:T(8,128)(2,1)S(1)}, u32[]{:S(2)}, u32[]{:S(2)}) collective-permute-start(bf16[4,128,128]{2,1,0:T(8,128)(2,1)S(1)} %bitcast.38), channel_id=1, source_target_pairs={{0,5},{1,4},{4,1},{5,0},{2,7},{3,6},{6,3},{7,2},{8,13},{9,12},{12,... | collective-permute-start | bytes 393224 | tf_op jit(solution)/shard_map/ppermute | solution.py:486
  131.6 4.2 %collective-permute-done.11.refs_2_ = bf16[4,128,128]{2,1,0:T(8,128)(2,1)S(1)} collective-permute-done((bf16[4,128,128]{2,1,0:T(8,128)(2,1)S(1)}, bf16[4,128,128]{2,1,0:T(8,128)(2,1)S(1)}, u32[]{:S(2)}, u32[]{:S(2)}) %collective-permute-start.11) | collective-permute-done | bytes 131104 | tf_op jit(solution)/shard_map/ppermute | solution.py:486
  135.8 1.3 collective-permute-done.12.refs_3_
  137.0 0.6 copy-done.9
  137.7 2.3 %partial_sums.1 = (f32[256,128]{1,0:T(8,128)}, f32[256,128]{1,0:T(8,128)}, f32[256,128]{1,0:T(8,128)}, f32[256,128]{1,0:T(8,128)}) custom-call(bf16[4,256,128]{2,1,0:T(8,128)(2,1)} %get-tuple-element.17.heads_ref, bf16[4,128,128]{2,1,0:T(8,128)(2,1)} %bitcast.33, bf16[4,128,128]{2,1,0:T(8,128)(2,1)} %copy-done.7, bf16[4,128,128]{2,1,0:T(8,128)(2,1)} %copy-done.8, ...), custom_call_target="tpu_custom_call" | custom-call | tf_op jit(solution)/shard_map/partial_sums/pallas_call | solution.py:436
  140.0 2.6 %collective-permute-start.13 = (f32[256,128]{1,0:T(8,128)}, f32[256,128]{1,0:T(8,128)S(1)}, u32[]{:S(2)}, u32[]{:S(2)}) collective-permute-start(f32[256,128]{1,0:T(8,128)} %get-tuple-element.19), channel_id=1, source_target_pairs={{0,1},{1,0},{4,5},{5,4},{2,3},{3,2},{6,7},{7,6},{8,9},{9,8},{12,13... | collective-permute-start | bytes 393224 | tf_op jit(solution)/shard_map/ppermute | solution.py:489
  142.6 3.1 %collective-permute-start.14 = (f32[256,128]{1,0:T(8,128)}, f32[256,128]{1,0:T(8,128)S(1)}, u32[]{:S(2)}, u32[]{:S(2)}) collective-permute-start(f32[256,128]{1,0:T(8,128)} %get-tuple-element.20), channel_id=1, source_target_pairs={{0,4},{1,5},{4,0},{5,1},{2,6},{3,7},{6,2},{7,3},{8,12},{9,13},{12,... | collective-permute-start | bytes 393224 | tf_op jit(solution)/shard_map/ppermute | solution.py:489
  145.6 3.6 %collective-permute-start.15 = (f32[256,128]{1,0:T(8,128)}, f32[256,128]{1,0:T(8,128)S(1)}, u32[]{:S(2)}, u32[]{:S(2)}) collective-permute-start(f32[256,128]{1,0:T(8,128)} %get-tuple-element.21), channel_id=1, source_target_pairs={{0,5},{1,4},{4,1},{5,0},{2,7},{3,6},{6,3},{7,2},{8,13},{9,12},{12,... | collective-permute-start | bytes 393224 | tf_op jit(solution)/shard_map/ppermute | solution.py:489
  149.2 2.3 %selectors.1 = bf16[384,1024]{1,0:T(8,128)(2,1)} custom-call(s32[128,4]{1,0:T(8,128)} %get-tuple-element.22.target_ref, f32[4,128]{1,0:T(4,128)} %bitcast.44), custom_call_target="tpu_custom_call" | custom-call | tf_op jit(solution)/shard_map/selectors/pallas_call | solution.py:296
  151.5 2.1 %collective-permute-done.15 = f32[256,128]{1,0:T(8,128)S(1)} collective-permute-done((f32[256,128]{1,0:T(8,128)}, f32[256,128]{1,0:T(8,128)S(1)}, u32[]{:S(2)}, u32[]{:S(2)}) %collective-permute-start.15) | collective-permute-done | bytes 131104 | tf_op jit(solution)/shard_map/ppermute | solution.py:489
  153.6 1.6 add_convert_fusion
  155.2 1.5 fusion
  156.7 0.6 fusion.3
  (34 shorter events, 0.1 us)
Async XLA Ops:
  1.9 47.4 %copy-start.1 = (bf16[4096,128]{1,0:T(8,128)(2,1)}, bf16[4096,128]{1,0:T(8,128)(2,1)S(1)}, u32[]{:S(2)}) copy-start(bf16[4096,128]{1,0:T(8,128)(2,1)S(1)} %pad_maximum_fusion.refs_0_) | copy-start | bytes 3145732
  1.9 26.8 %collective-permute-start.2 = (bf16[4096,128]{1,0:T(8,128)(2,1)S(1)}, bf16[4096,128]{1,0:T(8,128)(2,1)}, u32[]{:S(2)}, u32[]{:S(2)}) collective-permute-start(bf16[4096,128]{1,0:T(8,128)(2,1)S(1)} %pad_maximum_fusion.refs_0_), channel_id=1, source_target_pairs={{0,4},{1,16},{2,6},{3,18},{4,0},{5,20},{6,2},{7,22},{8,12},{9,24},... | collective-permute-start | bytes 3145736 | tf_op jit(solution)/shard_map/ppermute | solution.py:120
  5.1 25.5 %collective-permute-start.4 = (bf16[4096,128]{1,0:T(8,128)(2,1)S(1)}, bf16[4096,128]{1,0:T(8,128)(2,1)}, u32[]{:S(2)}, u32[]{:S(2)}) collective-permute-start(bf16[4096,128]{1,0:T(8,128)(2,1)S(1)} %pad_maximum_fusion.refs_0_), channel_id=1, source_target_pairs={{0,16},{1,4},{2,18},{3,6},{4,20},{5,0},{6,22},{7,2},{8,24},{9,12},... | collective-permute-start | bytes 3145736 | tf_op jit(solution)/shard_map/ppermute | solution.py:121
  9.9 38.4 %all-to-all-start = ((bf16[32,8,512]{2,1,0:T(8,128)(2,1)}), bf16[32,8,512]{2,1,0:T(8,128)(2,1)S(1)}, u32[]{:S(2)}, u32[]{:S(2)}) async-start(bf16[32,8,512]{2,1,0:T(8,128)(2,1)} %bitcast.37), calls=%async_computation | async-start | bytes 524288 | tf_op jit(solution)/shard_map/all_to_all | solution.py:25
  28.7 46.8 %collective-permute-start.3 = (bf16[4096,128]{1,0:T(8,128)(2,1)}, bf16[4096,128]{1,0:T(8,128)(2,1)S(1)}, u32[]{:S(2)}, u32[]{:S(2)}) collective-permute-start(bf16[4096,128]{1,0:T(8,128)(2,1)} %collective-permute-done.2.refs_1_), channel_id=1, source_target_pairs={{0,16},{1,17},{2,18},{3,19},{4,20},{5,21},{6,22},{7,23},{8,24},{9,... | collective-permute-start | bytes 3145736 | tf_op jit(solution)/shard_map/ppermute | solution.py:122
  30.6 44.9 %collective-permute-start.5 = (bf16[4096,128]{1,0:T(8,128)(2,1)}, bf16[4096,128]{1,0:T(8,128)(2,1)}, u32[]{:S(2)}, u32[]{:S(2)}) collective-permute-start(bf16[4096,128]{1,0:T(8,128)(2,1)} %collective-permute-done.4.refs_2_), channel_id=1, source_target_pairs={{0,16},{2,18},{4,20},{6,22},{8,24},{10,26},{12,28},{14,30},{17,1},... | collective-permute-start | bytes 3145736 | tf_op jit(solution)/shard_map/ppermute | solution.py:123
  49.3 27.4 %all-to-all-start.1 = ((bf16[4,256,512]{2,1,0:T(8,128)(2,1)}), bf16[4,256,512]{2,1,0:T(8,128)(2,1)S(1)}, u32[]{:S(2)}, u32[]{:S(2)}) async-start(bf16[4,256,512]{2,1,0:T(8,128)(2,1)} %broadcast_in_dim.26), calls=%async_computation.1 | async-start | bytes 2097152 | tf_op jit(solution)/shard_map/all_to_all | solution.py:25
  60.7 6.6 %collective-permute-start = (bf16[128,128]{1,0:T(8,128)(2,1)}, bf16[128,128]{1,0:T(8,128)(2,1)S(1)}, u32[]{:S(2)}, u32[]{:S(2)}) collective-permute-start(bf16[128,128]{1,0:T(8,128)(2,1)} %get-tuple-element.15.refs_2_), channel_id=1, source_target_pairs={{0,16},{16,32},{32,48},{48,64},{64,80},{80,96},{96,112},{112,128},... | collective-permute-start | bytes 98312 | tf_op jit(solution)/shard_map/ppermute | solution.py:418
  62.0 28.6 %collective-permute-start.6 = (bf16[2048,128]{1,0:T(8,128)(2,1)}, bf16[2048,128]{1,0:T(8,128)(2,1)}, u32[]{:S(2)}, u32[]{:S(2)}) collective-permute-start(bf16[2048,128]{1,0:T(8,128)(2,1)} %bitcast.9.refs_0_), channel_id=1, source_target_pairs={{0,4},{1,16},{2,6},{3,18},{4,0},{5,20},{6,2},{7,22},{8,12},{9,24},... | collective-permute-start | bytes 1572872 | tf_op jit(solution)/shard_map/ppermute | solution.py:120
  65.2 29.4 %collective-permute-start.8 = (bf16[2048,128]{1,0:T(8,128)(2,1)}, bf16[2048,128]{1,0:T(8,128)(2,1)}, u32[]{:S(2)}, u32[]{:S(2)}) collective-permute-start(bf16[2048,128]{1,0:T(8,128)(2,1)} %bitcast.9.refs_0_), channel_id=1, source_target_pairs={{0,16},{1,4},{2,18},{3,6},{4,20},{5,0},{6,22},{7,2},{8,24},{9,12},... | collective-permute-start | bytes 1572872 | tf_op jit(solution)/shard_map/ppermute | solution.py:121
  67.3 4.4 %copy-start.10 = (bf16[128,128]{1,0:T(8,128)(2,1)}, bf16[128,128]{1,0:T(8,128)(2,1)S(1)}, u32[]{:S(2)}) copy-start(bf16[128,128]{1,0:T(8,128)(2,1)S(1)} %collective-permute-done.refs_0_) | copy-start | bytes 98308
  67.3 4.4 %collective-permute-start.1 = (bf16[128,128]{1,0:T(8,128)(2,1)}, bf16[128,128]{1,0:T(8,128)(2,1)S(1)}, u32[]{:S(2)}, u32[]{:S(2)}) collective-permute-start(bf16[128,128]{1,0:T(8,128)(2,1)} %get-tuple-element.16.refs_1_), channel_id=1, source_target_pairs={{16,0},{32,16},{48,32},{64,48},{80,64},{96,80},{112,96},{128,112},... | collective-permute-start | bytes 98312 | tf_op jit(solution)/shard_map/ppermute | solution.py:419
  71.7 0.6 copy-start.11
  75.5 1.3 copy-start.3
  76.8 1.0 copy-start.2
  82.8 25.2 %all-to-all-start.2 = ((bf16[4,256,640]{2,1,0:T(8,128)(2,1)}), bf16[4,256,640]{2,1,0:T(8,128)(2,1)S(1)}, u32[]{:S(2)}, u32[]{:S(2)}) async-start(bf16[4,256,640]{2,1,0:T(8,128)(2,1)} %gated.1), calls=%async_computation.2 | async-start | bytes 2621440 | tf_op jit(solution)/shard_map/all_to_all | solution.py:25
  90.6 6.0 %collective-permute-start.7 = (bf16[2048,128]{1,0:T(8,128)(2,1)}, bf16[2048,128]{1,0:T(8,128)(2,1)S(1)}, u32[]{:S(2)}, u32[]{:S(2)}) collective-permute-start(bf16[2048,128]{1,0:T(8,128)(2,1)} %collective-permute-done.6.refs_1_), channel_id=1, source_target_pairs={{0,16},{1,17},{2,18},{3,19},{4,20},{5,21},{6,22},{7,23},{8,24},{9,... | collective-permute-start | bytes 1572872 | tf_op jit(solution)/shard_map/ppermute | solution.py:122
  94.6 3.7 %collective-permute-start.9 = (bf16[2048,128]{1,0:T(8,128)(2,1)}, bf16[2048,128]{1,0:T(8,128)(2,1)S(1)}, u32[]{:S(2)}, u32[]{:S(2)}) collective-permute-start(bf16[2048,128]{1,0:T(8,128)(2,1)} %collective-permute-done.8.refs_2_), channel_id=1, source_target_pairs={{0,16},{2,18},{4,20},{6,22},{8,24},{10,26},{12,28},{14,30},{17,1},... | collective-permute-start | bytes 1572872 | tf_op jit(solution)/shard_map/ppermute | solution.py:123
  96.6 11.3 %copy-start.4 = (bf16[2048,128]{1,0:T(8,128)(2,1)}, bf16[2048,128]{1,0:T(8,128)(2,1)S(1)}, u32[]{:S(2)}) copy-start(bf16[2048,128]{1,0:T(8,128)(2,1)S(1)} %collective-permute-done.7.refs_3_) | copy-start | bytes 1572868
  98.3 9.7 %copy-start.5 = (bf16[2048,128]{1,0:T(8,128)(2,1)}, bf16[2048,128]{1,0:T(8,128)(2,1)S(1)}, u32[]{:S(2)}) copy-start(bf16[2048,128]{1,0:T(8,128)(2,1)S(1)} %collective-permute-done.9.refs_4_) | copy-start | bytes 1572868
  98.9 22.7 %copy-start.6 = (bf16[2048,128]{1,0:T(8,128)(2,1)S(1)}, bf16[2048,128]{1,0:T(8,128)(2,1)}, u32[]{:S(2)}) copy-start(bf16[2048,128]{1,0:T(8,128)(2,1)} %param.19) | copy-start | bytes 1572868
  108.0 1.1 copy-start
  112.5 42.7 %all-to-all-start.3 = ((bf16[128,8,128]{2,1,0:T(8,128)(2,1)}), bf16[128,8,128]{2,1,0:T(8,128)(2,1)S(1)}, u32[]{:S(2)}, u32[]{:S(2)}) async-start(bf16[128,8,128]{2,1,0:T(8,128)(2,1)} %bitcast.36), calls=%async_computation.3 | async-start | bytes 524288 | tf_op jit(solution)/shard_map/all_to_all | solution.py:25
  122.4 9.2 %collective-permute-start.10 = (bf16[4,128,128]{2,1,0:T(8,128)(2,1)S(1)}, bf16[4,128,128]{2,1,0:T(8,128)(2,1)S(1)}, u32[]{:S(2)}, u32[]{:S(2)}) collective-permute-start(bf16[4,128,128]{2,1,0:T(8,128)(2,1)S(1)} %bitcast.40), channel_id=1, source_target_pairs={{0,1},{1,0},{4,5},{5,4},{2,3},{3,2},{6,7},{7,6},{8,9},{9,8},{12,13... | collective-permute-start | bytes 393224 | tf_op jit(solution)/shard_map/ppermute | solution.py:486
  125.4 10.4 %collective-permute-start.11 = (bf16[4,128,128]{2,1,0:T(8,128)(2,1)S(1)}, bf16[4,128,128]{2,1,0:T(8,128)(2,1)S(1)}, u32[]{:S(2)}, u32[]{:S(2)}) collective-permute-start(bf16[4,128,128]{2,1,0:T(8,128)(2,1)S(1)} %bitcast.39), channel_id=1, source_target_pairs={{0,4},{1,5},{4,0},{5,1},{2,6},{3,7},{6,2},{7,3},{8,12},{9,13},{12,... | collective-permute-start | bytes 393224 | tf_op jit(solution)/shard_map/ppermute | solution.py:486
  128.8 8.3 %collective-permute-start.12 = (bf16[4,128,128]{2,1,0:T(8,128)(2,1)S(1)}, bf16[4,128,128]{2,1,0:T(8,128)(2,1)S(1)}, u32[]{:S(2)}, u32[]{:S(2)}) collective-permute-start(bf16[4,128,128]{2,1,0:T(8,128)(2,1)S(1)} %bitcast.38), channel_id=1, source_target_pairs={{0,5},{1,4},{4,1},{5,0},{2,7},{3,6},{6,3},{7,2},{8,13},{9,12},{12,... | collective-permute-start | bytes 393224 | tf_op jit(solution)/shard_map/ppermute | solution.py:486
  131.6 5.4 %copy-start.7 = (bf16[4,128,128]{2,1,0:T(8,128)(2,1)}, bf16[4,128,128]{2,1,0:T(8,128)(2,1)S(1)}, u32[]{:S(2)}) copy-start(bf16[4,128,128]{2,1,0:T(8,128)(2,1)S(1)} %collective-permute-done.10.refs_1_) | copy-start | bytes 393220
  135.8 1.3 copy-start.8
  137.0 0.7 copy-start.9
  140.0 11.5 %collective-permute-start.13 = (f32[256,128]{1,0:T(8,128)}, f32[256,128]{1,0:T(8,128)S(1)}, u32[]{:S(2)}, u32[]{:S(2)}) collective-permute-start(f32[256,128]{1,0:T(8,128)} %get-tuple-element.19), channel_id=1, source_target_pairs={{0,1},{1,0},{4,5},{5,4},{2,3},{3,2},{6,7},{7,6},{8,9},{9,8},{12,13... | collective-permute-start | bytes 393224 | tf_op jit(solution)/shard_map/ppermute | solution.py:489
  142.6 9.0 %collective-permute-start.14 = (f32[256,128]{1,0:T(8,128)}, f32[256,128]{1,0:T(8,128)S(1)}, u32[]{:S(2)}, u32[]{:S(2)}) collective-permute-start(f32[256,128]{1,0:T(8,128)} %get-tuple-element.20), channel_id=1, source_target_pairs={{0,4},{1,5},{4,0},{5,1},{2,6},{3,7},{6,2},{7,3},{8,12},{9,13},{12,... | collective-permute-start | bytes 393224 | tf_op jit(solution)/shard_map/ppermute | solution.py:489
  145.6 8.0 %collective-permute-start.15 = (f32[256,128]{1,0:T(8,128)}, f32[256,128]{1,0:T(8,128)S(1)}, u32[]{:S(2)}, u32[]{:S(2)}) collective-permute-start(f32[256,128]{1,0:T(8,128)} %get-tuple-element.21), channel_id=1, source_target_pairs={{0,5},{1,4},{4,1},{5,0},{2,7},{3,6},{6,3},{7,2},{8,13},{9,12},{12,... | collective-permute-start | bytes 393224 | tf_op jit(solution)/shard_map/ppermute | solution.py:489

commit v6 on v4

--- a/solution.py
+++ b/solution.py
@@ -13,7 +13,7 @@
 WINDOW = 128
 GRID_W = 64
 EP = ("ep_0", "ep_1")
-TP = ("Y", "h", "X", "p")
+TP = ("h", "Y", "p", "X")
 
 EPSILON = 1e-06
 LIMIT = 7.0
@@ -133,19 +133,19 @@
 
 
 def gather_shares(own):
-    axes = ("ep_1", "Y", "h", "X", "p")
-
-    def outer(c, Y, h, X, p):
-        return (c, Y, 1 - h, X, p) if c == p else (1 - c, Y, h, X, 1 - p)
-
-    def cross(c, Y, h, X, p):
-        return (1 - c, Y, h, X, p) if c == p else (c, Y, 1 - h, X, 1 - p)
-
-    def trade(c, Y, h, X, p):
-        return (1 - c, Y, h, X, p)
-
-    def give(c, Y, h, X, p):
-        return (1 - c, Y, h, X, p) if c == p else None
+    axes = ("ep_1", "h", "Y", "p", "X")
+
+    def outer(c, h, Y, p, X):
+        return (c, 1 - h, Y, p, X) if c == p else (1 - c, h, Y, 1 - p, X)
+
+    def cross(c, h, Y, p, X):
+        return (1 - c, h, Y, p, X) if c == p else (c, 1 - h, Y, 1 - p, X)
+
+    def trade(c, h, Y, p, X):
+        return (1 - c, h, Y, p, X)
+
+    def give(c, h, Y, p, X):
+        return (1 - c, h, Y, p, X) if c == p else None
 
     first = lax.ppermute(own, axes, device_pairs(outer))
     second = lax.ppermute(own, axes, device_pairs(cross))
@@ -280,9 +280,10 @@
         for pair in range(2):
             total = jnp.zeros((n, 2 * f), jnp.float32)
             for Y, X, h in itertools.product(range(2), repeat=3):
-                unit = (8 * Y + 4 * h + 2 * X) * f
+                units = [(8 * h + 4 * Y + 2 * p + X) * f for p in range(2)]
+                below = [weights_ref[pair, unit : unit + f, :] for unit in units]
                 piece = here_ref[2 * Y + X, :, h * half : (h + 1) * half]
-                total = total + dot(piece, weights_ref[pair, unit : unit + half, :])
+                total = total + dot(piece, jnp.concatenate(below, axis=0))
             rounded = total.astype(jnp.bfloat16).reshape(n // slots, slots, 2 * f)
             out_ref[:, order[2 * pair]] = rounded[:, :, :f]
             out_ref[:, order[2 * pair + 1]] = rounded[:, :, f:]
@@ -511,8 +512,8 @@
     columns = []
     for k in range(4):
         h, p = lax.axis_index("h") ^ (k // 2), lax.axis_index("p") ^ (k % 2)
-        piece = lax.dynamic_slice_in_dim(blocks, h, 1, 1)
-        piece = lax.dynamic_slice_in_dim(piece, p, 1, 3).reshape(4, size, -1)
+        piece = lax.dynamic_slice_in_dim(blocks, h, 1, 0)
+        piece = lax.dynamic_slice_in_dim(piece, p, 1, 2).reshape(4, size, -1)
         columns.append(lax.ppermute(piece, ("h", "p"), around[k]) if k else piece)
     own_sum, *sums = partial_sums(heads, columns)
     for k in range(1, 4):
@@ -526,7 +527,7 @@
 
 
 def solution(mesh):
-    names = ("ep_0", "ep_1", "Y", "h", "X", "p")
+    names = ("ep_0", "ep_1", "h", "Y", "p", "X")
     finer = Mesh(mesh.devices.reshape(16, 2, 2, 2, 2, 2), names)
     in_specs = (
         P(EP, None),

time: 164 us -> 169 us (1.030)
  starting transfers between devices: 91.3 us -> 100 us
  blocking collectives: 26 us -> 20.1 us
  waiting for transfers between devices: 11.4 us -> 13.3 us
    all_to_all x1, blocking collectives: 26 us -> 20.1 us  [swap(): return lax.all_to_all(pieces, axis, 0, 0, tiled=True)]
    ppermute x3, starting transfers between devices: 8.36 us -> 11.4 us  [shards(): columns.append(lax.ppermute(piece, ('h', 'p'), around[k]) if k else piece)]
    ppermute x3, starting transfers between devices: 8.36 us -> 11.4 us  [shards(): own_sum = own_sum + lax.ppermute(sums[k - 1], ('h', 'p'), around[k])]
    ppermute x3, waiting for transfers between devices: 5.45 us -> 8.31 us  [shards(): columns.append(lax.ppermute(piece, ('h', 'p'), around[k]) if k else piece)]
  transfers between devices with their start and end apart: 15 -> 15, of which waited for: 5 -> 4; matrix products, arithmetic and copies ran while one was open for 3% -> 3% of each run, Pallas kernels for 7% -> 7%
where the time goes in v6:
time: 169 us; the launch traced here: 167 us
  starting transfers between devices  100 us (59%)
  Pallas kernels  23.6 us (14%)
  blocking collectives  20.1 us (12%)
  waiting for transfers between devices  13.3 us (8%)
  local copies, waits for them, and re-layouts  4.04 us (2%)
  other arithmetic  3.69 us (2%)
    all_to_all x3, starting transfers between devices, swap(): return lax.all_to_all(pieces, axis, 0, 0, tiled=True)  37.4 us
    ppermute x1, starting transfers between devices, gather_shares(): third = lax.ppermute(first, axes, device_pairs(trade))  24.2 us
    all_to_all x1, blocking collectives, swap(): return lax.all_to_all(pieces, axis, 0, 0, tiled=True)  20.1 us
    ppermute x3, starting transfers between devices, shards(): columns.append(lax.ppermute(piece, ('h', 'p'), around[k]) if k else piece)  11.4 us
    ppermute x3, starting transfers between devices, shards(): own_sum = own_sum + lax.ppermute(sums[k - 1], ('h', 'p'), around[k])  11.4 us
    ppermute x3, waiting for transfers between devices, shards(): columns.append(lax.ppermute(piece, ('h', 'p'), around[k]) if k else piece)  8.31 us
    ppermute x1, starting transfers between devices, gather_shares(): first = lax.ppermute(own, axes, device_pairs(outer))  6.03 us
    pallas_call x1, Pallas kernels, gated(): pl.pallas_call(kernel, out_shape=jax.ShapeDtypeStruct((parts, n, 4 * u +...  5 us
  transfers between devices with their start and end apart: 15, of which 4 were waited for; matrix products, arithmetic and copies ran while one was open for 3% of the time, Pallas kernels for 7%

profile of v6, /device:TPU:1, one launch (start us, length us, event | category | flops | bytes accessed | tf_op | source)
XLA Modules:
  0.0 167.3 jit_solution(5553890557463780588)
XLA Ops:
  0.6 3.9 %dispatch.1 = (bf16[256,512]{1,0:T(8,128)(2,1)}, s32[128,4]{1,0:T(8,128)}, bf16[6144,128]{1,0:T(8,128)(2,1)}) custom-call(bf16[128,2048]{1,0:T(8,128)(2,1)} %rows_ref.2, f32[1,2048]{1,0:T(1,128)} %bitcast.42, s32[4,128]{1,0:T(4,128)} %bitcast.44, bf16[2048,128]{1,0:T(8,128)(2,1)} %bitcast.30, bf16[2048,128]{1,0:T(8,128)(2,1)} %bitcast.31, ...), custom_call_target="tpu_custom_call" | custom-call | tf_op jit(solution)/shard_map/dispatch/pallas_call | solution.py:111
  4.5 6.0 %collective-permute-start.2 = (bf16[6144,128]{1,0:T(8,128)(2,1)}, bf16[6144,128]{1,0:T(8,128)(2,1)}, u32[]{:S(2)}, u32[]{:S(2)}) collective-permute-start(bf16[6144,128]{1,0:T(8,128)(2,1)} %get-tuple-element.18.refs_0_), channel_id=1, source_target_pairs={{0,8},{1,9},{2,16},{3,17},{4,12},{5,13},{6,20},{7,21},{8,0},{9,1},... | collective-permute-start | bytes 4718600 | tf_op jit(solution)/shard_map/ppermute | solution.py:150
  10.6 4.0 %collective-permute-start.4 = (bf16[6144,128]{1,0:T(8,128)(2,1)}, bf16[6144,128]{1,0:T(8,128)(2,1)}, u32[]{:S(2)}, u32[]{:S(2)}) collective-permute-start(bf16[6144,128]{1,0:T(8,128)(2,1)} %get-tuple-element.18.refs_0_), channel_id=1, source_target_pairs={{0,16},{1,17},{2,8},{3,9},{4,20},{5,21},{6,12},{7,13},{8,24},{9,25... | collective-permute-start | bytes 4718600 | tf_op jit(solution)/shard_map/ppermute | solution.py:151
  14.6 15.4 %all-to-all-start = ((bf16[32,8,512]{2,1,0:T(8,128)(2,1)}), bf16[32,8,512]{2,1,0:T(8,128)(2,1)S(1)}, u32[]{:S(2)}, u32[]{:S(2)}) async-start(bf16[32,8,512]{2,1,0:T(8,128)(2,1)} %bitcast.38), calls=%async_computation | async-start | bytes 524288 | tf_op jit(solution)/shard_map/all_to_all | solution.py:25
  30.0 0.0 collective-permute-done.2.refs_1_
  30.0 24.2 %collective-permute-start.3 = (bf16[6144,128]{1,0:T(8,128)(2,1)}, bf16[6144,128]{1,0:T(8,128)(2,1)S(1)}, u32[]{:S(2)}, u32[]{:S(2)}) collective-permute-start(bf16[6144,128]{1,0:T(8,128)(2,1)} %collective-permute-done.2.refs_1_), channel_id=1, source_target_pairs={{0,16},{1,17},{2,18},{3,19},{4,20},{5,21},{6,22},{7,23},{8,24},{9,... | collective-permute-start | bytes 4718600 | tf_op jit(solution)/shard_map/ppermute | solution.py:152
  54.2 0.0 collective-permute-done.4.refs_2_
  54.3 1.3 collective-permute-start.5
  55.6 0.0 all-to-all-done
  55.6 1.1 broadcast_in_dim.26
  56.6 4.3 %all-to-all-start.1 = ((bf16[4,256,512]{2,1,0:T(8,128)(2,1)}), bf16[4,256,512]{2,1,0:T(8,128)(2,1)}, u32[]{:S(2)}, u32[]{:S(2)}) async-start(bf16[4,256,512]{2,1,0:T(8,128)(2,1)} %broadcast_in_dim.26), calls=%async_computation.1 | async-start | bytes 2097152 | tf_op jit(solution)/shard_map/all_to_all | solution.py:25
  60.9 0.9 fusion.4
  61.8 3.5 %projections.1 = (bf16[256,128]{1,0:T(8,128)(2,1)}, bf16[128,128]{1,0:T(8,128)(2,1)}, bf16[128,128]{1,0:T(8,128)(2,1)}) custom-call(bf16[256,2048]{1,0:T(8,128)(2,1)} %rows_ref.3, f32[1,2048]{1,0:T(1,128)} %bitcast.43, bf16[2048,128]{1,0:T(8,128)(2,1)} %query_ref.1, bf16[64,2048]{1,0:T(8,128)(2,1)} %bitcast.35, bf16[64,2048]{1,0:T(8,128)(2,1)} %bitcast.36, ...), custom_call_target="tpu_custom_call" | custom-call | tf_op jit(solution)/shard_map/projections/pallas_call | solution.py:394
  65.3 1.9 %collective-permute-start = (bf16[128,128]{1,0:T(8,128)(2,1)}, bf16[128,128]{1,0:T(8,128)(2,1)S(1)}, u32[]{:S(2)}, u32[]{:S(2)}) collective-permute-start(bf16[128,128]{1,0:T(8,128)(2,1)} %get-tuple-element.16.refs_2_), channel_id=1, source_target_pairs={{0,16},{16,32},{32,48},{48,64},{64,80},{80,96},{96,112},{112,128},... | collective-permute-start | bytes 98312 | tf_op jit(solution)/shard_map/ppermute | solution.py:449
  67.2 2.5 %collective-permute-start.1 = (bf16[128,128]{1,0:T(8,128)(2,1)}, bf16[128,128]{1,0:T(8,128)(2,1)S(1)}, u32[]{:S(2)}, u32[]{:S(2)}) collective-permute-start(bf16[128,128]{1,0:T(8,128)(2,1)} %get-tuple-element.17.refs_1_), channel_id=1, source_target_pairs={{16,0},{32,16},{48,32},{64,48},{80,64},{96,80},{112,96},{128,112},... | collective-permute-start | bytes 98312 | tf_op jit(solution)/shard_map/ppermute | solution.py:450
  69.7 0.0 collective-permute-done.refs_0_
  69.7 3.3 %collective-permute-done.1.refs_3_ = bf16[128,128]{1,0:T(8,128)(2,1)S(1)} collective-permute-done((bf16[128,128]{1,0:T(8,128)(2,1)}, bf16[128,128]{1,0:T(8,128)(2,1)S(1)}, u32[]{:S(2)}, u32[]{:S(2)}) %collective-permute-start.1) | collective-permute-done | bytes 32800 | tf_op jit(solution)/shard_map/ppermute | solution.py:450
  73.1 0.6 copy-done.7
  73.7 3.2 %banded.1.mixed_ref = bf16[256,128]{1,0:T(8,128)(2,1)} custom-call(f32[2]{0:T(128)} %sink_ref.1, bf16[256,128]{1,0:T(8,128)(2,1)} %get-tuple-element.15.query_ref, bf16[128,128]{1,0:T(8,128)(2,1)} %copy-done.6, bf16[128,128]{1,0:T(8,128)(2,1)} %get-tuple-element.17.refs_1_, bf16[128,128]{1,0:T(8,128)(2,1)} %get-tuple-element.16.refs_2_, ...), custom_call_target="tpu_custom_call" | custom-call | tf_op jit(solution)/shard_map/banded/pallas_call | solution.py:437
  76.8 0.0 collective-permute-done.3.refs_3_
  76.8 0.0 collective-permute-done.5.refs_4_
  76.9 0.6 slice_add_fusion.1._
  77.5 0.0 all-to-all-done.1.rows_ref
  77.5 0.5 copy-done
  78.0 0.5 copy-done.1
  78.5 5.0 %gated.1 = bf16[4,256,640]{2,1,0:T(8,128)(2,1)} custom-call(bf16[4,256,512]{2,1,0:T(8,128)(2,1)} %all-to-all-done.1.rows_ref, bf16[256,128]{1,0:T(8,128)(2,1)} %banded.1.mixed_ref, bf16[8,128]{1,0:T(8,128)(2,1)} %slice_add_fusion.1._, bf16[6144,128]{1,0:T(8,128)(2,1)} %get-tuple-element.18.refs_0_, bf16[6144,128]{1,0:T(8,128)(2,1)} %collective-permute-done.2.refs_1_, ...), custom_call_target="tpu_custom_call" | custom-call | tf_op jit(solution)/shard_map/gated/pallas_call | solution.py:232
  83.5 20.1 %all_to_all.20.hidden_ref = bf16[4,256,640]{2,1,0:T(8,128)(2,1)} all-to-all(bf16[4,256,640]{2,1,0:T(8,128)(2,1)} %gated.1), channel_id=1, replica_groups=mesh['ep_0'=16,'ep_1'=2,'h'=2,'Y'=2,'p'=2,'X'=2] {'Y','X'}, dimensions={0} | all-to-all | bytes 2621440 | tf_op jit(solution)/shard_map/all_to_all | solution.py:25
  103.6 3.5 %lowered.1 = (bf16[32,4,8,128]{3,2,1,0:T(8,128)(2,1)}, bf16[4,256,128]{2,1,0:T(8,128)(2,1)}) custom-call(bf16[4,256,640]{2,1,0:T(8,128)(2,1)} %all_to_all.20.hidden_ref, bf16[6144,128]{1,0:T(8,128)(2,1)} %get-tuple-element.18.refs_0_, bf16[6144,128]{1,0:T(8,128)(2,1)} %collective-permute-done.2.refs_1_, bf16[6144,128]{1,0:T(8,128)(2,1)} %collective-permute-done.4.refs_2_, ...), custom_call_target="tpu_custom_call" | custom-call | tf_op jit(solution)/shard_map/lowered/pallas_call | solution.py:294
  107.1 17.7 %all-to-all-start.3 = ((bf16[128,8,128]{2,1,0:T(8,128)(2,1)}), bf16[128,8,128]{2,1,0:T(8,128)(2,1)S(1)}, u32[]{:S(2)}, u32[]{:S(2)}) async-start(bf16[128,8,128]{2,1,0:T(8,128)(2,1)} %bitcast.37), calls=%async_computation.3 | async-start | bytes 524288 | tf_op jit(solution)/shard_map/all_to_all | solution.py:25
  124.9 0.7 constant_dynamic-slice_fusion
  125.6 4.8 %collective-permute-start.6 = (bf16[4,128,128]{2,1,0:T(8,128)(2,1)S(1)}, bf16[4,128,128]{2,1,0:T(8,128)(2,1)S(1)}, u32[]{:S(2)}, u32[]{:S(2)}) collective-permute-start(bf16[4,128,128]{2,1,0:T(8,128)(2,1)S(1)} %bitcast.41), channel_id=1, source_target_pairs={{0,2},{2,0},{8,10},{10,8},{1,3},{3,1},{9,11},{11,9},{4,6},{6,4},{1... | collective-permute-start | bytes 393224 | tf_op jit(solution)/shard_map/ppermute | solution.py:517
  130.3 4.6 %collective-permute-start.7 = (bf16[4,128,128]{2,1,0:T(8,128)(2,1)S(1)}, bf16[4,128,128]{2,1,0:T(8,128)(2,1)S(1)}, u32[]{:S(2)}, u32[]{:S(2)}) collective-permute-start(bf16[4,128,128]{2,1,0:T(8,128)(2,1)S(1)} %bitcast.40), channel_id=1, source_target_pairs={{0,8},{2,10},{8,0},{10,2},{1,9},{3,11},{9,1},{11,3},{4,12},{6,14},... | collective-permute-start | bytes 393224 | tf_op jit(solution)/shard_map/ppermute | solution.py:517
  134.9 2.0 %collective-permute-start.8 = (bf16[4,128,128]{2,1,0:T(8,128)(2,1)S(1)}, bf16[4,128,128]{2,1,0:T(8,128)(2,1)S(1)}, u32[]{:S(2)}, u32[]{:S(2)}) collective-permute-start(bf16[4,128,128]{2,1,0:T(8,128)(2,1)S(1)} %bitcast.39), channel_id=1, source_target_pairs={{0,10},{2,8},{8,2},{10,0},{1,11},{3,9},{9,3},{11,1},{4,14},{6,12},... | collective-permute-start | bytes 393224 | tf_op jit(solution)/shard_map/ppermute | solution.py:517
  137.0 0.0 collective-permute-done.6.refs_1_
  137.0 2.0 %collective-permute-done.7.refs_2_ = bf16[4,128,128]{2,1,0:T(8,128)(2,1)S(1)} collective-permute-done((bf16[4,128,128]{2,1,0:T(8,128)(2,1)S(1)}, bf16[4,128,128]{2,1,0:T(8,128)(2,1)S(1)}, u32[]{:S(2)}, u32[]{:S(2)}) %collective-permute-start.7) | collective-permute-done | bytes 131104 | tf_op jit(solution)/shard_map/ppermute | solution.py:517
  139.0 6.3 %collective-permute-done.8.refs_3_ = bf16[4,128,128]{2,1,0:T(8,128)(2,1)S(1)} collective-permute-done((bf16[4,128,128]{2,1,0:T(8,128)(2,1)S(1)}, bf16[4,128,128]{2,1,0:T(8,128)(2,1)S(1)}, u32[]{:S(2)}, u32[]{:S(2)}) %collective-permute-start.8) | collective-permute-done | bytes 131104 | tf_op jit(solution)/shard_map/ppermute | solution.py:517
  145.3 0.7 copy-done.5
  146.0 2.3 %partial_sums.1 = (f32[256,128]{1,0:T(8,128)}, f32[256,128]{1,0:T(8,128)}, f32[256,128]{1,0:T(8,128)}, f32[256,128]{1,0:T(8,128)}) custom-call(bf16[4,256,128]{2,1,0:T(8,128)(2,1)} %get-tuple-element.19.heads_ref, bf16[4,128,128]{2,1,0:T(8,128)(2,1)} %bitcast.34, bf16[4,128,128]{2,1,0:T(8,128)(2,1)} %copy-done.3, bf16[4,128,128]{2,1,0:T(8,128)(2,1)} %copy-done.4, ...), custom_call_target="tpu_custom_call" | custom-call | tf_op jit(solution)/shard_map/partial_sums/pallas_call | solution.py:467
  148.2 2.1 %collective-permute-start.10 = (f32[256,128]{1,0:T(8,128)}, f32[256,128]{1,0:T(8,128)S(1)}, u32[]{:S(2)}, u32[]{:S(2)}) collective-permute-start(f32[256,128]{1,0:T(8,128)} %get-tuple-element.22), channel_id=1, source_target_pairs={{0,8},{2,10},{8,0},{10,2},{1,9},{3,11},{9,1},{11,3},{4,12},{6,14},... | collective-permute-start | bytes 393224 | tf_op jit(solution)/shard_map/ppermute | solution.py:520
  150.3 4.6 %collective-permute-start.11 = (f32[256,128]{1,0:T(8,128)}, f32[256,128]{1,0:T(8,128)S(1)}, u32[]{:S(2)}, u32[]{:S(2)}) collective-permute-start(f32[256,128]{1,0:T(8,128)} %get-tuple-element.23), channel_id=1, source_target_pairs={{0,10},{2,8},{8,2},{10,0},{1,11},{3,9},{9,3},{11,1},{4,14},{6,12},... | collective-permute-start | bytes 393224 | tf_op jit(solution)/shard_map/ppermute | solution.py:520
  154.9 4.7 %collective-permute-start.9 = (f32[256,128]{1,0:T(8,128)}, f32[256,128]{1,0:T(8,128)S(1)}, u32[]{:S(2)}, u32[]{:S(2)}) collective-permute-start(f32[256,128]{1,0:T(8,128)} %get-tuple-element.21), channel_id=1, source_target_pairs={{0,2},{2,0},{8,10},{10,8},{1,3},{3,1},{9,11},{11,9},{4,6},{6,4},{1... | collective-permute-start | bytes 393224 | tf_op jit(solution)/shard_map/ppermute | solution.py:520
  159.6 2.3 %selectors.1 = bf16[384,1024]{1,0:T(8,128)(2,1)} custom-call(s32[128,4]{1,0:T(8,128)} %get-tuple-element.24.target_ref, f32[4,128]{1,0:T(4,128)} %bitcast.45), custom_call_target="tpu_custom_call" | custom-call | tf_op jit(solution)/shard_map/selectors/pallas_call | solution.py:327
  161.9 0.0 collective-permute-done.10
  161.9 0.0 collective-permute-done.11
  162.0 1.7 %collective-permute-done.9 = f32[256,128]{1,0:T(8,128)S(1)} collective-permute-done((f32[256,128]{1,0:T(8,128)}, f32[256,128]{1,0:T(8,128)S(1)}, u32[]{:S(2)}, u32[]{:S(2)}) %collective-permute-start.9) | collective-permute-done | bytes 131104 | tf_op jit(solution)/shard_map/ppermute | solution.py:520
  163.6 1.6 add_convert_fusion
  165.2 1.5 fusion
  166.7 0.6 fusion.3
  (15 shorter events, 0.0 us)
Async XLA Ops:
  4.5 25.5 %collective-permute-start.2 = (bf16[6144,128]{1,0:T(8,128)(2,1)}, bf16[6144,128]{1,0:T(8,128)(2,1)}, u32[]{:S(2)}, u32[]{:S(2)}) collective-permute-start(bf16[6144,128]{1,0:T(8,128)(2,1)} %get-tuple-element.18.refs_0_), channel_id=1, source_target_pairs={{0,8},{1,9},{2,16},{3,17},{4,12},{5,13},{6,20},{7,21},{8,0},{9,1},... | collective-permute-start | bytes 4718600 | tf_op jit(solution)/shard_map/ppermute | solution.py:150
  10.6 43.7 %collective-permute-start.4 = (bf16[6144,128]{1,0:T(8,128)(2,1)}, bf16[6144,128]{1,0:T(8,128)(2,1)}, u32[]{:S(2)}, u32[]{:S(2)}) collective-permute-start(bf16[6144,128]{1,0:T(8,128)(2,1)} %get-tuple-element.18.refs_0_), channel_id=1, source_target_pairs={{0,16},{1,17},{2,8},{3,9},{4,20},{5,21},{6,12},{7,13},{8,24},{9,25... | collective-permute-start | bytes 4718600 | tf_op jit(solution)/shard_map/ppermute | solution.py:151
  14.6 41.0 %all-to-all-start = ((bf16[32,8,512]{2,1,0:T(8,128)(2,1)}), bf16[32,8,512]{2,1,0:T(8,128)(2,1)S(1)}, u32[]{:S(2)}, u32[]{:S(2)}) async-start(bf16[32,8,512]{2,1,0:T(8,128)(2,1)} %bitcast.38), calls=%async_computation | async-start | bytes 524288 | tf_op jit(solution)/shard_map/all_to_all | solution.py:25
  30.0 46.9 %collective-permute-start.3 = (bf16[6144,128]{1,0:T(8,128)(2,1)}, bf16[6144,128]{1,0:T(8,128)(2,1)S(1)}, u32[]{:S(2)}, u32[]{:S(2)}) collective-permute-start(bf16[6144,128]{1,0:T(8,128)(2,1)} %collective-permute-done.2.refs_1_), channel_id=1, source_target_pairs={{0,16},{1,17},{2,18},{3,19},{4,20},{5,21},{6,22},{7,23},{8,24},{9,... | collective-permute-start | bytes 4718600 | tf_op jit(solution)/shard_map/ppermute | solution.py:152
  54.3 22.6 %collective-permute-start.5 = (bf16[6144,128]{1,0:T(8,128)(2,1)}, bf16[6144,128]{1,0:T(8,128)(2,1)S(1)}, u32[]{:S(2)}, u32[]{:S(2)}) collective-permute-start(bf16[6144,128]{1,0:T(8,128)(2,1)} %collective-permute-done.4.refs_2_), channel_id=1, source_target_pairs={{0,16},{1,17},{4,20},{5,21},{8,24},{9,25},{12,28},{13,29},{18,2},{... | collective-permute-start | bytes 4718600 | tf_op jit(solution)/shard_map/ppermute | solution.py:153
  56.6 20.9 %all-to-all-start.1 = ((bf16[4,256,512]{2,1,0:T(8,128)(2,1)}), bf16[4,256,512]{2,1,0:T(8,128)(2,1)}, u32[]{:S(2)}, u32[]{:S(2)}) async-start(bf16[4,256,512]{2,1,0:T(8,128)(2,1)} %broadcast_in_dim.26), calls=%async_computation.1 | async-start | bytes 2097152 | tf_op jit(solution)/shard_map/all_to_all | solution.py:25
  65.3 4.4 %collective-permute-start = (bf16[128,128]{1,0:T(8,128)(2,1)}, bf16[128,128]{1,0:T(8,128)(2,1)S(1)}, u32[]{:S(2)}, u32[]{:S(2)}) collective-permute-start(bf16[128,128]{1,0:T(8,128)(2,1)} %get-tuple-element.16.refs_2_), channel_id=1, source_target_pairs={{0,16},{16,32},{32,48},{48,64},{64,80},{80,96},{96,112},{112,128},... | collective-permute-start | bytes 98312 | tf_op jit(solution)/shard_map/ppermute | solution.py:449
  67.2 5.8 %collective-permute-start.1 = (bf16[128,128]{1,0:T(8,128)(2,1)}, bf16[128,128]{1,0:T(8,128)(2,1)S(1)}, u32[]{:S(2)}, u32[]{:S(2)}) collective-permute-start(bf16[128,128]{1,0:T(8,128)(2,1)} %get-tuple-element.17.refs_1_), channel_id=1, source_target_pairs={{16,0},{32,16},{48,32},{64,48},{80,64},{96,80},{112,96},{128,112},... | collective-permute-start | bytes 98312 | tf_op jit(solution)/shard_map/ppermute | solution.py:450
  69.7 3.3 %copy-start.6 = (bf16[128,128]{1,0:T(8,128)(2,1)}, bf16[128,128]{1,0:T(8,128)(2,1)S(1)}, u32[]{:S(2)}) copy-start(bf16[128,128]{1,0:T(8,128)(2,1)S(1)} %collective-permute-done.refs_0_) | copy-start | bytes 98308
  73.1 0.6 copy-start.7
  76.8 1.2 copy-start
  76.9 1.6 copy-start.1
  103.6 21.2 %copy-start.2 = (bf16[2048,128]{1,0:T(8,128)(2,1)S(1)}, bf16[2048,128]{1,0:T(8,128)(2,1)}, u32[]{:S(2)}) copy-start(bf16[2048,128]{1,0:T(8,128)(2,1)} %param.19) | copy-start | bytes 1572868
  107.1 58.1 %all-to-all-start.3 = ((bf16[128,8,128]{2,1,0:T(8,128)(2,1)}), bf16[128,8,128]{2,1,0:T(8,128)(2,1)S(1)}, u32[]{:S(2)}, u32[]{:S(2)}) async-start(bf16[128,8,128]{2,1,0:T(8,128)(2,1)} %bitcast.37), calls=%async_computation.3 | async-start | bytes 524288 | tf_op jit(solution)/shard_map/all_to_all | solution.py:25
  125.6 11.4 %collective-permute-start.6 = (bf16[4,128,128]{2,1,0:T(8,128)(2,1)S(1)}, bf16[4,128,128]{2,1,0:T(8,128)(2,1)S(1)}, u32[]{:S(2)}, u32[]{:S(2)}) collective-permute-start(bf16[4,128,128]{2,1,0:T(8,128)(2,1)S(1)} %bitcast.41), channel_id=1, source_target_pairs={{0,2},{2,0},{8,10},{10,8},{1,3},{3,1},{9,11},{11,9},{4,6},{6,4},{1... | collective-permute-start | bytes 393224 | tf_op jit(solution)/shard_map/ppermute | solution.py:517
  130.3 8.7 %collective-permute-start.7 = (bf16[4,128,128]{2,1,0:T(8,128)(2,1)S(1)}, bf16[4,128,128]{2,1,0:T(8,128)(2,1)S(1)}, u32[]{:S(2)}, u32[]{:S(2)}) collective-permute-start(bf16[4,128,128]{2,1,0:T(8,128)(2,1)S(1)} %bitcast.40), channel_id=1, source_target_pairs={{0,8},{2,10},{8,0},{10,2},{1,9},{3,11},{9,1},{11,3},{4,12},{6,14},... | collective-permute-start | bytes 393224 | tf_op jit(solution)/shard_map/ppermute | solution.py:517
  134.9 10.4 %collective-permute-start.8 = (bf16[4,128,128]{2,1,0:T(8,128)(2,1)S(1)}, bf16[4,128,128]{2,1,0:T(8,128)(2,1)S(1)}, u32[]{:S(2)}, u32[]{:S(2)}) collective-permute-start(bf16[4,128,128]{2,1,0:T(8,128)(2,1)S(1)} %bitcast.39), channel_id=1, source_target_pairs={{0,10},{2,8},{8,2},{10,0},{1,11},{3,9},{9,3},{11,1},{4,14},{6,12},... | collective-permute-start | bytes 393224 | tf_op jit(solution)/shard_map/ppermute | solution.py:517
  137.0 8.3 %copy-start.3 = (bf16[4,128,128]{2,1,0:T(8,128)(2,1)}, bf16[4,128,128]{2,1,0:T(8,128)(2,1)S(1)}, u32[]{:S(2)}) copy-start(bf16[4,128,128]{2,1,0:T(8,128)(2,1)S(1)} %collective-permute-done.6.refs_1_) | copy-start | bytes 393220
  139.0 6.3 %copy-start.4 = (bf16[4,128,128]{2,1,0:T(8,128)(2,1)}, bf16[4,128,128]{2,1,0:T(8,128)(2,1)S(1)}, u32[]{:S(2)}) copy-start(bf16[4,128,128]{2,1,0:T(8,128)(2,1)S(1)} %collective-permute-done.7.refs_2_) | copy-start | bytes 393220
  145.3 0.7 copy-start.5
  148.2 13.7 %collective-permute-start.10 = (f32[256,128]{1,0:T(8,128)}, f32[256,128]{1,0:T(8,128)S(1)}, u32[]{:S(2)}, u32[]{:S(2)}) collective-permute-start(f32[256,128]{1,0:T(8,128)} %get-tuple-element.22), channel_id=1, source_target_pairs={{0,8},{2,10},{8,0},{10,2},{1,9},{3,11},{9,1},{11,3},{4,12},{6,14},... | collective-permute-start | bytes 393224 | tf_op jit(solution)/shard_map/ppermute | solution.py:520
  150.3 11.6 %collective-permute-start.11 = (f32[256,128]{1,0:T(8,128)}, f32[256,128]{1,0:T(8,128)S(1)}, u32[]{:S(2)}, u32[]{:S(2)}) collective-permute-start(f32[256,128]{1,0:T(8,128)} %get-tuple-element.23), channel_id=1, source_target_pairs={{0,10},{2,8},{8,2},{10,0},{1,11},{3,9},{9,3},{11,1},{4,14},{6,12},... | collective-permute-start | bytes 393224 | tf_op jit(solution)/shard_map/ppermute | solution.py:520
  154.9 8.7 %collective-permute-start.9 = (f32[256,128]{1,0:T(8,128)}, f32[256,128]{1,0:T(8,128)S(1)}, u32[]{:S(2)}, u32[]{:S(2)}) collective-permute-start(f32[256,128]{1,0:T(8,128)} %get-tuple-element.21), channel_id=1, source_target_pairs={{0,2},{2,0},{8,10},{10,8},{1,3},{3,1},{9,11},{11,9},{4,6},{6,4},{1... | collective-permute-start | bytes 393224 | tf_op jit(solution)/shard_map/ppermute | solution.py:520

commit v7 on v4

--- a/solution.py
+++ b/solution.py
@@ -246,66 +246,37 @@
     )(rows, mixed, arrived, *shares)
 
 
-def lowered(hidden, shares, slots):
-    parts, n, wide = hidden.shape
+def ordered(shares, parts):
     f = shares[0].shape[1]
     k = 4 * f
-    j = wide - k
     whole = parts * k
     half = k // 2
-
-    def kernel(hidden_ref, *refs):
-        shares, refs = refs[:5], refs[5:]
-        out_ref, heads_ref, here_ref, weights_ref, sems, row_sems = refs
+    places = list(itertools.product(range(2), repeat=3))
+
+    def kernel(*refs):
+        shares, (out_ref, sems) = refs[:5], refs[5:]
         native, order = share_order()
-        targets = [
-            (weights_ref.at[i // 2, :, pl.ds((i % 2) * f, f)], sems.at[i]) for i in range(4)
-        ]
-        arrivals = [
-            pltpu.make_async_copy(hidden_ref.at[part], here_ref.at[part], row_sems.at[part])
-            for part in range(parts)
-        ]
-        heads = pltpu.make_async_copy(
-            here_ref.at[:, :, pl.ds(k, j)], heads_ref, row_sems.at[parts]
-        )
-        for copy in arrivals:
-            copy.start()
         for i in range(4):
-            copy_share(native, shares, i, 2 * whole, whole, *targets[i])
-        for copy in arrivals:
-            copy.wait()
-        heads.start()
-        for target in targets:
-            pltpu.make_async_copy(shares[1].at[pl.ds(0, whole)], *target).wait()
-        for pair in range(2):
-            total = jnp.zeros((n, 2 * f), jnp.float32)
-            for Y, X, h in itertools.product(range(2), repeat=3):
-                unit = (8 * Y + 4 * h + 2 * X) * f
-                piece = here_ref[2 * Y + X, :, h * half : (h + 1) * half]
-                total = total + dot(piece, weights_ref[pair, unit : unit + half, :])
-            rounded = total.astype(jnp.bfloat16).reshape(n // slots, slots, 2 * f)
-            out_ref[:, order[2 * pair]] = rounded[:, :, :f]
-            out_ref[:, order[2 * pair + 1]] = rounded[:, :, f:]
-        heads.wait()
-
-    vmem = pl.BlockSpec(memory_space=pltpu.VMEM)
+            lane = pl.multiple_of(order[i] * f, f)
+            for n, (Y, X, h) in enumerate(places):
+                start = 2 * whole + (8 * Y + 4 * h + 2 * X) * f
+                target = out_ref.at[2 * Y + X, pl.ds(h * half, half), pl.ds(lane, f)]
+                copy_share(native, shares, i, start, half, target, sems.at[i, n])
+        for i in range(4):
+            for n in range(len(places)):
+                target = out_ref.at[0, pl.ds(0, half), pl.ds(0, f)]
+                source = shares[1].at[pl.ds(0, half)]
+                pltpu.make_async_copy(source, target, sems.at[i, n]).wait()
+
     anywhere = pl.BlockSpec(memory_space=pl.ANY)
     return pl.pallas_call(
         kernel,
-        out_shape=(
-            jax.ShapeDtypeStruct((n // slots, 4, slots, f), jnp.bfloat16),
-            jax.ShapeDtypeStruct((parts, n, j), jnp.bfloat16),
-        ),
-        in_specs=[anywhere] * 6,
-        out_specs=(vmem, anywhere),
-        scratch_shapes=[
-            pltpu.VMEM((parts, n, wide), jnp.bfloat16),
-            pltpu.VMEM((2, whole, 2 * f), jnp.bfloat16),
-            pltpu.SemaphoreType.DMA((4,)),
-            pltpu.SemaphoreType.DMA((parts + 1,)),
-        ],
-        name="lowered",
-    )(hidden, *shares)
+        out_shape=jax.ShapeDtypeStruct((parts, k, 4 * f), jnp.bfloat16),
+        in_specs=[anywhere] * 5,
+        out_specs=pl.BlockSpec(memory_space=pltpu.VMEM),
+        scratch_shapes=[pltpu.SemaphoreType.DMA((4, len(places)))],
+        name="ordered",
+    )(*shares)
 
 
 def selectors(target, logits, slots):
@@ -503,7 +474,12 @@
     arrived = shares[3][:8] + shares[4][:8]
     inner = gated(rows, mixed, shares, arrived)
     hidden = swap(inner, ("Y", "X"))
-    result, heads = lowered(hidden, shares, slots)
+    down = ordered(shares, 4)
+    result = jnp.einsum(
+        "qrl,qlf->rf", hidden[:, :, :width], down, preferred_element_type=jnp.float32
+    ).astype(jnp.bfloat16)
+    result = result.reshape(experts, slots, 4, -1).transpose(0, 2, 1, 3)
+    heads = hidden[:, :, width:]
     returned = swap(result.reshape(4 * experts, slots, -1), (*EP, "h", "p"))
     around = [[(i, i ^ k) for i in range(4)] for k in range(4)]
     size = mixed.shape[1]

time: 164 us -> 162 us (0.988)
  blocking collectives: 26 us -> 0 us
  waiting for transfers between devices: 11.4 us -> 24.8 us
  starting transfers between devices: 91.3 us -> 97.9 us
  matrix products: 1.5 us -> 4.52 us
    all_to_all x1 -> x0, blocking collectives: 26 us -> none  [swap(): return lax.all_to_all(pieces, axis, 0, 0, tiled=True)]
    all_to_all x3 -> x4, waiting for transfers between devices: 0.01 us -> 14.1 us  [swap(): return lax.all_to_all(pieces, axis, 0, 0, tiled=True)]
    all_to_all x3 -> x4, starting transfers between devices: 36.9 us -> 43.4 us  [swap(): return lax.all_to_all(pieces, axis, 0, 0, tiled=True)]
    dot_general x0 -> x1, matrix products: none -> 3.01 us  [shards(): jnp.einsum('qrl,qlf->rf', hidden[:, :, :width], down, preferred_element_t...]
  transfers between devices with their start and end apart: 15 -> 16, of which waited for: 5 -> 6; matrix products, arithmetic and copies ran while one was open for 3% -> 3% of each run, Pallas kernels for 7% -> 9%
where the time goes in v7:
time: 162 us; the launch traced here: 160 us
  starting transfers between devices  97.9 us (60%)
  waiting for transfers between devices  24.8 us (15%)
  Pallas kernels  23.2 us (14%)
  local copies, waits for them, and re-layouts  4.82 us (3%)
  matrix products  4.52 us (3%)
  other arithmetic  3.69 us (2%)
    all_to_all x4, starting transfers between devices, swap(): return lax.all_to_all(pieces, axis, 0, 0, tiled=True)  43.4 us
    ppermute x1, starting transfers between devices, gather_shares(): third = lax.ppermute(first, axes, device_pairs(trade))  25 us
    all_to_all x4, waiting for transfers between devices, swap(): return lax.all_to_all(pieces, axis, 0, 0, tiled=True)  14.1 us
    ppermute x3, starting transfers between devices, shards(): columns.append(lax.ppermute(piece, ('h', 'p'), around[k]) if k else piece)  8.36 us
    ppermute x3, starting transfers between devices, shards(): own_sum = own_sum + lax.ppermute(sums[k - 1], ('h', 'p'), around[k])  8.36 us
    pallas_call x1, Pallas kernels, gated(): pl.pallas_call(kernel, out_shape=jax.ShapeDtypeStruct((parts, n, 4 * u +...  4.98 us
    ppermute x3, waiting for transfers between devices, shards(): columns.append(lax.ppermute(piece, ('h', 'p'), around[k]) if k else piece)  4.73 us
    ppermute x1, starting transfers between devices, gather_shares(): first = lax.ppermute(own, axes, device_pairs(outer))  4.5 us
  transfers between devices with their start and end apart: 16, of which 6 were waited for; matrix products, arithmetic and copies ran while one was open for 3% of the time, Pallas kernels for 9%

profile of v7, /device:TPU:1, one launch (start us, length us, event | category | flops | bytes accessed | tf_op | source)
XLA Modules:
  0.0 159.9 jit_solution(6582273635771793103)
XLA Ops:
  0.6 3.8 %dispatch.1 = (bf16[256,512]{1,0:T(8,128)(2,1)}, s32[128,4]{1,0:T(8,128)}, bf16[6144,128]{1,0:T(8,128)(2,1)}) custom-call(bf16[128,2048]{1,0:T(8,128)(2,1)} %rows_ref.2, f32[1,2048]{1,0:T(1,128)} %bitcast.50, s32[4,128]{1,0:T(4,128)} %bitcast.52, bf16[2048,128]{1,0:T(8,128)(2,1)} %bitcast.39, bf16[2048,128]{1,0:T(8,128)(2,1)} %bitcast.40, ...), custom_call_target="tpu_custom_call" | custom-call | tf_op jit(solution)/shard_map/dispatch/pallas_call | solution.py:111
  4.5 4.5 %collective-permute-start.2 = (bf16[6144,128]{1,0:T(8,128)(2,1)}, bf16[6144,128]{1,0:T(8,128)(2,1)}, u32[]{:S(2)}, u32[]{:S(2)}) collective-permute-start(bf16[6144,128]{1,0:T(8,128)(2,1)} %get-tuple-element.16.refs_0_), channel_id=1, source_target_pairs={{0,4},{1,16},{2,6},{3,18},{4,0},{5,20},{6,2},{7,22},{8,12},{9,24},... | collective-permute-start | bytes 4718600 | tf_op jit(solution)/shard_map/ppermute | solution.py:150
  9.0 2.5 %collective-permute-start.4 = (bf16[6144,128]{1,0:T(8,128)(2,1)}, bf16[6144,128]{1,0:T(8,128)(2,1)}, u32[]{:S(2)}, u32[]{:S(2)}) collective-permute-start(bf16[6144,128]{1,0:T(8,128)(2,1)} %get-tuple-element.16.refs_0_), channel_id=1, source_target_pairs={{0,16},{1,4},{2,18},{3,6},{4,20},{5,0},{6,22},{7,2},{8,24},{9,12},... | collective-permute-start | bytes 4718600 | tf_op jit(solution)/shard_map/ppermute | solution.py:151
  11.5 15.4 %all-to-all-start = ((bf16[32,8,512]{2,1,0:T(8,128)(2,1)}), bf16[32,8,512]{2,1,0:T(8,128)(2,1)S(1)}, u32[]{:S(2)}, u32[]{:S(2)}) async-start(bf16[32,8,512]{2,1,0:T(8,128)(2,1)} %bitcast.46), calls=%async_computation | async-start | bytes 524288 | tf_op jit(solution)/shard_map/all_to_all | solution.py:25
  26.9 0.8 collective-permute-done.2.refs_1_
  27.7 25.0 %collective-permute-start.3 = (bf16[6144,128]{1,0:T(8,128)(2,1)}, bf16[6144,128]{1,0:T(8,128)(2,1)S(1)}, u32[]{:S(2)}, u32[]{:S(2)}) collective-permute-start(bf16[6144,128]{1,0:T(8,128)(2,1)} %collective-permute-done.2.refs_1_), channel_id=1, source_target_pairs={{0,16},{1,17},{2,18},{3,19},{4,20},{5,21},{6,22},{7,23},{8,24},{9,... | collective-permute-start | bytes 4718600 | tf_op jit(solution)/shard_map/ppermute | solution.py:152
  52.7 0.0 collective-permute-done.4.refs_2_
  52.7 1.3 collective-permute-start.5
  54.0 1.1 broadcast_in_dim.26
  55.0 4.2 %all-to-all-start.1 = ((bf16[4,256,512]{2,1,0:T(8,128)(2,1)}), bf16[4,256,512]{2,1,0:T(8,128)(2,1)}, u32[]{:S(2)}, u32[]{:S(2)}) async-start(bf16[4,256,512]{2,1,0:T(8,128)(2,1)} %broadcast_in_dim.26), calls=%async_computation.1 | async-start | bytes 2097152 | tf_op jit(solution)/shard_map/all_to_all | solution.py:25
  59.3 0.8 fusion.6
  60.2 3.5 %projections.1 = (bf16[256,128]{1,0:T(8,128)(2,1)}, bf16[128,128]{1,0:T(8,128)(2,1)}, bf16[128,128]{1,0:T(8,128)(2,1)}) custom-call(bf16[256,2048]{1,0:T(8,128)(2,1)} %rows_ref.3, f32[1,2048]{1,0:T(1,128)} %bitcast.51, bf16[2048,128]{1,0:T(8,128)(2,1)} %query_ref.1, bf16[64,2048]{1,0:T(8,128)(2,1)} %bitcast.44, bf16[64,2048]{1,0:T(8,128)(2,1)} %bitcast.45, ...), custom_call_target="tpu_custom_call" | custom-call | tf_op jit(solution)/shard_map/projections/pallas_call | solution.py:364
  63.7 1.9 %collective-permute-start = (bf16[128,128]{1,0:T(8,128)(2,1)}, bf16[128,128]{1,0:T(8,128)(2,1)S(1)}, u32[]{:S(2)}, u32[]{:S(2)}) collective-permute-start(bf16[128,128]{1,0:T(8,128)(2,1)} %get-tuple-element.14.refs_2_), channel_id=1, source_target_pairs={{0,16},{16,32},{32,48},{48,64},{64,80},{80,96},{96,112},{112,128},... | collective-permute-start | bytes 98312 | tf_op jit(solution)/shard_map/ppermute | solution.py:419
  65.6 2.5 %collective-permute-start.1 = (bf16[128,128]{1,0:T(8,128)(2,1)}, bf16[128,128]{1,0:T(8,128)(2,1)S(1)}, u32[]{:S(2)}, u32[]{:S(2)}) collective-permute-start(bf16[128,128]{1,0:T(8,128)(2,1)} %get-tuple-element.15.refs_1_), channel_id=1, source_target_pairs={{16,0},{32,16},{48,32},{64,48},{80,64},{96,80},{112,96},{128,112},... | collective-permute-start | bytes 98312 | tf_op jit(solution)/shard_map/ppermute | solution.py:420
  68.1 3.3 %collective-permute-done.1.refs_3_ = bf16[128,128]{1,0:T(8,128)(2,1)S(1)} collective-permute-done((bf16[128,128]{1,0:T(8,128)(2,1)}, bf16[128,128]{1,0:T(8,128)(2,1)S(1)}, u32[]{:S(2)}, u32[]{:S(2)}) %collective-permute-start.1) | collective-permute-done | bytes 32800 | tf_op jit(solution)/shard_map/ppermute | solution.py:420
  71.4 0.6 copy-done.7
  72.0 3.1 %banded.1.mixed_ref = bf16[256,128]{1,0:T(8,128)(2,1)} custom-call(f32[2]{0:T(128)} %sink_ref.1, bf16[256,128]{1,0:T(8,128)(2,1)} %get-tuple-element.13.query_ref, bf16[128,128]{1,0:T(8,128)(2,1)} %copy-done.6, bf16[128,128]{1,0:T(8,128)(2,1)} %get-tuple-element.15.refs_1_, bf16[128,128]{1,0:T(8,128)(2,1)} %get-tuple-element.14.refs_2_, ...), custom_call_target="tpu_custom_call" | custom-call | tf_op jit(solution)/shard_map/banded/pallas_call | solution.py:407
  75.2 0.0 collective-permute-done.3.refs_3_
  75.2 0.0 collective-permute-done.5.refs_4_
  75.2 0.6 slice_add_fusion.1._
  75.8 0.0 all-to-all-done.1.rows_ref
  75.8 0.6 copy-done
  76.4 0.5 copy-done.1
  76.9 5.0 %gated.1 = bf16[4,256,640]{2,1,0:T(8,128)(2,1)} custom-call(bf16[4,256,512]{2,1,0:T(8,128)(2,1)} %all-to-all-done.1.rows_ref, bf16[256,128]{1,0:T(8,128)(2,1)} %banded.1.mixed_ref, bf16[8,128]{1,0:T(8,128)(2,1)} %slice_add_fusion.1._, bf16[6144,128]{1,0:T(8,128)(2,1)} %get-tuple-element.16.refs_0_, bf16[6144,128]{1,0:T(8,128)(2,1)} %collective-permute-done.2.refs_1_, ...), custom_call_target="tpu_custom_call" | custom-call | tf_op jit(solution)/shard_map/gated/pallas_call | solution.py:232
  81.9 6.6 %all-to-all-start.2 = ((bf16[4,256,640]{2,1,0:T(8,128)(2,1)}), bf16[4,256,640]{2,1,0:T(8,128)(2,1)S(1)}, u32[]{:S(2)}, u32[]{:S(2)}) async-start(bf16[4,256,640]{2,1,0:T(8,128)(2,1)} %gated.1), calls=%async_computation.2 | async-start | bytes 2621440 | tf_op jit(solution)/shard_map/all_to_all | solution.py:25
  88.5 3.2 %ordered.1 = bf16[4,512,512]{2,1,0:T(8,128)(2,1)} custom-call(bf16[6144,128]{1,0:T(8,128)(2,1)} %get-tuple-element.16.refs_0_, bf16[6144,128]{1,0:T(8,128)(2,1)} %collective-permute-done.2.refs_1_, bf16[6144,128]{1,0:T(8,128)(2,1)} %collective-permute-done.4.refs_2_, bf16[6144,128]{1,0:T(8,128)(2,1)} %copy-done, bf16[6144,128]{1,0:T(8,128)(2,1)} %copy-done.1), custom_call_target="tpu_custom_call" | custom-call | tf_op jit(solution)/shard_map/ordered/pallas_call | solution.py:272
  91.7 0.0 copy-start.2
  91.7 14.1 %all-to-all-done.2 = bf16[4,256,640]{2,1,0:T(8,128)(2,1)S(1)} async-done(((bf16[4,256,640]{2,1,0:T(8,128)(2,1)}), bf16[4,256,640]{2,1,0:T(8,128)(2,1)S(1)}, u32[]{:S(2)}, u32[]{:S(2)}) %all-to-all-start.2) | async-done | bytes 1310752 | tf_op jit(solution)/shard_map/all_to_all | solution.py:25
  105.8 3.0 %fusion = bf16[256,512]{1,0:T(8,128)(2,1)} fusion(bf16[4,512,512]{2,1,0:T(8,128)(2,1)} %ordered.1, bf16[4,256,640]{2,1,0:T(8,128)(2,1)S(1)} %all-to-all-done.2), kind=kOutput, calls=%fused_computation.1 | convolution fusion | flops 537001984 | bytes 3407872 | tf_op jit(solution)/shard_map/qrl,qlf->rf/dot_general | solution.py:478
  108.8 17.2 %all-to-all-start.3 = ((bf16[128,8,128]{2,1,0:T(8,128)(2,1)}), bf16[128,8,128]{2,1,0:T(8,128)(2,1)S(1)}, u32[]{:S(2)}, u32[]{:S(2)}) async-start(bf16[128,8,128]{2,1,0:T(8,128)(2,1)} %bitcast.19), calls=%async_computation.3 | async-start | bytes 524288 | tf_op jit(solution)/shard_map/all_to_all | solution.py:25
  126.1 0.7 constant_dynamic-slice_fusion
  126.8 3.2 %collective-permute-start.6 = (bf16[4,128,128]{2,1,0:T(8,128)(2,1)S(1)}, bf16[4,128,128]{2,1,0:T(8,128)(2,1)S(1)}, u32[]{:S(2)}, u32[]{:S(2)}) collective-permute-start(bf16[4,128,128]{2,1,0:T(8,128)(2,1)S(1)} %bitcast.49), channel_id=1, source_target_pairs={{0,1},{1,0},{4,5},{5,4},{2,3},{3,2},{6,7},{7,6},{8,9},{9,8},{12,13... | collective-permute-start | bytes 393224 | tf_op jit(solution)/shard_map/ppermute | solution.py:492
  130.0 3.1 %collective-permute-start.7 = (bf16[4,128,128]{2,1,0:T(8,128)(2,1)S(1)}, bf16[4,128,128]{2,1,0:T(8,128)(2,1)S(1)}, u32[]{:S(2)}, u32[]{:S(2)}) collective-permute-start(bf16[4,128,128]{2,1,0:T(8,128)(2,1)S(1)} %bitcast.48), channel_id=1, source_target_pairs={{0,4},{1,5},{4,0},{5,1},{2,6},{3,7},{6,2},{7,3},{8,12},{9,13},{12,... | collective-permute-start | bytes 393224 | tf_op jit(solution)/shard_map/ppermute | solution.py:492
  133.1 2.0 %collective-permute-start.8 = (bf16[4,128,128]{2,1,0:T(8,128)(2,1)S(1)}, bf16[4,128,128]{2,1,0:T(8,128)(2,1)S(1)}, u32[]{:S(2)}, u32[]{:S(2)}) collective-permute-start(bf16[4,128,128]{2,1,0:T(8,128)(2,1)S(1)} %bitcast.47), channel_id=1, source_target_pairs={{0,5},{1,4},{4,1},{5,0},{2,7},{3,6},{6,3},{7,2},{8,13},{9,12},{12,... | collective-permute-start | bytes 393224 | tf_op jit(solution)/shard_map/ppermute | solution.py:492
  135.2 0.7 slice.33.heads_ref
  135.9 1.3 collective-permute-done.7.refs_2_
  137.2 3.4 %collective-permute-done.8.refs_3_ = bf16[4,128,128]{2,1,0:T(8,128)(2,1)S(1)} collective-permute-done((bf16[4,128,128]{2,1,0:T(8,128)(2,1)S(1)}, bf16[4,128,128]{2,1,0:T(8,128)(2,1)S(1)}, u32[]{:S(2)}, u32[]{:S(2)}) %collective-permute-start.8) | collective-permute-done | bytes 131104 | tf_op jit(solution)/shard_map/ppermute | solution.py:492
  140.6 0.7 copy-done.5
  141.3 2.3 %partial_sums.1 = (f32[256,128]{1,0:T(8,128)}, f32[256,128]{1,0:T(8,128)}, f32[256,128]{1,0:T(8,128)}, f32[256,128]{1,0:T(8,128)}) custom-call(bf16[4,256,128]{2,1,0:T(8,128)(2,1)} %slice.33.heads_ref, bf16[4,128,128]{2,1,0:T(8,128)(2,1)} %bitcast.43, bf16[4,128,128]{2,1,0:T(8,128)(2,1)} %copy-done.3, bf16[4,128,128]{2,1,0:T(8,128)(2,1)} %copy-done.4, ...), custom_call_target="tpu_custom_call" | custom-call | tf_op jit(solution)/shard_map/partial_sums/pallas_call | solution.py:437
  143.6 2.2 %collective-permute-start.10 = (f32[256,128]{1,0:T(8,128)}, f32[256,128]{1,0:T(8,128)S(1)}, u32[]{:S(2)}, u32[]{:S(2)}) collective-permute-start(f32[256,128]{1,0:T(8,128)} %get-tuple-element.19), channel_id=1, source_target_pairs={{0,4},{1,5},{4,0},{5,1},{2,6},{3,7},{6,2},{7,3},{8,12},{9,13},{12,... | collective-permute-start | bytes 393224 | tf_op jit(solution)/shard_map/ppermute | solution.py:495
  145.8 3.0 %collective-permute-start.11 = (f32[256,128]{1,0:T(8,128)}, f32[256,128]{1,0:T(8,128)S(1)}, u32[]{:S(2)}, u32[]{:S(2)}) collective-permute-start(f32[256,128]{1,0:T(8,128)} %get-tuple-element.20), channel_id=1, source_target_pairs={{0,5},{1,4},{4,1},{5,0},{2,7},{3,6},{6,3},{7,2},{8,13},{9,12},{12,... | collective-permute-start | bytes 393224 | tf_op jit(solution)/shard_map/ppermute | solution.py:495
  148.8 3.1 %collective-permute-start.9 = (f32[256,128]{1,0:T(8,128)}, f32[256,128]{1,0:T(8,128)S(1)}, u32[]{:S(2)}, u32[]{:S(2)}) collective-permute-start(f32[256,128]{1,0:T(8,128)} %get-tuple-element.18), channel_id=1, source_target_pairs={{0,1},{1,0},{4,5},{5,4},{2,3},{3,2},{6,7},{7,6},{8,9},{9,8},{12,13... | collective-permute-start | bytes 393224 | tf_op jit(solution)/shard_map/ppermute | solution.py:495
  152.0 2.3 %selectors.1 = bf16[384,1024]{1,0:T(8,128)(2,1)} custom-call(s32[128,4]{1,0:T(8,128)} %get-tuple-element.21.target_ref, f32[4,128]{1,0:T(4,128)} %bitcast.53), custom_call_target="tpu_custom_call" | custom-call | tf_op jit(solution)/shard_map/selectors/pallas_call | solution.py:297
  154.3 1.9 %collective-permute-done.9 = f32[256,128]{1,0:T(8,128)S(1)} collective-permute-done((f32[256,128]{1,0:T(8,128)}, f32[256,128]{1,0:T(8,128)S(1)}, u32[]{:S(2)}, u32[]{:S(2)}) %collective-permute-start.9) | collective-permute-done | bytes 131104 | tf_op jit(solution)/shard_map/ppermute | solution.py:495
  156.2 1.6 add_convert_fusion
  157.7 0.0 all-to-all-done.3
  157.7 1.5 fusion.2
  159.3 0.6 fusion.5
  (18 shorter events, 0.0 us)
Async XLA Ops:
  4.5 23.2 %collective-permute-start.2 = (bf16[6144,128]{1,0:T(8,128)(2,1)}, bf16[6144,128]{1,0:T(8,128)(2,1)}, u32[]{:S(2)}, u32[]{:S(2)}) collective-permute-start(bf16[6144,128]{1,0:T(8,128)(2,1)} %get-tuple-element.16.refs_0_), channel_id=1, source_target_pairs={{0,4},{1,16},{2,6},{3,18},{4,0},{5,20},{6,2},{7,22},{8,12},{9,24},... | collective-permute-start | bytes 4718600 | tf_op jit(solution)/shard_map/ppermute | solution.py:150
  9.0 43.7 %collective-permute-start.4 = (bf16[6144,128]{1,0:T(8,128)(2,1)}, bf16[6144,128]{1,0:T(8,128)(2,1)}, u32[]{:S(2)}, u32[]{:S(2)}) collective-permute-start(bf16[6144,128]{1,0:T(8,128)(2,1)} %get-tuple-element.16.refs_0_), channel_id=1, source_target_pairs={{0,16},{1,4},{2,18},{3,6},{4,20},{5,0},{6,22},{7,2},{8,24},{9,12},... | collective-permute-start | bytes 4718600 | tf_op jit(solution)/shard_map/ppermute | solution.py:151
  11.5 42.5 %all-to-all-start = ((bf16[32,8,512]{2,1,0:T(8,128)(2,1)}), bf16[32,8,512]{2,1,0:T(8,128)(2,1)S(1)}, u32[]{:S(2)}, u32[]{:S(2)}) async-start(bf16[32,8,512]{2,1,0:T(8,128)(2,1)} %bitcast.46), calls=%async_computation | async-start | bytes 524288 | tf_op jit(solution)/shard_map/all_to_all | solution.py:25
  27.7 47.5 %collective-permute-start.3 = (bf16[6144,128]{1,0:T(8,128)(2,1)}, bf16[6144,128]{1,0:T(8,128)(2,1)S(1)}, u32[]{:S(2)}, u32[]{:S(2)}) collective-permute-start(bf16[6144,128]{1,0:T(8,128)(2,1)} %collective-permute-done.2.refs_1_), channel_id=1, source_target_pairs={{0,16},{1,17},{2,18},{3,19},{4,20},{5,21},{6,22},{7,23},{8,24},{9,... | collective-permute-start | bytes 4718600 | tf_op jit(solution)/shard_map/ppermute | solution.py:152
  52.7 22.5 %collective-permute-start.5 = (bf16[6144,128]{1,0:T(8,128)(2,1)}, bf16[6144,128]{1,0:T(8,128)(2,1)S(1)}, u32[]{:S(2)}, u32[]{:S(2)}) collective-permute-start(bf16[6144,128]{1,0:T(8,128)(2,1)} %collective-permute-done.4.refs_2_), channel_id=1, source_target_pairs={{0,16},{2,18},{4,20},{6,22},{8,24},{10,26},{12,28},{14,30},{17,1},... | collective-permute-start | bytes 4718600 | tf_op jit(solution)/shard_map/ppermute | solution.py:153
  55.0 20.8 %all-to-all-start.1 = ((bf16[4,256,512]{2,1,0:T(8,128)(2,1)}), bf16[4,256,512]{2,1,0:T(8,128)(2,1)}, u32[]{:S(2)}, u32[]{:S(2)}) async-start(bf16[4,256,512]{2,1,0:T(8,128)(2,1)} %broadcast_in_dim.26), calls=%async_computation.1 | async-start | bytes 2097152 | tf_op jit(solution)/shard_map/all_to_all | solution.py:25
  63.7 4.4 %collective-permute-start = (bf16[128,128]{1,0:T(8,128)(2,1)}, bf16[128,128]{1,0:T(8,128)(2,1)S(1)}, u32[]{:S(2)}, u32[]{:S(2)}) collective-permute-start(bf16[128,128]{1,0:T(8,128)(2,1)} %get-tuple-element.14.refs_2_), channel_id=1, source_target_pairs={{0,16},{16,32},{32,48},{48,64},{64,80},{80,96},{96,112},{112,128},... | collective-permute-start | bytes 98312 | tf_op jit(solution)/shard_map/ppermute | solution.py:419
  65.6 5.8 %collective-permute-start.1 = (bf16[128,128]{1,0:T(8,128)(2,1)}, bf16[128,128]{1,0:T(8,128)(2,1)S(1)}, u32[]{:S(2)}, u32[]{:S(2)}) collective-permute-start(bf16[128,128]{1,0:T(8,128)(2,1)} %get-tuple-element.15.refs_1_), channel_id=1, source_target_pairs={{16,0},{32,16},{48,32},{64,48},{80,64},{96,80},{112,96},{128,112},... | collective-permute-start | bytes 98312 | tf_op jit(solution)/shard_map/ppermute | solution.py:420
  68.1 3.3 %copy-start.6 = (bf16[128,128]{1,0:T(8,128)(2,1)}, bf16[128,128]{1,0:T(8,128)(2,1)S(1)}, u32[]{:S(2)}) copy-start(bf16[128,128]{1,0:T(8,128)(2,1)S(1)} %collective-permute-done.refs_0_) | copy-start | bytes 98308
  71.4 0.6 copy-start.7
  75.2 1.2 copy-start
  75.2 1.7 %copy-start.1 = (bf16[6144,128]{1,0:T(8,128)(2,1)}, bf16[6144,128]{1,0:T(8,128)(2,1)S(1)}, u32[]{:S(2)}) copy-start(bf16[6144,128]{1,0:T(8,128)(2,1)S(1)} %collective-permute-done.5.refs_4_) | copy-start | bytes 4718596
  81.9 23.9 %all-to-all-start.2 = ((bf16[4,256,640]{2,1,0:T(8,128)(2,1)}), bf16[4,256,640]{2,1,0:T(8,128)(2,1)S(1)}, u32[]{:S(2)}, u32[]{:S(2)}) async-start(bf16[4,256,640]{2,1,0:T(8,128)(2,1)} %gated.1), calls=%async_computation.2 | async-start | bytes 2621440 | tf_op jit(solution)/shard_map/all_to_all | solution.py:25
  91.7 34.4 %copy-start.2 = (bf16[2048,128]{1,0:T(8,128)(2,1)S(1)}, bf16[2048,128]{1,0:T(8,128)(2,1)}, u32[]{:S(2)}) copy-start(bf16[2048,128]{1,0:T(8,128)(2,1)} %param.19) | copy-start | bytes 1572868
  108.8 49.0 %all-to-all-start.3 = ((bf16[128,8,128]{2,1,0:T(8,128)(2,1)}), bf16[128,8,128]{2,1,0:T(8,128)(2,1)S(1)}, u32[]{:S(2)}, u32[]{:S(2)}) async-start(bf16[128,8,128]{2,1,0:T(8,128)(2,1)} %bitcast.19), calls=%async_computation.3 | async-start | bytes 524288 | tf_op jit(solution)/shard_map/all_to_all | solution.py:25
  126.8 9.1 %collective-permute-start.6 = (bf16[4,128,128]{2,1,0:T(8,128)(2,1)S(1)}, bf16[4,128,128]{2,1,0:T(8,128)(2,1)S(1)}, u32[]{:S(2)}, u32[]{:S(2)}) collective-permute-start(bf16[4,128,128]{2,1,0:T(8,128)(2,1)S(1)} %bitcast.49), channel_id=1, source_target_pairs={{0,1},{1,0},{4,5},{5,4},{2,3},{3,2},{6,7},{7,6},{8,9},{9,8},{12,13... | collective-permute-start | bytes 393224 | tf_op jit(solution)/shard_map/ppermute | solution.py:492
  130.0 7.2 %collective-permute-start.7 = (bf16[4,128,128]{2,1,0:T(8,128)(2,1)S(1)}, bf16[4,128,128]{2,1,0:T(8,128)(2,1)S(1)}, u32[]{:S(2)}, u32[]{:S(2)}) collective-permute-start(bf16[4,128,128]{2,1,0:T(8,128)(2,1)S(1)} %bitcast.48), channel_id=1, source_target_pairs={{0,4},{1,5},{4,0},{5,1},{2,6},{3,7},{6,2},{7,3},{8,12},{9,13},{12,... | collective-permute-start | bytes 393224 | tf_op jit(solution)/shard_map/ppermute | solution.py:492
  133.1 7.5 %collective-permute-start.8 = (bf16[4,128,128]{2,1,0:T(8,128)(2,1)S(1)}, bf16[4,128,128]{2,1,0:T(8,128)(2,1)S(1)}, u32[]{:S(2)}, u32[]{:S(2)}) collective-permute-start(bf16[4,128,128]{2,1,0:T(8,128)(2,1)S(1)} %bitcast.47), channel_id=1, source_target_pairs={{0,5},{1,4},{4,1},{5,0},{2,7},{3,6},{6,3},{7,2},{8,13},{9,12},{12,... | collective-permute-start | bytes 393224 | tf_op jit(solution)/shard_map/ppermute | solution.py:492
  135.9 4.7 %copy-start.3 = (bf16[4,128,128]{2,1,0:T(8,128)(2,1)}, bf16[4,128,128]{2,1,0:T(8,128)(2,1)S(1)}, u32[]{:S(2)}) copy-start(bf16[4,128,128]{2,1,0:T(8,128)(2,1)S(1)} %collective-permute-done.6.refs_1_) | copy-start | bytes 393220
  137.2 3.5 %copy-start.4 = (bf16[4,128,128]{2,1,0:T(8,128)(2,1)}, bf16[4,128,128]{2,1,0:T(8,128)(2,1)S(1)}, u32[]{:S(2)}) copy-start(bf16[4,128,128]{2,1,0:T(8,128)(2,1)S(1)} %collective-permute-done.7.refs_2_) | copy-start | bytes 393220
  140.6 0.7 copy-start.5
  143.6 10.7 %collective-permute-start.10 = (f32[256,128]{1,0:T(8,128)}, f32[256,128]{1,0:T(8,128)S(1)}, u32[]{:S(2)}, u32[]{:S(2)}) collective-permute-start(f32[256,128]{1,0:T(8,128)} %get-tuple-element.19), channel_id=1, source_target_pairs={{0,4},{1,5},{4,0},{5,1},{2,6},{3,7},{6,2},{7,3},{8,12},{9,13},{12,... | collective-permute-start | bytes 393224 | tf_op jit(solution)/shard_map/ppermute | solution.py:495
  145.8 8.5 %collective-permute-start.11 = (f32[256,128]{1,0:T(8,128)}, f32[256,128]{1,0:T(8,128)S(1)}, u32[]{:S(2)}, u32[]{:S(2)}) collective-permute-start(f32[256,128]{1,0:T(8,128)} %get-tuple-element.20), channel_id=1, source_target_pairs={{0,5},{1,4},{4,1},{5,0},{2,7},{3,6},{6,3},{7,2},{8,13},{9,12},{12,... | collective-permute-start | bytes 393224 | tf_op jit(solution)/shard_map/ppermute | solution.py:495
  148.8 7.3 %collective-permute-start.9 = (f32[256,128]{1,0:T(8,128)}, f32[256,128]{1,0:T(8,128)S(1)}, u32[]{:S(2)}, u32[]{:S(2)}) collective-permute-start(f32[256,128]{1,0:T(8,128)} %get-tuple-element.18), channel_id=1, source_target_pairs={{0,1},{1,0},{4,5},{5,4},{2,3},{3,2},{6,7},{7,6},{8,9},{9,8},{12,13... | collective-permute-start | bytes 393224 | tf_op jit(solution)/shard_map/ppermute | solution.py:495
